TPU v7x, 128 devices: a whole 4x4x4 slice. The times are simulated.
128 devices in a mesh: rep: 2 (over z_hi), fs: 32 (over z_lo, y, x), tp: 2 (over core).
Axes of the slice: x: 4, y: 4, z: 4 (z_hi: 2, z_lo: 2; z = z_hi * 2 + z_lo), core: 2. Of those that a mesh axis runs over, the one named last changes fastest.
Arguments:
- tokens: bfloat16 [65536, 2048], P(('rep', 'fs')), may hold values from -6 to 6
- norm_mix: bfloat16 [2048], replicated, may hold values from 0.099609375 to 1.8984375
- w_unit: bfloat16 [2048, 1024], P('fs', 'tp'), may hold values from -0.125 to 0.125
- w_value: bfloat16 [2048, 1024], P('fs', 'tp'), may hold values from -0.125 to 0.125
- spatial: bfloat16 [4, 128, 128], replicated, may hold values from -0.52734375 to 0.52734375
- spatial_bias: bfloat16 [4, 128], replicated, may hold values from 0.099609375 to 1.8984375
- group_gain: bfloat16 [1024], replicated, may hold values from 0.099609375 to 1.8984375
- group_shift: bfloat16 [1024], replicated, may hold values from -3 to 3
- w_mix_out: bfloat16 [1024, 2048], P('tp', 'fs'), may hold values from -0.1875 to 0.1875
- norm_ffn: bfloat16 [2048], replicated, may hold values from 0.099609375 to 1.8984375
- w_gate: bfloat16 [2048, 2816], P('fs', 'tp'), may hold values from -0.125 to 0.125
- w_up: bfloat16 [2048, 2816], P('fs', 'tp'), may hold values from -0.125 to 0.125
- w_down: bfloat16 [2816, 2048], P('tp', 'fs'), may hold values from -0.109375 to 0.109375
Outputs:
- layer_out: bfloat16 [65536, 2048], P(('rep', 'fs', 'tp'))
All inputs are finite; a program needn't handle non-finite values.
Results may differ from a plain program's by a relative error of at most 0.008.
Values may be sent and summed in bfloat16 or wider, within the bound.
No kernel may reach another device: no remote copies, remote signals or barrier semaphores. Data moves between devices by JAX's collectives and lax.ppermute only.
A program may use at most 128 MiB of HBM per device.

v0:
```python
import functools

import jax
import jax.numpy as jnp
from jax import lax
from jax.experimental import pallas as pl
from jax.experimental.pallas import tpu as pltpu
from jax.sharding import PartitionSpec as P


EVERY = ("tp", "rep", "fs")
CHIPS = ("rep", "fs")
RING = 4
BF16, F32 = jnp.bfloat16, jnp.float32
ANY = pl.BlockSpec(memory_space=pl.ANY)
VMEM = pl.BlockSpec(memory_space=pltpu.VMEM)


def shift(x, axis, by):
    pairs = []
    for z in range(RING):
        for y in range(RING):
            for c in range(RING):
                to = [z, y, c]
                to[axis] = (to[axis] + by) % RING
                pairs.append(((z * RING + y) * RING + c, (to[0] * RING + to[1]) * RING + to[2]))
    return lax.ppermute(x, CHIPS, pairs)


def direct_ring(x, axis):
    return [x, shift(x, axis, 1), shift(x, axis, 2), shift(x, axis, 3)]


def passed_ring(x, axis, by):
    behind, ahead = shift(x, axis, 1), shift(x, axis, RING - 1)
    far = shift(behind if by == 1 else ahead, axis, by % RING)
    return [x, behind, far, ahead]


def relayed_ring(x, axis):
    half = x.shape[0] // 2
    behind, ahead = shift(x, axis, 1), shift(x, axis, RING - 1)
    return [x, behind, ahead, shift(behind[:half], axis, 1), shift(ahead[half:], axis, RING - 1)]


RELAYED = ((0, 0, 4, 0), (1, 0, 4, 1), (2, 0, 4, 3), (3, 0, 2, 2), (4, 2, 2, 2))


def in_place(pieces, position):
    out = []
    for j in range(RING):
        q = (position - j) % RING
        piece = pieces[0]
        for k in range(1, RING):
            piece = jnp.where(q == k, pieces[k], piece)
        out.append(piece)
    return jnp.stack(out)


def rms_scale(values, gain):
    values = values.astype(F32)
    scale = lax.rsqrt(jnp.mean(values * values, axis=-1, keepdims=True) + 1e-06)
    return values * scale * gain.astype(F32)


def dot_nn(a, b):
    return jnp.dot(a, b, preferred_element_type=F32)


def dot_nt(a, b):
    return lax.dot_general(a, b, (((1,), (1,)), ((), ())), preferred_element_type=F32)


def gelu(x):
    return 0.5 * x * (1.0 + jnp.tanh(0.7978845608028654 * (x + 0.044715 * (x * x * x))))


def mixer_body(own, *refs):
    normed_hbm = refs[0]
    for_unit, for_value, for_out = refs[1:6], refs[6:11], refs[11:16]
    mask_w, bias, gain, shifts, out, rows, w_unit, w_value, w_out, sem_x, sem_u, sem_v, sem_o = refs[16:]
    tp, rep, fs = lax.axis_index("tp"), lax.axis_index("rep"), lax.axis_index("fs")
    z, y, x_at = 2 * rep + fs // 16, fs // RING % RING, fs % RING
    count = rows.shape[0]
    start = pl.multiple_of((tp if own else 1 - tp) * count, count)
    pltpu.make_async_copy(normed_hbm.at[pl.ds(start, count)], rows, sem_x).start()
    part = w_unit.shape[3] // 2

    def line(ref, index, w, sem, at_z, at_y):
        to = pl.ds(pl.multiple_of(at_z // 2 * part, part), part)
        pltpu.make_async_copy(ref.at[index], w.at[at_z % 2, at_y, :, to], sem).start()

    for piece, low, inner, outer in RELAYED:
        at_z, at_y = (z + RING - outer) % RING, (y + RING - outer) % RING

        def copies(i, carry, piece=piece, low=low, outer=outer):
            near_z, near_y = (z + RING - low - i) % RING, (y + RING - low - i) % RING
            line(for_value[piece], i, w_value, sem_v, near_z, at_y)
            line(for_unit[piece], i, w_unit, sem_u, at_z, near_y)
            for r in range(2):
                pltpu.make_async_copy(
                    for_out[piece].at[i, pl.ds(2 * r, 2)],
                    w_out.at[:, near_y, (x_at + RING - outer) % RING, pl.ds(r * part, part)],
                    sem_o,
                ).start()
            return carry

        lax.fori_loop(0, inner, copies, 0)

    pltpu.make_async_copy(normed_hbm.at[pl.ds(start, count)], rows, sem_x).wait()
    pltpu.make_async_copy(w_value, w_value, sem_v).wait()
    x = rows[...]
    model, width = x.shape[1], w_value.shape[-1]
    value = gelu(dot_nn(x, w_value[...].reshape(model, width)))
    pltpu.make_async_copy(w_unit, w_unit, sem_u).wait()
    unit = gelu(dot_nn(x, w_unit[...].reshape(model, width)))
    groups, block = mask_w.shape[0], mask_w.shape[1]
    per = width // groups
    parts = []
    for g in range(groups):
        a = value[:, g * per : (g + 1) * per]
        a = a - jnp.mean(a, axis=-1, keepdims=True)
        a = a * lax.rsqrt(jnp.mean(a * a, axis=-1, keepdims=True) + 1e-06)
        a = a * gain[:, g * per : (g + 1) * per] + shifts[:, g * per : (g + 1) * per]
        a = a.astype(BF16)
        mixed = [
            dot_nn(mask_w[g], a[n * block : (n + 1) * block]) + bias[:, g : g + 1]
            for n in range(count // block)
        ]
        parts.append((unit[:, g * per : (g + 1) * per] * jnp.concatenate(mixed, axis=0)).astype(BF16))
    gated = jnp.concatenate(parts, axis=1)
    pltpu.make_async_copy(w_out, w_out, sem_o).wait()
    out[...] = dot_nt(gated, w_out[...].reshape(model, width)).astype(out.dtype)


def mixer(own, normed, pieces, mask_w, bias, gain, shifts, count, dtype):
    model, width = normed.shape[1], pieces[0].shape[-1]
    weight = pltpu.VMEM((2, RING, RING, model // 32, width), BF16)
    return pl.pallas_call(
        functools.partial(mixer_body, own),
        out_shape=jax.ShapeDtypeStruct((count, model), dtype),
        in_specs=[ANY] * 16 + [VMEM] * 4,
        out_specs=VMEM,
        scratch_shapes=[pltpu.VMEM((count, model), BF16), weight, weight, weight] + [pltpu.SemaphoreType.DMA] * 4,
        compiler_params=pltpu.CompilerParams(vmem_limit_bytes=56 * 2**20),
        name="mixer_own" if own else "mixer_other",
    )(normed, *pieces, mask_w, bias, gain, shifts)


CHUNK = 512


def ffn_body(h_hbm, n_hbm, packed, out_hbm, h_mid, normed, mid, down, hidden, out, sem_h, sem_n, sem_w, sem_d, sem_o):
    tps, share, wide = packed.shape[0], down.shape[2], packed.shape[-1]
    _, model = out.shape
    starts = list(range(0, tps * wide, CHUNK))
    sizes = [min(CHUNK, tps * wide - at) for at in starts]

    def columns(j):
        copies = []
        for w in range(2):
            low, end = starts[j], starts[j] + sizes[j]
            while low < end:
                t = low // wide
                high = min(end, (t + 1) * wide)
                to = starts[j] + w * sizes[j] + low
                copies.append(
                    pltpu.make_async_copy(
                        packed.at[t, w, :, pl.ds(0, share), pl.ds(low - t * wide, high - low)],
                        mid.at[:, :, pl.ds(to, high - low)],
                        sem_w.at[j],
                    )
                )
                low = high
        return copies

    def downs(t):
        half = share // 2
        return [
            pltpu.make_async_copy(
                packed.at[t, r, :, pl.ds(share, half)], down.at[t, :, pl.ds(r * half, half)], sem_d
            )
            for r in range(2)
        ]

    rows = pltpu.make_async_copy(n_hbm, normed, sem_n)
    mids = pltpu.make_async_copy(h_hbm, h_mid, sem_h)
    rows.start()
    for j in range(len(sizes)):
        for copy in columns(j):
            copy.start()
    for t in range(tps):
        for copy in downs(t):
            copy.start()
    mids.start()
    rows.wait()

    def up_to(j, at, size):
        w = mid.at[:, :, pl.ds(2 * at, 2 * size)]
        pltpu.make_async_copy(w, w, sem_w.at[j]).wait()
        r = dot_nn(normed[...], w[...].reshape(model, 2 * size))
        hidden[:, pl.ds(at, size)] = (jax.nn.silu(r[:, :size]) * r[:, size:]).astype(BF16)

    def whole(j, carry):
        up_to(j, pl.multiple_of(j * CHUNK, CHUNK), CHUNK)
        return carry

    full = tps * wide // CHUNK
    lax.fori_loop(0, full, whole, 0)
    if full < len(sizes):
        up_to(full, starts[full], sizes[full])
    pltpu.make_async_copy(down, down, sem_d).wait()
    mids.wait()

    def leave(k):
        cols = pl.ds(pl.multiple_of(k * CHUNK, CHUNK), CHUNK)
        return pltpu.make_async_copy(out.at[:, cols], out_hbm.at[:, cols], sem_o.at[k])

    lines = CHUNK // share

    def back(k, carry):
        cols = pl.ds(pl.multiple_of(k * CHUNK, CHUNK), CHUNK)
        acc = h_mid[:, cols].astype(F32)
        for t in range(tps):
            w = down[t, pl.ds(k * lines, lines)].reshape(CHUNK, wide)
            acc = acc + dot_nt(hidden[:, t * wide : (t + 1) * wide], w)
        out[:, cols] = acc.astype(BF16)
        leave(k).start()
        return carry

    lax.fori_loop(0, model // CHUNK, back, 0)
    for k in range(model // CHUNK):
        leave(k).wait()


def ffn(h_mid, normed, packed, share):
    tps, _, fs, _, wide = packed.shape
    row = pltpu.VMEM(h_mid.shape, BF16)
    return pl.pallas_call(
        ffn_body,
        out_shape=jax.ShapeDtypeStruct(h_mid.shape, BF16),
        in_specs=[ANY] * 3,
        out_specs=ANY,
        scratch_shapes=[
            row, row, pltpu.VMEM((fs, share, 2 * tps * wide), BF16), pltpu.VMEM((tps, fs, share, wide), BF16),
            pltpu.VMEM((h_mid.shape[0], tps * wide), BF16), row,
            pltpu.SemaphoreType.DMA, pltpu.SemaphoreType.DMA, pltpu.SemaphoreType.DMA((-(-tps * wide // CHUNK),)),
            pltpu.SemaphoreType.DMA, pltpu.SemaphoreType.DMA((h_mid.shape[1] // CHUNK,)),
        ],
        compiler_params=pltpu.CompilerParams(vmem_limit_bytes=58 * 2**20),
        name="ffn",
    )(h_mid, normed, packed)


def half_rows(x, part):
    size = x.shape[0] // 2
    return lax.dynamic_slice_in_dim(x, part * size, size, 0)


def on_device(
    tokens, norm_mix, w_unit, w_value, spatial, spatial_bias, group_gain, group_shift,
    w_mix_out, norm_ffn, w_gate, w_up, w_down,
):
    tp, rep, fs = (lax.axis_index(a) for a in ("tp", "rep", "fs"))
    tps, reps, fss = (lax.axis_size(a) for a in ("tp", "rep", "fs"))
    rows = tokens.shape[0] // tps
    share, width = w_unit.shape

    packed = jnp.concatenate([jnp.where(rep == 0, w_gate, w_up), half_rows(w_down.T, rep)], axis=0)
    packed = lax.all_gather(packed, EVERY).reshape(tps, reps, fss, *packed.shape)

    part = share // 2
    line = jnp.concatenate([half_rows(w_unit, rep), half_rows(w_value, rep)], axis=0)
    line = in_place(direct_ring(line, 2), fs % RING)
    for_unit = relayed_ring(jnp.stack(passed_ring(line[:, :part], 1, 1)), 0)
    for_value = relayed_ring(jnp.stack(passed_ring(line[:, part:], 0, 1)), 1)
    for_out = in_place(direct_ring(half_rows(w_mix_out.T, rep), 0), 2 * rep + fs // 16)
    for_out = relayed_ring(jnp.stack(passed_ring(for_out, 1, -1)), 2)

    groups = spatial.shape[0] // tps
    causal = jnp.tril(jnp.ones(spatial.shape[1:], dtype=bool))
    mask_w = lax.dynamic_slice_in_dim(jnp.where(causal[None], spatial, 0), tp * groups, groups, 0)
    bias = lax.dynamic_slice_in_dim(spatial_bias, tp * groups, groups, 0).astype(F32).T
    gain = lax.dynamic_slice_in_dim(group_gain, tp * width, width, 0).astype(F32)[None]
    shifts = lax.dynamic_slice_in_dim(group_shift, tp * width, width, 0).astype(F32)[None]
    normed = rms_scale(tokens, norm_mix).astype(BF16)

    unit = functools.partial(
        mixer, normed=normed, pieces=(*for_unit, *for_value, *for_out), mask_w=mask_w, bias=bias, gain=gain,
        shifts=shifts, count=rows,
    )
    other = unit(False, dtype=BF16)
    arrived = lax.ppermute(other, "tp", [(i, (i + 1) % tps) for i in range(tps)])
    kept = unit(True, dtype=F32)
    residual = lax.dynamic_slice_in_dim(tokens, tp * rows, rows, 0).astype(F32)
    h_mid = (residual + (kept + arrived.astype(F32))).astype(BF16)
    normed_mid = rms_scale(h_mid, norm_ffn).astype(BF16)
    return ffn(h_mid, normed_mid, packed, share)


def solution(mesh):
    placed = (
        P(("rep", "fs"), None), P(), P("fs", "tp"), P("fs", "tp"), P(), P(), P(), P(),
        P("tp", "fs"), P(), P("fs", "tp"), P("fs", "tp"), P("tp", "fs"),
    )

    return jax.shard_map(on_device, mesh=mesh, in_specs=placed, out_specs=P(("rep", "fs", "tp"), None), check_vma=False)
```

profile of v0, /device:TPU:1, one launch (start us, length us, event | category | flops | bytes accessed | tf_op | source)
XLA Modules:
  0.0 167.0 jit_solution(12950101266955865874)
XLA Ops:
  7.5 1.0 broadcast_select_fusion
  9.9 4.6 %collective-permute-start.17 = (bf16[32,512]{1,0:T(8,128)(2,1)S(1)}, bf16[32,512]{1,0:T(8,128)(2,1)S(1)}, u32[]{:S(2)}, u32[]{:S(2)}) collective-permute-start(bf16[32,512]{1,0:T(8,128)(2,1)S(1)} %dynamic-slice_bitcast_fusion.1), channel_id=1, source_target_pairs={{0,96},{2,98},{4,100},{6,102},{8,104},{10,106},{12,108},{14,110},{... | collective-permute-start | bytes 98312 | tf_op jit(solution)/shard_map/ppermute | solution.py:27
  16.0 2.5 %collective-permute-start = (bf16[64,512]{1,0:T(8,128)(2,1)S(1)}, bf16[64,512]{1,0:T(8,128)(2,1)S(1)}, u32[]{:S(2)}, u32[]{:S(2)}) collective-permute-start(bf16[64,512]{1,0:T(8,128)(2,1)S(1)} %pad_maximum_fusion.6), channel_id=1, source_target_pairs={{0,6},{2,0},{4,2},{6,4},{8,14},{10,8},{12,10},{14,12},{16,22},{18,... | collective-permute-start | bytes 196616 | tf_op jit(solution)/shard_map/ppermute | solution.py:27
  20.5 2.8 %collective-permute-start.21 = (bf16[4,32,512]{2,1,0:T(8,128)(2,1)S(1)}, bf16[4,32,512]{2,1,0:T(8,128)(2,1)S(1)}, u32[]{:S(2)}, u32[]{:S(2)}) collective-permute-start(bf16[4,32,512]{2,1,0:T(8,128)(2,1)S(1)} %get-tuple-element.15), channel_id=1, source_target_pairs={{0,24},{2,26},{4,28},{6,30},{8,0},{10,2},{12,4},{14,6},{16,8},{18,... | collective-permute-start | bytes 393224 | tf_op jit(solution)/shard_map/ppermute | solution.py:27
  24.1 1.5 collective-permute-done.21
  25.5 3.5 %collective-permute-start.22 = (bf16[4,32,512]{2,1,0:T(8,128)(2,1)S(1)}, bf16[4,32,512]{2,1,0:T(8,128)(2,1)S(1)}, u32[]{:S(2)}, u32[]{:S(2)}) collective-permute-start(bf16[4,32,512]{2,1,0:T(8,128)(2,1)S(1)} %collective-permute-done.21), channel_id=1, source_target_pairs={{0,24},{2,26},{4,28},{6,30},{8,0},{10,2},{12,4},{14,6},{16,8},{18,... | collective-permute-start | bytes 393224 | tf_op jit(solution)/shard_map/ppermute | solution.py:27
  29.1 2.7 %collective-permute-start.10 = (bf16[4,32,512]{2,1,0:T(8,128)(2,1)S(1)}, bf16[4,32,512]{2,1,0:T(8,128)(2,1)S(1)}, u32[]{:S(2)}, u32[]{:S(2)}) collective-permute-start(bf16[4,32,512]{2,1,0:T(8,128)(2,1)S(1)} %get-tuple-element.9), channel_id=1, source_target_pairs={{0,32},{2,34},{4,36},{6,38},{8,40},{10,42},{12,44},{14,46},{16,48}... | collective-permute-start | bytes 393224 | tf_op jit(solution)/shard_map/ppermute | solution.py:27
  31.9 1.7 %collective-permute-start.23 = (bf16[4,4,32,512]{3,2,1,0:T(8,128)(2,1)S(1)}, bf16[4,4,32,512]{3,2,1,0:T(8,128)(2,1)S(1)}, u32[]{:S(2)}, u32[]{:S(2)}) collective-permute-start(bf16[4,4,32,512]{3,2,1,0:T(8,128)(2,1)S(1)} %pad_maximum_fusion.2.refs_11_), channel_id=1, source_target_pairs={{0,2},{2,4},{4,6},{6,0},{8,10},{10,12},{12,14},{14,8},{16,18},{18,... | collective-permute-start | bytes 1572872 | tf_op jit(solution)/shard_map/ppermute | solution.py:27
  33.6 3.1 %fusion = f32[1024]{0:T(1024)S(1)} fusion(bf16[1024,2048]{1,0:T(8,128)(2,1)} %param.13), kind=kLoop, calls=%fused_computation.2 | loop fusion | flops 6290432 | bytes 4198400 | tf_op jit(solution)/shard_map/reduce_sum | solution.py:62
  37.6 3.6 %collective-permute-start.5 = (bf16[4,32,512]{2,1,0:T(8,128)(2,1)S(1)}, bf16[4,32,512]{2,1,0:T(8,128)(2,1)S(1)}, u32[]{:S(2)}, u32[]{:S(2)}) collective-permute-start(bf16[4,32,512]{2,1,0:T(8,128)(2,1)S(1)} %get-tuple-element.10), channel_id=1, source_target_pairs={{0,24},{2,26},{4,28},{6,30},{8,0},{10,2},{12,4},{14,6},{16,8},{18,... | collective-permute-start | bytes 393224 | tf_op jit(solution)/shard_map/ppermute | solution.py:27
  41.9 1.2 collective-permute-start.24
  43.1 3.4 %collective-permute-done.11 = bf16[4,32,512]{2,1,0:T(8,128)(2,1)S(1)} collective-permute-done((bf16[4,32,512]{2,1,0:T(8,128)(2,1)S(1)}, bf16[4,32,512]{2,1,0:T(8,128)(2,1)S(1)}, u32[]{:S(2)}, u32[]{:S(2)}) %collective-permute-start.11) | collective-permute-done | bytes 131104 | tf_op jit(solution)/shard_map/ppermute | solution.py:27
  46.7 2.7 %collective-permute-start.14 = (bf16[4,4,32,512]{3,2,1,0:T(8,128)(2,1)S(1)}, bf16[4,4,32,512]{3,2,1,0:T(8,128)(2,1)}, u32[]{:S(2)}, u32[]{:S(2)}) collective-permute-start(bf16[4,4,32,512]{3,2,1,0:T(8,128)(2,1)S(1)} %pad_maximum_fusion.1.refs_6_), channel_id=1, source_target_pairs={{0,24},{2,26},{4,28},{6,30},{8,0},{10,2},{12,4},{14,6},{16,8},{18,... | collective-permute-start | bytes 1572872 | tf_op jit(solution)/shard_map/ppermute | solution.py:27
  49.6 2.6 %collective-permute-start.7 = (bf16[4,4,32,512]{3,2,1,0:T(8,128)(2,1)S(1)}, bf16[4,4,32,512]{3,2,1,0:T(8,128)(2,1)}, u32[]{:S(2)}, u32[]{:S(2)}) collective-permute-start(bf16[4,4,32,512]{3,2,1,0:T(8,128)(2,1)S(1)} %pad_maximum_fusion.refs_1_), channel_id=1, source_target_pairs={{0,96},{2,98},{4,100},{6,102},{8,104},{10,106},{12,108},{14,110},{... | collective-permute-start | bytes 1572872 | tf_op jit(solution)/shard_map/ppermute | solution.py:27
  52.3 3.0 %fusion.2.refs_0_ = bf16[1024,2048]{1,0:T(8,128)(2,1)} fusion(bf16[1024,2048]{1,0:T(8,128)(2,1)S(1)} %copy-done.2, f32[2048]{0:T(1024)S(1)} %convert_element_type.34, f32[1024]{0:T(1024)S(1)} %add_rsqrt_fusion), kind=kLoop, calls=%fused_computation.4 | loop fusion | flops 8388608 | bytes 8400896 | tf_op jit(solution)/shard_map/convert_element_type | solution.py:286
  56.0 3.8 %collective-permute-done.24.refs_13_ = bf16[4,4,32,512]{3,2,1,0:T(8,128)(2,1)S(1)} collective-permute-done((bf16[4,4,32,512]{3,2,1,0:T(8,128)(2,1)S(1)}, bf16[4,4,32,512]{3,2,1,0:T(8,128)(2,1)S(1)}, u32[]{:S(2)}, u32[]{:S(2)}) %collective-permute-start.24) | collective-permute-done | bytes 524320 | tf_op jit(solution)/shard_map/ppermute | solution.py:27
  62.0 8.4 %collective-permute-done.13.refs_7_ = bf16[4,4,32,512]{3,2,1,0:T(8,128)(2,1)S(1)} collective-permute-done((bf16[4,4,32,512]{3,2,1,0:T(8,128)(2,1)S(1)}, bf16[4,4,32,512]{3,2,1,0:T(8,128)(2,1)S(1)}, u32[]{:S(2)}, u32[]{:S(2)}) %collective-permute-start.13) | collective-permute-done | bytes 524320 | tf_op jit(solution)/shard_map/ppermute | solution.py:27
  70.4 2.0 %collective-permute-start.26 = (bf16[2,4,32,512]{3,2,1,0:T(8,128)(2,1)}, bf16[2,4,32,512]{3,2,1,0:T(8,128)(2,1)S(1)}, u32[]{:S(2)}, u32[]{:S(2)}) collective-permute-start(bf16[2,4,32,512]{3,2,1,0:T(8,128)(2,1)} %slice.39), channel_id=1, source_target_pairs={{0,6},{2,0},{4,2},{6,4},{8,14},{10,8},{12,10},{14,12},{16,22},{18,... | collective-permute-start | bytes 786440 | tf_op jit(solution)/shard_map/ppermute | solution.py:27
  73.2 1.7 %slice.37 = bf16[2,4,32,512]{3,2,1,0:T(8,128)(2,1)} slice(bf16[4,4,32,512]{3,2,1,0:T(8,128)(2,1)} %collective-permute-done.14.refs_8_), slice={[2:4], [0:4], [0:32], [0:512]} | slice | bytes 524288 | tf_op jit(solution)/shard_map/slice | solution.py:43
  74.9 2.7 %collective-permute-start.16 = (bf16[2,4,32,512]{3,2,1,0:T(8,128)(2,1)}, bf16[2,4,32,512]{3,2,1,0:T(8,128)(2,1)S(1)}, u32[]{:S(2)}, u32[]{:S(2)}) collective-permute-start(bf16[2,4,32,512]{3,2,1,0:T(8,128)(2,1)} %slice.37), channel_id=1, source_target_pairs={{0,24},{2,26},{4,28},{6,30},{8,0},{10,2},{12,4},{14,6},{16,8},{18,... | collective-permute-start | bytes 786440 | tf_op jit(solution)/shard_map/ppermute | solution.py:27
  77.5 1.7 %slice.33 = bf16[2,4,32,512]{3,2,1,0:T(8,128)(2,1)} slice(bf16[4,4,32,512]{3,2,1,0:T(8,128)(2,1)} %collective-permute-done.6.refs_2_), slice={[0:2], [0:4], [0:32], [0:512]} | slice | bytes 524288 | tf_op jit(solution)/shard_map/slice | solution.py:43
  79.3 1.0 slice.34
  80.4 2.7 %collective-permute-start.9 = (bf16[2,4,32,512]{3,2,1,0:T(8,128)(2,1)S(1)}, bf16[2,4,32,512]{3,2,1,0:T(8,128)(2,1)S(1)}, u32[]{:S(2)}, u32[]{:S(2)}) collective-permute-start(bf16[2,4,32,512]{3,2,1,0:T(8,128)(2,1)S(1)} %slice.34), channel_id=1, source_target_pairs={{0,96},{2,98},{4,100},{6,102},{8,104},{10,106},{12,108},{14,110},{... | collective-permute-start | bytes 786440 | tf_op jit(solution)/shard_map/ppermute | solution.py:27
  83.9 4.0 %collective-permute-done.16.refs_10_ = bf16[2,4,32,512]{3,2,1,0:T(8,128)(2,1)S(1)} collective-permute-done((bf16[2,4,32,512]{3,2,1,0:T(8,128)(2,1)}, bf16[2,4,32,512]{3,2,1,0:T(8,128)(2,1)S(1)}, u32[]{:S(2)}, u32[]{:S(2)}) %collective-permute-start.16) | collective-permute-done | bytes 262176 | tf_op jit(solution)/shard_map/ppermute | solution.py:27
  87.9 5.6 %collective-permute-done.8.refs_4_ = bf16[2,4,32,512]{3,2,1,0:T(8,128)(2,1)S(1)} collective-permute-done((bf16[2,4,32,512]{3,2,1,0:T(8,128)(2,1)}, bf16[2,4,32,512]{3,2,1,0:T(8,128)(2,1)S(1)}, u32[]{:S(2)}, u32[]{:S(2)}) %collective-permute-start.8) | collective-permute-done | bytes 262176 | tf_op jit(solution)/shard_map/ppermute | solution.py:27
  94.2 9.9 %mixer_other.1 = bf16[512,2048]{1,0:T(8,128)(2,1)} custom-call(bf16[1024,2048]{1,0:T(8,128)(2,1)} %fusion.2.refs_0_, bf16[4,4,32,512]{3,2,1,0:T(8,128)(2,1)} %copy-done.7, bf16[4,4,32,512]{3,2,1,0:T(8,128)(2,1)} %collective-permute-done.6.refs_2_, bf16[4,4,32,512]{3,2,1,0:T(8,128)(2,1)} %collective-permute-done.7.refs_3_, ...), custom_call_target="tpu_custom_call" | custom-call | tf_op jit(solution)/shard_map/mixer_other/pallas_call | solution.py:139
  104.2 5.3 %collective-permute-start.27 = (bf16[512,2048]{1,0:T(8,128)(2,1)}, bf16[512,2048]{1,0:T(8,128)(2,1)}, u32[]{:S(2)}, u32[]{:S(2)}) collective-permute-start(bf16[512,2048]{1,0:T(8,128)(2,1)} %mixer_other.1), channel_id=1, source_target_pairs={{0,1},{1,0},{2,3},{3,2},{4,5},{5,4},{6,7},{7,6},{8,9},{9,8},{10,11... | collective-permute-start | bytes 6291464 | tf_op jit(solution)/shard_map/ppermute | solution.py:293
  109.5 11.8 %mixer_own.1 = f32[512,2048]{1,0:T(8,128)} custom-call(bf16[1024,2048]{1,0:T(8,128)(2,1)} %fusion.2.refs_0_, bf16[4,4,32,512]{3,2,1,0:T(8,128)(2,1)} %copy-done.7, bf16[4,4,32,512]{3,2,1,0:T(8,128)(2,1)} %collective-permute-done.6.refs_2_, bf16[4,4,32,512]{3,2,1,0:T(8,128)(2,1)} %collective-permute-done.7.refs_3_, bf16[2,4,32,512]{3,2,1,0:T(8,128)(2,1)} %copy-done.15, ...), custom_call_target="tpu_custom_call" | custom-call | tf_op jit(solution)/shard_map/mixer_own/pallas_call | solution.py:139
  121.3 4.3 %fusion.3 = (f32[512]{0:T(512)S(1)}, bf16[512,2048]{1,0:T(8,128)(2,1)S(1)}) fusion(f32[512,2048]{1,0:T(8,128)} %mixer_own.1, bf16[512,2048]{1,0:T(8,128)(2,1)} %collective-permute-done.27, bf16[1024,2048]{1,0:T(8,128)(2,1)S(1)} %copy-done.3, s32[]{:T(128)S(6)} %select_n.220), kind=kLoop, calls=%fused_computation.7 | loop fusion | flops 8388096 | bytes 10487812 | tf_op jit(solution)/shard_map/reduce_sum | solution.py:62
  125.6 1.9 %fusion.5.n_hbm = bf16[512,2048]{1,0:T(8,128)(2,1)} fusion(bf16[512,2048]{1,0:T(8,128)(2,1)S(1)} %get-tuple-element.6.h_hbm, f32[2048]{0:T(1024)S(1)} %convert_element_type.39, f32[512]{0:T(512)S(1)} %add_rsqrt_fusion.1), kind=kLoop, calls=%fused_computation.9 | loop fusion | flops 4194304 | bytes 4204544 | tf_op jit(solution)/shard_map/convert_element_type | solution.py:297
  127.6 8.5 %all-gather.3.cloned.1.call-done = bf16[12288,1408]{1,0:T(8,128)(2,1)} async-done(((bf16[96,1408]{1,0:T(8,128)(2,1)}), bf16[12288,1408]{1,0:T(8,128)(2,1)}) %all-gather.3.cloned.1.call-update) | async-done | bytes 34603024 | tf_op jit(solution)/shard_map/all_gather | solution.py:270
  136.1 24.0 %ffn.1 = bf16[512,2048]{1,0:T(8,128)(2,1)} custom-call(bf16[512,2048]{1,0:T(8,128)(2,1)} %copy-done.4, bf16[512,2048]{1,0:T(8,128)(2,1)} %fusion.5.n_hbm, bf16[2,2,32,96,1408]{4,3,2,1,0:T(8,128)(2,1)} %bitcast.42), custom_call_target="tpu_custom_call" | custom-call | tf_op jit(solution)/shard_map/ffn/pallas_call | solution.py:239
  (111 shorter events, 13.8 us)
Async XLA Ops:
  6.5 129.6 %all-gather.3.cloned.1.call-start = ((), (), s32[]{:S(2)}) async-start(), calls=%async_computation | async-start | bytes 34873344 | tf_op jit(solution)/shard_map/all_gather | solution.py:270
  9.9 9.2 %collective-permute-start.17 = (bf16[32,512]{1,0:T(8,128)(2,1)S(1)}, bf16[32,512]{1,0:T(8,128)(2,1)S(1)}, u32[]{:S(2)}, u32[]{:S(2)}) collective-permute-start(bf16[32,512]{1,0:T(8,128)(2,1)S(1)} %dynamic-slice_bitcast_fusion.1), channel_id=1, source_target_pairs={{0,96},{2,98},{4,100},{6,102},{8,104},{10,106},{12,108},{14,110},{... | collective-permute-start | bytes 98312 | tf_op jit(solution)/shard_map/ppermute | solution.py:27
  14.5 5.2 %collective-permute-start.18 = (bf16[32,512]{1,0:T(8,128)(2,1)S(1)}, bf16[32,512]{1,0:T(8,128)(2,1)S(1)}, u32[]{:S(2)}, u32[]{:S(2)}) collective-permute-start(bf16[32,512]{1,0:T(8,128)(2,1)S(1)} %dynamic-slice_bitcast_fusion.1), channel_id=1, source_target_pairs={{0,64},{2,66},{4,68},{6,70},{8,72},{10,74},{12,76},{14,78},{16,80}... | collective-permute-start | bytes 98312 | tf_op jit(solution)/shard_map/ppermute | solution.py:27
  14.5 5.2 %collective-permute-start.19 = (bf16[32,512]{1,0:T(8,128)(2,1)S(1)}, bf16[32,512]{1,0:T(8,128)(2,1)S(1)}, u32[]{:S(2)}, u32[]{:S(2)}) collective-permute-start(bf16[32,512]{1,0:T(8,128)(2,1)S(1)} %dynamic-slice_bitcast_fusion.1), channel_id=1, source_target_pairs={{0,32},{2,34},{4,36},{6,38},{8,40},{10,42},{12,44},{14,46},{16,48}... | collective-permute-start | bytes 98312 | tf_op jit(solution)/shard_map/ppermute | solution.py:27
  16.0 7.3 %collective-permute-start = (bf16[64,512]{1,0:T(8,128)(2,1)S(1)}, bf16[64,512]{1,0:T(8,128)(2,1)S(1)}, u32[]{:S(2)}, u32[]{:S(2)}) collective-permute-start(bf16[64,512]{1,0:T(8,128)(2,1)S(1)} %pad_maximum_fusion.6), channel_id=1, source_target_pairs={{0,6},{2,0},{4,2},{6,4},{8,14},{10,8},{12,10},{14,12},{16,22},{18,... | collective-permute-start | bytes 196616 | tf_op jit(solution)/shard_map/ppermute | solution.py:27
  18.6 4.8 %collective-permute-start.1 = (bf16[64,512]{1,0:T(8,128)(2,1)S(1)}, bf16[64,512]{1,0:T(8,128)(2,1)S(1)}, u32[]{:S(2)}, u32[]{:S(2)}) collective-permute-start(bf16[64,512]{1,0:T(8,128)(2,1)S(1)} %pad_maximum_fusion.6), channel_id=1, source_target_pairs={{0,4},{2,6},{4,0},{6,2},{8,12},{10,14},{12,8},{14,10},{16,20},{18,... | collective-permute-start | bytes 196616 | tf_op jit(solution)/shard_map/ppermute | solution.py:27
  19.1 4.8 %collective-permute-start.2 = (bf16[64,512]{1,0:T(8,128)(2,1)S(1)}, bf16[64,512]{1,0:T(8,128)(2,1)S(1)}, u32[]{:S(2)}, u32[]{:S(2)}) collective-permute-start(bf16[64,512]{1,0:T(8,128)(2,1)S(1)} %pad_maximum_fusion.6), channel_id=1, source_target_pairs={{0,2},{2,4},{4,6},{6,0},{8,10},{10,12},{12,14},{14,8},{16,18},{18,... | collective-permute-start | bytes 196616 | tf_op jit(solution)/shard_map/ppermute | solution.py:27
  20.5 5.0 %collective-permute-start.21 = (bf16[4,32,512]{2,1,0:T(8,128)(2,1)S(1)}, bf16[4,32,512]{2,1,0:T(8,128)(2,1)S(1)}, u32[]{:S(2)}, u32[]{:S(2)}) collective-permute-start(bf16[4,32,512]{2,1,0:T(8,128)(2,1)S(1)} %get-tuple-element.15), channel_id=1, source_target_pairs={{0,24},{2,26},{4,28},{6,30},{8,0},{10,2},{12,4},{14,6},{16,8},{18,... | collective-permute-start | bytes 393224 | tf_op jit(solution)/shard_map/ppermute | solution.py:27
  23.3 8.4 %collective-permute-start.20 = (bf16[4,32,512]{2,1,0:T(8,128)(2,1)S(1)}, bf16[4,32,512]{2,1,0:T(8,128)(2,1)S(1)}, u32[]{:S(2)}, u32[]{:S(2)}) collective-permute-start(bf16[4,32,512]{2,1,0:T(8,128)(2,1)S(1)} %get-tuple-element.15), channel_id=1, source_target_pairs={{0,8},{2,10},{4,12},{6,14},{8,16},{10,18},{12,20},{14,22},{16,24},... | collective-permute-start | bytes 393224 | tf_op jit(solution)/shard_map/ppermute | solution.py:27
  24.0 28.2 %copy-start.2 = (bf16[1024,2048]{1,0:T(8,128)(2,1)S(1)}, bf16[1024,2048]{1,0:T(8,128)(2,1)}, u32[]{:S(2)}) copy-start(bf16[1024,2048]{1,0:T(8,128)(2,1)} %param.13) | copy-start | bytes 12582916
  25.5 6.3 %collective-permute-start.22 = (bf16[4,32,512]{2,1,0:T(8,128)(2,1)S(1)}, bf16[4,32,512]{2,1,0:T(8,128)(2,1)S(1)}, u32[]{:S(2)}, u32[]{:S(2)}) collective-permute-start(bf16[4,32,512]{2,1,0:T(8,128)(2,1)S(1)} %collective-permute-done.21), channel_id=1, source_target_pairs={{0,24},{2,26},{4,28},{6,30},{8,0},{10,2},{12,4},{14,6},{16,8},{18,... | collective-permute-start | bytes 393224 | tf_op jit(solution)/shard_map/ppermute | solution.py:27
  29.1 12.2 %collective-permute-start.10 = (bf16[4,32,512]{2,1,0:T(8,128)(2,1)S(1)}, bf16[4,32,512]{2,1,0:T(8,128)(2,1)S(1)}, u32[]{:S(2)}, u32[]{:S(2)}) collective-permute-start(bf16[4,32,512]{2,1,0:T(8,128)(2,1)S(1)} %get-tuple-element.9), channel_id=1, source_target_pairs={{0,32},{2,34},{4,36},{6,38},{8,40},{10,42},{12,44},{14,46},{16,48}... | collective-permute-start | bytes 393224 | tf_op jit(solution)/shard_map/ppermute | solution.py:27
  31.8 10.1 %collective-permute-start.3 = (bf16[4,32,512]{2,1,0:T(8,128)(2,1)S(1)}, bf16[4,32,512]{2,1,0:T(8,128)(2,1)S(1)}, u32[]{:S(2)}, u32[]{:S(2)}) collective-permute-start(bf16[4,32,512]{2,1,0:T(8,128)(2,1)S(1)} %get-tuple-element.10), channel_id=1, source_target_pairs={{0,8},{2,10},{4,12},{6,14},{8,16},{10,18},{12,20},{14,22},{16,24},... | collective-permute-start | bytes 393224 | tf_op jit(solution)/shard_map/ppermute | solution.py:27
  31.9 17.7 %collective-permute-start.23 = (bf16[4,4,32,512]{3,2,1,0:T(8,128)(2,1)S(1)}, bf16[4,4,32,512]{3,2,1,0:T(8,128)(2,1)S(1)}, u32[]{:S(2)}, u32[]{:S(2)}) collective-permute-start(bf16[4,4,32,512]{3,2,1,0:T(8,128)(2,1)S(1)} %pad_maximum_fusion.2.refs_11_), channel_id=1, source_target_pairs={{0,2},{2,4},{4,6},{6,0},{8,10},{10,12},{12,14},{14,8},{16,18},{18,... | collective-permute-start | bytes 1572872 | tf_op jit(solution)/shard_map/ppermute | solution.py:27
  36.7 5.2 %collective-permute-start.12 = (bf16[4,32,512]{2,1,0:T(8,128)(2,1)S(1)}, bf16[4,32,512]{2,1,0:T(8,128)(2,1)S(1)}, u32[]{:S(2)}, u32[]{:S(2)}) collective-permute-start(bf16[4,32,512]{2,1,0:T(8,128)(2,1)S(1)} %get-tuple-element.9), channel_id=1, source_target_pairs={{0,96},{2,98},{4,100},{6,102},{8,104},{10,106},{12,108},{14,110},{... | collective-permute-start | bytes 393224 | tf_op jit(solution)/shard_map/ppermute | solution.py:27
  37.6 9.1 %collective-permute-start.5 = (bf16[4,32,512]{2,1,0:T(8,128)(2,1)S(1)}, bf16[4,32,512]{2,1,0:T(8,128)(2,1)S(1)}, u32[]{:S(2)}, u32[]{:S(2)}) collective-permute-start(bf16[4,32,512]{2,1,0:T(8,128)(2,1)S(1)} %get-tuple-element.10), channel_id=1, source_target_pairs={{0,24},{2,26},{4,28},{6,30},{8,0},{10,2},{12,4},{14,6},{16,8},{18,... | collective-permute-start | bytes 393224 | tf_op jit(solution)/shard_map/ppermute | solution.py:27
  41.2 5.3 %collective-permute-start.11 = (bf16[4,32,512]{2,1,0:T(8,128)(2,1)S(1)}, bf16[4,32,512]{2,1,0:T(8,128)(2,1)S(1)}, u32[]{:S(2)}, u32[]{:S(2)}) collective-permute-start(bf16[4,32,512]{2,1,0:T(8,128)(2,1)S(1)} %collective-permute-done.10), channel_id=1, source_target_pairs={{0,32},{2,34},{4,36},{6,38},{8,40},{10,42},{12,44},{14,46},{16,48}... | collective-permute-start | bytes 393224 | tf_op jit(solution)/shard_map/ppermute | solution.py:27
  41.9 7.5 %collective-permute-start.4 = (bf16[4,32,512]{2,1,0:T(8,128)(2,1)S(1)}, bf16[4,32,512]{2,1,0:T(8,128)(2,1)S(1)}, u32[]{:S(2)}, u32[]{:S(2)}) collective-permute-start(bf16[4,32,512]{2,1,0:T(8,128)(2,1)S(1)} %collective-permute-done.3), channel_id=1, source_target_pairs={{0,8},{2,10},{4,12},{6,14},{8,16},{10,18},{12,20},{14,22},{16,24},... | collective-permute-start | bytes 393224 | tf_op jit(solution)/shard_map/ppermute | solution.py:27
  41.9 17.9 %collective-permute-start.24 = (bf16[4,4,32,512]{3,2,1,0:T(8,128)(2,1)S(1)}, bf16[4,4,32,512]{3,2,1,0:T(8,128)(2,1)S(1)}, u32[]{:S(2)}, u32[]{:S(2)}) collective-permute-start(bf16[4,4,32,512]{3,2,1,0:T(8,128)(2,1)S(1)} %pad_maximum_fusion.2.refs_11_), channel_id=1, source_target_pairs={{0,6},{2,0},{4,2},{6,4},{8,14},{10,8},{12,10},{14,12},{16,22},{18,... | collective-permute-start | bytes 1572872 | tf_op jit(solution)/shard_map/ppermute | solution.py:27
  46.6 23.8 %collective-permute-start.13 = (bf16[4,4,32,512]{3,2,1,0:T(8,128)(2,1)S(1)}, bf16[4,4,32,512]{3,2,1,0:T(8,128)(2,1)S(1)}, u32[]{:S(2)}, u32[]{:S(2)}) collective-permute-start(bf16[4,4,32,512]{3,2,1,0:T(8,128)(2,1)S(1)} %pad_maximum_fusion.1.refs_6_), channel_id=1, source_target_pairs={{0,8},{2,10},{4,12},{6,14},{8,16},{10,18},{12,20},{14,22},{16,24},... | collective-permute-start | bytes 1572872 | tf_op jit(solution)/shard_map/ppermute | solution.py:27
  46.7 26.5 %collective-permute-start.14 = (bf16[4,4,32,512]{3,2,1,0:T(8,128)(2,1)S(1)}, bf16[4,4,32,512]{3,2,1,0:T(8,128)(2,1)}, u32[]{:S(2)}, u32[]{:S(2)}) collective-permute-start(bf16[4,4,32,512]{3,2,1,0:T(8,128)(2,1)S(1)} %pad_maximum_fusion.1.refs_6_), channel_id=1, source_target_pairs={{0,24},{2,26},{4,28},{6,30},{8,0},{10,2},{12,4},{14,6},{16,8},{18,... | collective-permute-start | bytes 1572872 | tf_op jit(solution)/shard_map/ppermute | solution.py:27
  49.5 33.6 %copy-start.22 = (bf16[4,128]{1,0:T(4,128)(2,1)S(1)}, bf16[4,128]{1,0:T(4,128)(2,1)}, u32[]{:S(2)}) copy-start(bf16[4,128]{1,0:T(4,128)(2,1)} %param.18) | copy-start | bytes 3076
  49.5 25.3 %collective-permute-start.6 = (bf16[4,4,32,512]{3,2,1,0:T(8,128)(2,1)S(1)}, bf16[4,4,32,512]{3,2,1,0:T(8,128)(2,1)}, u32[]{:S(2)}, u32[]{:S(2)}) collective-permute-start(bf16[4,4,32,512]{3,2,1,0:T(8,128)(2,1)S(1)} %pad_maximum_fusion.refs_1_), channel_id=1, source_target_pairs={{0,32},{2,34},{4,36},{6,38},{8,40},{10,42},{12,44},{14,46},{16,48}... | collective-permute-start | bytes 1572872 | tf_op jit(solution)/shard_map/ppermute | solution.py:27
  49.6 29.7 %collective-permute-start.7 = (bf16[4,4,32,512]{3,2,1,0:T(8,128)(2,1)S(1)}, bf16[4,4,32,512]{3,2,1,0:T(8,128)(2,1)}, u32[]{:S(2)}, u32[]{:S(2)}) collective-permute-start(bf16[4,4,32,512]{3,2,1,0:T(8,128)(2,1)S(1)} %pad_maximum_fusion.refs_1_), channel_id=1, source_target_pairs={{0,96},{2,98},{4,100},{6,102},{8,104},{10,106},{12,108},{14,110},{... | collective-permute-start | bytes 1572872 | tf_op jit(solution)/shard_map/ppermute | solution.py:27
  59.8 33.6 %copy-start.9 = (bf16[4,4,32,512]{3,2,1,0:T(8,128)(2,1)}, bf16[4,4,32,512]{3,2,1,0:T(8,128)(2,1)S(1)}, u32[]{:S(2)}) copy-start(bf16[4,4,32,512]{3,2,1,0:T(8,128)(2,1)S(1)} %collective-permute-done.24.refs_13_) | copy-start | bytes 1572868
  59.8 20.5 %collective-permute-start.25 = (bf16[2,4,32,512]{3,2,1,0:T(8,128)(2,1)}, bf16[2,4,32,512]{3,2,1,0:T(8,128)(2,1)S(1)}, u32[]{:S(2)}, u32[]{:S(2)}) collective-permute-start(bf16[2,4,32,512]{3,2,1,0:T(8,128)(2,1)} %slice.38), channel_id=1, source_target_pairs={{0,2},{2,4},{4,6},{6,0},{8,10},{10,12},{12,14},{14,8},{16,18},{18,... | collective-permute-start | bytes 786440 | tf_op jit(solution)/shard_map/ppermute | solution.py:27
  70.4 13.5 %collective-permute-start.26 = (bf16[2,4,32,512]{3,2,1,0:T(8,128)(2,1)}, bf16[2,4,32,512]{3,2,1,0:T(8,128)(2,1)S(1)}, u32[]{:S(2)}, u32[]{:S(2)}) collective-permute-start(bf16[2,4,32,512]{3,2,1,0:T(8,128)(2,1)} %slice.39), channel_id=1, source_target_pairs={{0,6},{2,0},{4,2},{6,4},{8,14},{10,8},{12,10},{14,12},{16,22},{18,... | collective-permute-start | bytes 786440 | tf_op jit(solution)/shard_map/ppermute | solution.py:27
  73.2 10.7 %collective-permute-start.15 = (bf16[2,4,32,512]{3,2,1,0:T(8,128)(2,1)}, bf16[2,4,32,512]{3,2,1,0:T(8,128)(2,1)S(1)}, u32[]{:S(2)}, u32[]{:S(2)}) collective-permute-start(bf16[2,4,32,512]{3,2,1,0:T(8,128)(2,1)} %slice.36), channel_id=1, source_target_pairs={{0,8},{2,10},{4,12},{6,14},{8,16},{10,18},{12,20},{14,22},{16,24},... | collective-permute-start | bytes 786440 | tf_op jit(solution)/shard_map/ppermute | solution.py:27
  74.9 13.1 %collective-permute-start.16 = (bf16[2,4,32,512]{3,2,1,0:T(8,128)(2,1)}, bf16[2,4,32,512]{3,2,1,0:T(8,128)(2,1)S(1)}, u32[]{:S(2)}, u32[]{:S(2)}) collective-permute-start(bf16[2,4,32,512]{3,2,1,0:T(8,128)(2,1)} %slice.37), channel_id=1, source_target_pairs={{0,24},{2,26},{4,28},{6,30},{8,0},{10,2},{12,4},{14,6},{16,8},{18,... | collective-permute-start | bytes 786440 | tf_op jit(solution)/shard_map/ppermute | solution.py:27
  79.3 14.2 %collective-permute-start.8 = (bf16[2,4,32,512]{3,2,1,0:T(8,128)(2,1)}, bf16[2,4,32,512]{3,2,1,0:T(8,128)(2,1)S(1)}, u32[]{:S(2)}, u32[]{:S(2)}) collective-permute-start(bf16[2,4,32,512]{3,2,1,0:T(8,128)(2,1)} %slice.33), channel_id=1, source_target_pairs={{0,32},{2,34},{4,36},{6,38},{8,40},{10,42},{12,44},{14,46},{16,48}... | collective-permute-start | bytes 786440 | tf_op jit(solution)/shard_map/ppermute | solution.py:27
  80.4 13.1 %collective-permute-start.9 = (bf16[2,4,32,512]{3,2,1,0:T(8,128)(2,1)S(1)}, bf16[2,4,32,512]{3,2,1,0:T(8,128)(2,1)S(1)}, u32[]{:S(2)}, u32[]{:S(2)}) collective-permute-start(bf16[2,4,32,512]{3,2,1,0:T(8,128)(2,1)S(1)} %slice.34), channel_id=1, source_target_pairs={{0,96},{2,98},{4,100},{6,102},{8,104},{10,106},{12,108},{14,110},{... | collective-permute-start | bytes 786440 | tf_op jit(solution)/shard_map/ppermute | solution.py:27
  104.2 17.1 %collective-permute-start.27 = (bf16[512,2048]{1,0:T(8,128)(2,1)}, bf16[512,2048]{1,0:T(8,128)(2,1)}, u32[]{:S(2)}, u32[]{:S(2)}) collective-permute-start(bf16[512,2048]{1,0:T(8,128)(2,1)} %mixer_other.1), channel_id=1, source_target_pairs={{0,1},{1,0},{2,3},{3,2},{4,5},{5,4},{6,7},{7,6},{8,9},{9,8},{10,11... | collective-permute-start | bytes 6291464 | tf_op jit(solution)/shard_map/ppermute | solution.py:293
  (20 other events, 226.4 us)
Sparse Core Ops, SparseCore 0:
  10.3 125.7 all-gather.2
where the time goes:
time: 168 us; the launch traced here: 167 us
  Pallas kernels  45.7 us (27%)
  starting transfers between devices  44.2 us (26%)
  waiting for transfers between devices  35.8 us (21%)
  other arithmetic  17.3 us (10%)
  between operations  13.8 us (8%)
  local copies, waits for them, and re-layouts  10.1 us (6%)
    ppermute x27, starting transfers between devices, shift(): return lax.ppermute(x, CHIPS, pairs)  38.9 us
    ppermute x27, waiting for transfers between devices, shift(): return lax.ppermute(x, CHIPS, pairs)  27.3 us
    pallas_call x1, Pallas kernels, ffn(): pl.pallas_call(ffn_body, out_shape=jax.ShapeDtypeStruct(h_mid.shape, BF16...  24 us
    pallas_call x2, Pallas kernels, mixer(): pl.pallas_call(functools.partial(mixer_body, own), out_shape=jax.ShapeDty...  21.7 us
    all_gather x1, waiting for transfers between devices, on_device(): lax.all_gather(packed, EVERY).reshape(tps, reps, fss, *packed.shape)  8.54 us
    reduce_sum x2, other arithmetic, rms_scale(): scale = lax.rsqrt(jnp.mean(values * values, axis=-1, keepdims=True) + 1e-06)  7.42 us
    ppermute x1, starting transfers between devices, on_device(): lax.ppermute(other, 'tp', [(i, (i + 1) % tps) for i in range(tps)])  5.29 us
    slice x3, local copies, waits for them, and re-layouts, relayed_ring(): ahead[half:]  3.44 us
  transfers between devices with their start and end apart: 29, of which 8 were waited for; matrix products, arithmetic and copies ran while one was open for 14% of the time, Pallas kernels for 13%

commit v1 on v0

--- a/solution.py
+++ b/solution.py
@@ -153,8 +153,9 @@
 def ffn_body(h_hbm, n_hbm, packed, out_hbm, h_mid, normed, mid, down, hidden, out, sem_h, sem_n, sem_w, sem_d, sem_o):
     tps, share, wide = packed.shape[0], down.shape[2], packed.shape[-1]
     _, model = out.shape
-    starts = list(range(0, tps * wide, CHUNK))
-    sizes = [min(CHUNK, tps * wide - at) for at in starts]
+    first = tps * wide % CHUNK
+    starts = [0] * (first > 0) + list(range(first, tps * wide, CHUNK))
+    sizes = [first] * (first > 0) + [CHUNK] * (tps * wide // CHUNK)
 
     def columns(j):
         copies = []
@@ -185,8 +186,10 @@
 
     rows = pltpu.make_async_copy(n_hbm, normed, sem_n)
     mids = pltpu.make_async_copy(h_hbm, h_mid, sem_h)
+    for copy in columns(0):
+        copy.start()
     rows.start()
-    for j in range(len(sizes)):
+    for j in range(1, len(sizes)):
         for copy in columns(j):
             copy.start()
     for t in range(tps):
@@ -201,14 +204,15 @@
         r = dot_nn(normed[...], w[...].reshape(model, 2 * size))
         hidden[:, pl.ds(at, size)] = (jax.nn.silu(r[:, :size]) * r[:, size:]).astype(BF16)
 
+    if first:
+        up_to(0, 0, first)
+
     def whole(j, carry):
-        up_to(j, pl.multiple_of(j * CHUNK, CHUNK), CHUNK)
+        at = pl.multiple_of(first + j * CHUNK, 128)
+        up_to(j + (first > 0), at, CHUNK)
         return carry
 
-    full = tps * wide // CHUNK
-    lax.fori_loop(0, full, whole, 0)
-    if full < len(sizes):
-        up_to(full, starts[full], sizes[full])
+    lax.fori_loop(0, tps * wide // CHUNK, whole, 0)
     pltpu.make_async_copy(down, down, sem_d).wait()
     mids.wait()
 
@@ -252,6 +256,25 @@
     )(h_mid, normed, packed)
 
 
+def pack_body(gate, up, down, out):
+    rep = lax.axis_index("rep")
+    share = gate.shape[0]
+    half = share // 2
+    out[:share] = jnp.where(rep == 0, gate[...], up[...])
+    out[share:] = down[pl.ds(pl.multiple_of(rep * half, half), half)]
+
+
+def pack(gate, up, down):
+    share, wide = gate.shape
+    return pl.pallas_call(
+        pack_body,
+        out_shape=jax.ShapeDtypeStruct((share + share // 2, wide), gate.dtype),
+        in_specs=[VMEM] * 3,
+        out_specs=VMEM,
+        name="pack",
+    )(gate, up, down)
+
+
 def half_rows(x, part):
     size = x.shape[0] // 2
     return lax.dynamic_slice_in_dim(x, part * size, size, 0)
@@ -266,7 +289,7 @@
     rows = tokens.shape[0] // tps
     share, width = w_unit.shape
 
-    packed = jnp.concatenate([jnp.where(rep == 0, w_gate, w_up), half_rows(w_down.T, rep)], axis=0)
+    packed = pack(w_gate, w_up, w_down.T)
     packed = lax.all_gather(packed, EVERY).reshape(tps, reps, fss, *packed.shape)
 
     part = share // 2

time: 168 us -> 166 us (0.988)
  waiting for transfers between devices: 35.8 us -> 33.6 us
  Pallas kernels: 45.7 us -> 47.6 us
  local copies, waits for them, and re-layouts: 10.1 us -> 8.39 us
  starting transfers between devices: 44.2 us -> 45.9 us
    ppermute x1, starting transfers between devices: 5.29 us -> 9 us  [on_device(): lax.ppermute(other, 'tp', [(i, (i + 1) % tps) for i in range(tps)])]
    ppermute x27, starting transfers between devices: 38.9 us -> 36.9 us  [shift(): return lax.ppermute(x, CHIPS, pairs)]
    pallas_call x0 -> x1, Pallas kernels: none -> 1.84 us  [pack(): pl.pallas_call(pack_body, out_shape=jax.ShapeDtypeStruct((share + share /...]
  transfers between devices with their start and end apart: 29 -> 29, of which waited for: 8 -> 10; matrix products, arithmetic and copies ran while one was open for 14% -> 14% of each run, Pallas kernels for 13% -> 13%
where the time goes in v1:
time: 166 us; the launch traced here: 165 us
  Pallas kernels  47.6 us (29%)
  starting transfers between devices  45.9 us (28%)
  waiting for transfers between devices  33.6 us (20%)
  other arithmetic  16.2 us (10%)
  between operations  13.7 us (8%)
  local copies, waits for them, and re-layouts  8.39 us (5%)
    ppermute x27, starting transfers between devices, shift(): return lax.ppermute(x, CHIPS, pairs)  36.9 us
    ppermute x27, waiting for transfers between devices, shift(): return lax.ppermute(x, CHIPS, pairs)  25.8 us
    pallas_call x1, Pallas kernels, ffn(): pl.pallas_call(ffn_body, out_shape=jax.ShapeDtypeStruct(h_mid.shape, BF16...  23.5 us
    pallas_call x2, Pallas kernels, mixer(): pl.pallas_call(functools.partial(mixer_body, own), out_shape=jax.ShapeDty...  22.3 us
    ppermute x1, starting transfers between devices, on_device(): lax.ppermute(other, 'tp', [(i, (i + 1) % tps) for i in range(tps)])  9 us
    all_gather x1, waiting for transfers between devices, on_device(): lax.all_gather(packed, EVERY).reshape(tps, reps, fss, *packed.shape)  7.7 us
    reduce_sum x2, other arithmetic, rms_scale(): scale = lax.rsqrt(jnp.mean(values * values, axis=-1, keepdims=True) + 1e-06)  7.19 us
    slice x3, local copies, waits for them, and re-layouts, relayed_ring(): ahead[half:]  3.43 us
  transfers between devices with their start and end apart: 29, of which 10 were waited for; matrix products, arithmetic and copies ran while one was open for 14% of the time, Pallas kernels for 13%

profile of v1, /device:TPU:1, one launch (start us, length us, event | category | flops | bytes accessed | tf_op | source)
XLA Modules:
  0.0 165.4 jit_solution(15570398531692128773)
XLA Ops:
  6.5 1.8 %pack.1 = bf16[96,1408]{1,0:T(8,128)(2,1)} custom-call(bf16[64,1408]{1,0:T(8,128)(2,1)} %gate.1, bf16[64,1408]{1,0:T(8,128)(2,1)} %up.1, bf16[64,1408]{1,0:T(8,128)(2,1)} %bitcast.42), custom_call_target="tpu_custom_call" | custom-call | tf_op jit(solution)/shard_map/pack/pallas_call | solution.py:269
  9.2 4.6 %collective-permute-start.17 = (bf16[32,512]{1,0:T(8,128)(2,1)S(1)}, bf16[32,512]{1,0:T(8,128)(2,1)S(1)}, u32[]{:S(2)}, u32[]{:S(2)}) collective-permute-start(bf16[32,512]{1,0:T(8,128)(2,1)S(1)} %dynamic-slice_bitcast_fusion), channel_id=1, source_target_pairs={{0,96},{2,98},{4,100},{6,102},{8,104},{10,106},{12,108},{14,110},{... | collective-permute-start | bytes 98312 | tf_op jit(solution)/shard_map/ppermute | solution.py:27
  15.3 2.5 %collective-permute-start = (bf16[64,512]{1,0:T(8,128)(2,1)S(1)}, bf16[64,512]{1,0:T(8,128)(2,1)S(1)}, u32[]{:S(2)}, u32[]{:S(2)}) collective-permute-start(bf16[64,512]{1,0:T(8,128)(2,1)S(1)} %pad_maximum_fusion.5), channel_id=1, source_target_pairs={{0,6},{2,0},{4,2},{6,4},{8,14},{10,8},{12,10},{14,12},{16,22},{18,... | collective-permute-start | bytes 196616 | tf_op jit(solution)/shard_map/ppermute | solution.py:27
  19.8 2.8 %collective-permute-start.21 = (bf16[4,32,512]{2,1,0:T(8,128)(2,1)S(1)}, bf16[4,32,512]{2,1,0:T(8,128)(2,1)S(1)}, u32[]{:S(2)}, u32[]{:S(2)}) collective-permute-start(bf16[4,32,512]{2,1,0:T(8,128)(2,1)S(1)} %get-tuple-element.15), channel_id=1, source_target_pairs={{0,24},{2,26},{4,28},{6,30},{8,0},{10,2},{12,4},{14,6},{16,8},{18,... | collective-permute-start | bytes 393224 | tf_op jit(solution)/shard_map/ppermute | solution.py:27
  23.3 1.2 collective-permute-done.21
  24.5 3.4 %collective-permute-start.22 = (bf16[4,32,512]{2,1,0:T(8,128)(2,1)S(1)}, bf16[4,32,512]{2,1,0:T(8,128)(2,1)S(1)}, u32[]{:S(2)}, u32[]{:S(2)}) collective-permute-start(bf16[4,32,512]{2,1,0:T(8,128)(2,1)S(1)} %collective-permute-done.21), channel_id=1, source_target_pairs={{0,24},{2,26},{4,28},{6,30},{8,0},{10,2},{12,4},{14,6},{16,8},{18,... | collective-permute-start | bytes 393224 | tf_op jit(solution)/shard_map/ppermute | solution.py:27
  28.0 2.0 %collective-permute-start.10 = (bf16[4,32,512]{2,1,0:T(8,128)(2,1)S(1)}, bf16[4,32,512]{2,1,0:T(8,128)(2,1)S(1)}, u32[]{:S(2)}, u32[]{:S(2)}) collective-permute-start(bf16[4,32,512]{2,1,0:T(8,128)(2,1)S(1)} %get-tuple-element.9), channel_id=1, source_target_pairs={{0,32},{2,34},{4,36},{6,38},{8,40},{10,42},{12,44},{14,46},{16,48}... | collective-permute-start | bytes 393224 | tf_op jit(solution)/shard_map/ppermute | solution.py:27
  30.3 2.0 %collective-permute-start.23 = (bf16[4,4,32,512]{3,2,1,0:T(8,128)(2,1)S(1)}, bf16[4,4,32,512]{3,2,1,0:T(8,128)(2,1)S(1)}, u32[]{:S(2)}, u32[]{:S(2)}) collective-permute-start(bf16[4,4,32,512]{3,2,1,0:T(8,128)(2,1)S(1)} %pad_maximum_fusion.2.refs_11_), channel_id=1, source_target_pairs={{0,2},{2,4},{4,6},{6,0},{8,10},{10,12},{12,14},{14,8},{16,18},{18,... | collective-permute-start | bytes 1572872 | tf_op jit(solution)/shard_map/ppermute | solution.py:27
  32.3 3.1 %fusion = f32[1024]{0:T(1024)S(1)} fusion(bf16[1024,2048]{1,0:T(8,128)(2,1)} %param.13), kind=kLoop, calls=%fused_computation.2 | loop fusion | flops 6290432 | bytes 4198400 | tf_op jit(solution)/shard_map/reduce_sum | solution.py:62
  35.4 1.1 collective-permute-start.12
  36.5 3.2 %collective-permute-start.5 = (bf16[4,32,512]{2,1,0:T(8,128)(2,1)S(1)}, bf16[4,32,512]{2,1,0:T(8,128)(2,1)S(1)}, u32[]{:S(2)}, u32[]{:S(2)}) collective-permute-start(bf16[4,32,512]{2,1,0:T(8,128)(2,1)S(1)} %get-tuple-element.10), channel_id=1, source_target_pairs={{0,24},{2,26},{4,28},{6,30},{8,0},{10,2},{12,4},{14,6},{16,8},{18,... | collective-permute-start | bytes 393224 | tf_op jit(solution)/shard_map/ppermute | solution.py:27
  39.7 1.5 collective-permute-start.11
  41.3 1.1 collective-permute-start.24
  42.3 2.7 %collective-permute-done.11 = bf16[4,32,512]{2,1,0:T(8,128)(2,1)S(1)} collective-permute-done((bf16[4,32,512]{2,1,0:T(8,128)(2,1)S(1)}, bf16[4,32,512]{2,1,0:T(8,128)(2,1)S(1)}, u32[]{:S(2)}, u32[]{:S(2)}) %collective-permute-start.11) | collective-permute-done | bytes 131104 | tf_op jit(solution)/shard_map/ppermute | solution.py:27
  45.2 2.7 %collective-permute-start.14 = (bf16[4,4,32,512]{3,2,1,0:T(8,128)(2,1)S(1)}, bf16[4,4,32,512]{3,2,1,0:T(8,128)(2,1)}, u32[]{:S(2)}, u32[]{:S(2)}) collective-permute-start(bf16[4,4,32,512]{3,2,1,0:T(8,128)(2,1)S(1)} %pad_maximum_fusion.1.refs_6_), channel_id=1, source_target_pairs={{0,24},{2,26},{4,28},{6,30},{8,0},{10,2},{12,4},{14,6},{16,8},{18,... | collective-permute-start | bytes 1572872 | tf_op jit(solution)/shard_map/ppermute | solution.py:27
  48.3 2.4 %collective-permute-start.7 = (bf16[4,4,32,512]{3,2,1,0:T(8,128)(2,1)S(1)}, bf16[4,4,32,512]{3,2,1,0:T(8,128)(2,1)}, u32[]{:S(2)}, u32[]{:S(2)}) collective-permute-start(bf16[4,4,32,512]{3,2,1,0:T(8,128)(2,1)S(1)} %pad_maximum_fusion.refs_1_), channel_id=1, source_target_pairs={{0,96},{2,98},{4,100},{6,102},{8,104},{10,106},{12,108},{14,110},{... | collective-permute-start | bytes 1572872 | tf_op jit(solution)/shard_map/ppermute | solution.py:27
  50.7 3.0 %fusion.2.refs_0_ = bf16[1024,2048]{1,0:T(8,128)(2,1)} fusion(bf16[1024,2048]{1,0:T(8,128)(2,1)S(1)} %copy-done.2, f32[2048]{0:T(1024)S(1)} %convert_element_type.34, f32[1024]{0:T(1024)S(1)} %add_rsqrt_fusion), kind=kLoop, calls=%fused_computation.4 | loop fusion | flops 8388608 | bytes 8400896 | tf_op jit(solution)/shard_map/convert_element_type | solution.py:309
  53.7 3.3 %collective-permute-done.24.refs_13_ = bf16[4,4,32,512]{3,2,1,0:T(8,128)(2,1)S(1)} collective-permute-done((bf16[4,4,32,512]{3,2,1,0:T(8,128)(2,1)S(1)}, bf16[4,4,32,512]{3,2,1,0:T(8,128)(2,1)S(1)}, u32[]{:S(2)}, u32[]{:S(2)}) %collective-permute-start.24) | collective-permute-done | bytes 524320 | tf_op jit(solution)/shard_map/ppermute | solution.py:27
  57.8 1.5 dynamic-slice_select_fusion.refs_16_
  60.0 9.3 %collective-permute-done.13.refs_7_ = bf16[4,4,32,512]{3,2,1,0:T(8,128)(2,1)S(1)} collective-permute-done((bf16[4,4,32,512]{3,2,1,0:T(8,128)(2,1)S(1)}, bf16[4,4,32,512]{3,2,1,0:T(8,128)(2,1)S(1)}, u32[]{:S(2)}, u32[]{:S(2)}) %collective-permute-start.13) | collective-permute-done | bytes 524320 | tf_op jit(solution)/shard_map/ppermute | solution.py:27
  70.1 1.7 slice.37
  71.8 2.7 %collective-permute-start.16 = (bf16[2,4,32,512]{3,2,1,0:T(8,128)(2,1)}, bf16[2,4,32,512]{3,2,1,0:T(8,128)(2,1)S(1)}, u32[]{:S(2)}, u32[]{:S(2)}) collective-permute-start(bf16[2,4,32,512]{3,2,1,0:T(8,128)(2,1)} %slice.37), channel_id=1, source_target_pairs={{0,24},{2,26},{4,28},{6,30},{8,0},{10,2},{12,4},{14,6},{16,8},{18,... | collective-permute-start | bytes 786440 | tf_op jit(solution)/shard_map/ppermute | solution.py:27
  74.4 1.7 %slice.33 = bf16[2,4,32,512]{3,2,1,0:T(8,128)(2,1)} slice(bf16[4,4,32,512]{3,2,1,0:T(8,128)(2,1)} %collective-permute-done.6.refs_2_), slice={[0:2], [0:4], [0:32], [0:512]} | slice | bytes 524288 | tf_op jit(solution)/shard_map/slice | solution.py:43
  77.5 2.4 %collective-permute-start.9 = (bf16[2,4,32,512]{3,2,1,0:T(8,128)(2,1)S(1)}, bf16[2,4,32,512]{3,2,1,0:T(8,128)(2,1)S(1)}, u32[]{:S(2)}, u32[]{:S(2)}) collective-permute-start(bf16[2,4,32,512]{3,2,1,0:T(8,128)(2,1)S(1)} %slice.34), channel_id=1, source_target_pairs={{0,96},{2,98},{4,100},{6,102},{8,104},{10,106},{12,108},{14,110},{... | collective-permute-start | bytes 786440 | tf_op jit(solution)/shard_map/ppermute | solution.py:27
  81.1 7.8 %collective-permute-done.8.refs_4_ = bf16[2,4,32,512]{3,2,1,0:T(8,128)(2,1)S(1)} collective-permute-done((bf16[2,4,32,512]{3,2,1,0:T(8,128)(2,1)}, bf16[2,4,32,512]{3,2,1,0:T(8,128)(2,1)S(1)}, u32[]{:S(2)}, u32[]{:S(2)}) %collective-permute-start.8) | collective-permute-done | bytes 262176 | tf_op jit(solution)/shard_map/ppermute | solution.py:27
  90.0 10.6 %mixer_other.1 = bf16[512,2048]{1,0:T(8,128)(2,1)} custom-call(bf16[1024,2048]{1,0:T(8,128)(2,1)} %fusion.2.refs_0_, bf16[4,4,32,512]{3,2,1,0:T(8,128)(2,1)} %copy-done.7, bf16[4,4,32,512]{3,2,1,0:T(8,128)(2,1)} %collective-permute-done.6.refs_2_, bf16[4,4,32,512]{3,2,1,0:T(8,128)(2,1)} %collective-permute-done.7.refs_3_, ...), custom_call_target="tpu_custom_call" | custom-call | tf_op jit(solution)/shard_map/mixer_other/pallas_call | solution.py:139
  100.6 9.0 %collective-permute-start.27 = (bf16[512,2048]{1,0:T(8,128)(2,1)}, bf16[512,2048]{1,0:T(8,128)(2,1)}, u32[]{:S(2)}, u32[]{:S(2)}) collective-permute-start(bf16[512,2048]{1,0:T(8,128)(2,1)} %mixer_other.1), channel_id=1, source_target_pairs={{0,1},{1,0},{2,3},{3,2},{4,5},{5,4},{6,7},{7,6},{8,9},{9,8},{10,11... | collective-permute-start | bytes 6291464 | tf_op jit(solution)/shard_map/ppermute | solution.py:316
  109.6 11.7 %mixer_own.1 = f32[512,2048]{1,0:T(8,128)} custom-call(bf16[1024,2048]{1,0:T(8,128)(2,1)} %fusion.2.refs_0_, bf16[4,4,32,512]{3,2,1,0:T(8,128)(2,1)} %copy-done.7, bf16[4,4,32,512]{3,2,1,0:T(8,128)(2,1)} %collective-permute-done.6.refs_2_, bf16[4,4,32,512]{3,2,1,0:T(8,128)(2,1)} %collective-permute-done.7.refs_3_, bf16[2,4,32,512]{3,2,1,0:T(8,128)(2,1)} %copy-done.15, ...), custom_call_target="tpu_custom_call" | custom-call | tf_op jit(solution)/shard_map/mixer_own/pallas_call | solution.py:139
  121.3 4.1 %fusion.3 = (f32[512]{0:T(512)S(1)}, bf16[512,2048]{1,0:T(8,128)(2,1)S(1)}) fusion(f32[512,2048]{1,0:T(8,128)} %mixer_own.1, bf16[512,2048]{1,0:T(8,128)(2,1)} %collective-permute-done.27, bf16[1024,2048]{1,0:T(8,128)(2,1)S(1)} %copy-done.3, s32[]{:T(128)S(6)} %select_n.211), kind=kLoop, calls=%fused_computation.7 | loop fusion | flops 8388096 | bytes 10487812 | tf_op jit(solution)/shard_map/reduce_sum | solution.py:62
  125.4 1.9 %fusion.5.n_hbm = bf16[512,2048]{1,0:T(8,128)(2,1)} fusion(bf16[512,2048]{1,0:T(8,128)(2,1)S(1)} %get-tuple-element.6.h_hbm, f32[2048]{0:T(1024)S(1)} %convert_element_type.39, f32[512]{0:T(512)S(1)} %add_rsqrt_fusion.1), kind=kLoop, calls=%fused_computation.9 | loop fusion | flops 4194304 | bytes 4204544 | tf_op jit(solution)/shard_map/convert_element_type | solution.py:320
  127.3 7.7 %all-gather.3.cloned.1.call-done = bf16[12288,1408]{1,0:T(8,128)(2,1)} async-done(((bf16[96,1408]{1,0:T(8,128)(2,1)}), bf16[12288,1408]{1,0:T(8,128)(2,1)}) %all-gather.3.cloned.1.call-update) | async-done | bytes 34603024 | tf_op jit(solution)/shard_map/all_gather | solution.py:293
  135.0 23.5 %ffn.1 = bf16[512,2048]{1,0:T(8,128)(2,1)} custom-call(bf16[512,2048]{1,0:T(8,128)(2,1)} %copy-done.4, bf16[512,2048]{1,0:T(8,128)(2,1)} %fusion.5.n_hbm, bf16[2,2,32,96,1408]{4,3,2,1,0:T(8,128)(2,1)} %bitcast.41), custom_call_target="tpu_custom_call" | custom-call | tf_op jit(solution)/shard_map/ffn/pallas_call | solution.py:243
  (105 shorter events, 11.9 us)
Async XLA Ops:
  6.5 73.4 %copy-start = (bf16[4,128]{1,0:T(4,128)(2,1)S(1)}, bf16[4,128]{1,0:T(4,128)(2,1)}, u32[]{:S(2)}) copy-start(bf16[4,128]{1,0:T(4,128)(2,1)} %param.18) | copy-start | bytes 3076
  6.5 128.5 %all-gather.3.cloned.1.call-start = ((), (), s32[]{:S(2)}) async-start(), calls=%async_computation | async-start | bytes 34873344 | tf_op jit(solution)/shard_map/all_gather | solution.py:293
  9.2 9.1 %collective-permute-start.17 = (bf16[32,512]{1,0:T(8,128)(2,1)S(1)}, bf16[32,512]{1,0:T(8,128)(2,1)S(1)}, u32[]{:S(2)}, u32[]{:S(2)}) collective-permute-start(bf16[32,512]{1,0:T(8,128)(2,1)S(1)} %dynamic-slice_bitcast_fusion), channel_id=1, source_target_pairs={{0,96},{2,98},{4,100},{6,102},{8,104},{10,106},{12,108},{14,110},{... | collective-permute-start | bytes 98312 | tf_op jit(solution)/shard_map/ppermute | solution.py:27
  13.8 5.2 %collective-permute-start.18 = (bf16[32,512]{1,0:T(8,128)(2,1)S(1)}, bf16[32,512]{1,0:T(8,128)(2,1)S(1)}, u32[]{:S(2)}, u32[]{:S(2)}) collective-permute-start(bf16[32,512]{1,0:T(8,128)(2,1)S(1)} %dynamic-slice_bitcast_fusion), channel_id=1, source_target_pairs={{0,64},{2,66},{4,68},{6,70},{8,72},{10,74},{12,76},{14,78},{16,80}... | collective-permute-start | bytes 98312 | tf_op jit(solution)/shard_map/ppermute | solution.py:27
  13.8 5.2 %collective-permute-start.19 = (bf16[32,512]{1,0:T(8,128)(2,1)S(1)}, bf16[32,512]{1,0:T(8,128)(2,1)S(1)}, u32[]{:S(2)}, u32[]{:S(2)}) collective-permute-start(bf16[32,512]{1,0:T(8,128)(2,1)S(1)} %dynamic-slice_bitcast_fusion), channel_id=1, source_target_pairs={{0,32},{2,34},{4,36},{6,38},{8,40},{10,42},{12,44},{14,46},{16,48}... | collective-permute-start | bytes 98312 | tf_op jit(solution)/shard_map/ppermute | solution.py:27
  15.3 7.3 %collective-permute-start = (bf16[64,512]{1,0:T(8,128)(2,1)S(1)}, bf16[64,512]{1,0:T(8,128)(2,1)S(1)}, u32[]{:S(2)}, u32[]{:S(2)}) collective-permute-start(bf16[64,512]{1,0:T(8,128)(2,1)S(1)} %pad_maximum_fusion.5), channel_id=1, source_target_pairs={{0,6},{2,0},{4,2},{6,4},{8,14},{10,8},{12,10},{14,12},{16,22},{18,... | collective-permute-start | bytes 196616 | tf_op jit(solution)/shard_map/ppermute | solution.py:27
  17.8 4.8 %collective-permute-start.1 = (bf16[64,512]{1,0:T(8,128)(2,1)S(1)}, bf16[64,512]{1,0:T(8,128)(2,1)S(1)}, u32[]{:S(2)}, u32[]{:S(2)}) collective-permute-start(bf16[64,512]{1,0:T(8,128)(2,1)S(1)} %pad_maximum_fusion.5), channel_id=1, source_target_pairs={{0,4},{2,6},{4,0},{6,2},{8,12},{10,14},{12,8},{14,10},{16,20},{18,... | collective-permute-start | bytes 196616 | tf_op jit(solution)/shard_map/ppermute | solution.py:27
  18.3 4.8 %collective-permute-start.2 = (bf16[64,512]{1,0:T(8,128)(2,1)S(1)}, bf16[64,512]{1,0:T(8,128)(2,1)S(1)}, u32[]{:S(2)}, u32[]{:S(2)}) collective-permute-start(bf16[64,512]{1,0:T(8,128)(2,1)S(1)} %pad_maximum_fusion.5), channel_id=1, source_target_pairs={{0,2},{2,4},{4,6},{6,0},{8,10},{10,12},{12,14},{14,8},{16,18},{18,... | collective-permute-start | bytes 196616 | tf_op jit(solution)/shard_map/ppermute | solution.py:27
  19.8 4.8 %collective-permute-start.21 = (bf16[4,32,512]{2,1,0:T(8,128)(2,1)S(1)}, bf16[4,32,512]{2,1,0:T(8,128)(2,1)S(1)}, u32[]{:S(2)}, u32[]{:S(2)}) collective-permute-start(bf16[4,32,512]{2,1,0:T(8,128)(2,1)S(1)} %get-tuple-element.15), channel_id=1, source_target_pairs={{0,24},{2,26},{4,28},{6,30},{8,0},{10,2},{12,4},{14,6},{16,8},{18,... | collective-permute-start | bytes 393224 | tf_op jit(solution)/shard_map/ppermute | solution.py:27
  22.6 7.4 %collective-permute-start.20 = (bf16[4,32,512]{2,1,0:T(8,128)(2,1)S(1)}, bf16[4,32,512]{2,1,0:T(8,128)(2,1)S(1)}, u32[]{:S(2)}, u32[]{:S(2)}) collective-permute-start(bf16[4,32,512]{2,1,0:T(8,128)(2,1)S(1)} %get-tuple-element.15), channel_id=1, source_target_pairs={{0,8},{2,10},{4,12},{6,14},{8,16},{10,18},{12,20},{14,22},{16,24},... | collective-permute-start | bytes 393224 | tf_op jit(solution)/shard_map/ppermute | solution.py:27
  23.3 27.4 %copy-start.2 = (bf16[1024,2048]{1,0:T(8,128)(2,1)S(1)}, bf16[1024,2048]{1,0:T(8,128)(2,1)}, u32[]{:S(2)}) copy-start(bf16[1024,2048]{1,0:T(8,128)(2,1)} %param.13) | copy-start | bytes 12582916
  24.5 5.7 %collective-permute-start.22 = (bf16[4,32,512]{2,1,0:T(8,128)(2,1)S(1)}, bf16[4,32,512]{2,1,0:T(8,128)(2,1)S(1)}, u32[]{:S(2)}, u32[]{:S(2)}) collective-permute-start(bf16[4,32,512]{2,1,0:T(8,128)(2,1)S(1)} %collective-permute-done.21), channel_id=1, source_target_pairs={{0,24},{2,26},{4,28},{6,30},{8,0},{10,2},{12,4},{14,6},{16,8},{18,... | collective-permute-start | bytes 393224 | tf_op jit(solution)/shard_map/ppermute | solution.py:27
  28.0 11.7 %collective-permute-start.10 = (bf16[4,32,512]{2,1,0:T(8,128)(2,1)S(1)}, bf16[4,32,512]{2,1,0:T(8,128)(2,1)S(1)}, u32[]{:S(2)}, u32[]{:S(2)}) collective-permute-start(bf16[4,32,512]{2,1,0:T(8,128)(2,1)S(1)} %get-tuple-element.9), channel_id=1, source_target_pairs={{0,32},{2,34},{4,36},{6,38},{8,40},{10,42},{12,44},{14,46},{16,48}... | collective-permute-start | bytes 393224 | tf_op jit(solution)/shard_map/ppermute | solution.py:27
  30.0 11.2 %collective-permute-start.3 = (bf16[4,32,512]{2,1,0:T(8,128)(2,1)S(1)}, bf16[4,32,512]{2,1,0:T(8,128)(2,1)S(1)}, u32[]{:S(2)}, u32[]{:S(2)}) collective-permute-start(bf16[4,32,512]{2,1,0:T(8,128)(2,1)S(1)} %get-tuple-element.10), channel_id=1, source_target_pairs={{0,8},{2,10},{4,12},{6,14},{8,16},{10,18},{12,20},{14,22},{16,24},... | collective-permute-start | bytes 393224 | tf_op jit(solution)/shard_map/ppermute | solution.py:27
  30.3 18.0 %collective-permute-start.23 = (bf16[4,4,32,512]{3,2,1,0:T(8,128)(2,1)S(1)}, bf16[4,4,32,512]{3,2,1,0:T(8,128)(2,1)S(1)}, u32[]{:S(2)}, u32[]{:S(2)}) collective-permute-start(bf16[4,4,32,512]{3,2,1,0:T(8,128)(2,1)S(1)} %pad_maximum_fusion.2.refs_11_), channel_id=1, source_target_pairs={{0,2},{2,4},{4,6},{6,0},{8,10},{10,12},{12,14},{14,8},{16,18},{18,... | collective-permute-start | bytes 1572872 | tf_op jit(solution)/shard_map/ppermute | solution.py:27
  35.4 5.8 %collective-permute-start.12 = (bf16[4,32,512]{2,1,0:T(8,128)(2,1)S(1)}, bf16[4,32,512]{2,1,0:T(8,128)(2,1)S(1)}, u32[]{:S(2)}, u32[]{:S(2)}) collective-permute-start(bf16[4,32,512]{2,1,0:T(8,128)(2,1)S(1)} %get-tuple-element.9), channel_id=1, source_target_pairs={{0,96},{2,98},{4,100},{6,102},{8,104},{10,106},{12,108},{14,110},{... | collective-permute-start | bytes 393224 | tf_op jit(solution)/shard_map/ppermute | solution.py:27
  36.5 8.7 %collective-permute-start.5 = (bf16[4,32,512]{2,1,0:T(8,128)(2,1)S(1)}, bf16[4,32,512]{2,1,0:T(8,128)(2,1)S(1)}, u32[]{:S(2)}, u32[]{:S(2)}) collective-permute-start(bf16[4,32,512]{2,1,0:T(8,128)(2,1)S(1)} %get-tuple-element.10), channel_id=1, source_target_pairs={{0,24},{2,26},{4,28},{6,30},{8,0},{10,2},{12,4},{14,6},{16,8},{18,... | collective-permute-start | bytes 393224 | tf_op jit(solution)/shard_map/ppermute | solution.py:27
  39.7 5.3 %collective-permute-start.11 = (bf16[4,32,512]{2,1,0:T(8,128)(2,1)S(1)}, bf16[4,32,512]{2,1,0:T(8,128)(2,1)S(1)}, u32[]{:S(2)}, u32[]{:S(2)}) collective-permute-start(bf16[4,32,512]{2,1,0:T(8,128)(2,1)S(1)} %collective-permute-done.10), channel_id=1, source_target_pairs={{0,32},{2,34},{4,36},{6,38},{8,40},{10,42},{12,44},{14,46},{16,48}... | collective-permute-start | bytes 393224 | tf_op jit(solution)/shard_map/ppermute | solution.py:27
  41.2 6.6 %collective-permute-start.4 = (bf16[4,32,512]{2,1,0:T(8,128)(2,1)S(1)}, bf16[4,32,512]{2,1,0:T(8,128)(2,1)S(1)}, u32[]{:S(2)}, u32[]{:S(2)}) collective-permute-start(bf16[4,32,512]{2,1,0:T(8,128)(2,1)S(1)} %collective-permute-done.3), channel_id=1, source_target_pairs={{0,8},{2,10},{4,12},{6,14},{8,16},{10,18},{12,20},{14,22},{16,24},... | collective-permute-start | bytes 393224 | tf_op jit(solution)/shard_map/ppermute | solution.py:27
  41.3 15.8 %collective-permute-start.24 = (bf16[4,4,32,512]{3,2,1,0:T(8,128)(2,1)S(1)}, bf16[4,4,32,512]{3,2,1,0:T(8,128)(2,1)S(1)}, u32[]{:S(2)}, u32[]{:S(2)}) collective-permute-start(bf16[4,4,32,512]{3,2,1,0:T(8,128)(2,1)S(1)} %pad_maximum_fusion.2.refs_11_), channel_id=1, source_target_pairs={{0,6},{2,0},{4,2},{6,4},{8,14},{10,8},{12,10},{14,12},{16,22},{18,... | collective-permute-start | bytes 1572872 | tf_op jit(solution)/shard_map/ppermute | solution.py:27
  45.1 24.2 %collective-permute-start.13 = (bf16[4,4,32,512]{3,2,1,0:T(8,128)(2,1)S(1)}, bf16[4,4,32,512]{3,2,1,0:T(8,128)(2,1)S(1)}, u32[]{:S(2)}, u32[]{:S(2)}) collective-permute-start(bf16[4,4,32,512]{3,2,1,0:T(8,128)(2,1)S(1)} %pad_maximum_fusion.1.refs_6_), channel_id=1, source_target_pairs={{0,8},{2,10},{4,12},{6,14},{8,16},{10,18},{12,20},{14,22},{16,24},... | collective-permute-start | bytes 1572872 | tf_op jit(solution)/shard_map/ppermute | solution.py:27
  45.2 24.9 %collective-permute-start.14 = (bf16[4,4,32,512]{3,2,1,0:T(8,128)(2,1)S(1)}, bf16[4,4,32,512]{3,2,1,0:T(8,128)(2,1)}, u32[]{:S(2)}, u32[]{:S(2)}) collective-permute-start(bf16[4,4,32,512]{3,2,1,0:T(8,128)(2,1)S(1)} %pad_maximum_fusion.1.refs_6_), channel_id=1, source_target_pairs={{0,24},{2,26},{4,28},{6,30},{8,0},{10,2},{12,4},{14,6},{16,8},{18,... | collective-permute-start | bytes 1572872 | tf_op jit(solution)/shard_map/ppermute | solution.py:27
  48.0 23.8 %collective-permute-start.6 = (bf16[4,4,32,512]{3,2,1,0:T(8,128)(2,1)S(1)}, bf16[4,4,32,512]{3,2,1,0:T(8,128)(2,1)}, u32[]{:S(2)}, u32[]{:S(2)}) collective-permute-start(bf16[4,4,32,512]{3,2,1,0:T(8,128)(2,1)S(1)} %pad_maximum_fusion.refs_1_), channel_id=1, source_target_pairs={{0,32},{2,34},{4,36},{6,38},{8,40},{10,42},{12,44},{14,46},{16,48}... | collective-permute-start | bytes 1572872 | tf_op jit(solution)/shard_map/ppermute | solution.py:27
  48.3 27.8 %collective-permute-start.7 = (bf16[4,4,32,512]{3,2,1,0:T(8,128)(2,1)S(1)}, bf16[4,4,32,512]{3,2,1,0:T(8,128)(2,1)}, u32[]{:S(2)}, u32[]{:S(2)}) collective-permute-start(bf16[4,4,32,512]{3,2,1,0:T(8,128)(2,1)S(1)} %pad_maximum_fusion.refs_1_), channel_id=1, source_target_pairs={{0,96},{2,98},{4,100},{6,102},{8,104},{10,106},{12,108},{14,110},{... | collective-permute-start | bytes 1572872 | tf_op jit(solution)/shard_map/ppermute | solution.py:27
  57.0 32.2 %copy-start.9 = (bf16[4,4,32,512]{3,2,1,0:T(8,128)(2,1)}, bf16[4,4,32,512]{3,2,1,0:T(8,128)(2,1)S(1)}, u32[]{:S(2)}) copy-start(bf16[4,4,32,512]{3,2,1,0:T(8,128)(2,1)S(1)} %collective-permute-done.24.refs_13_) | copy-start | bytes 1572868
  57.0 20.4 %collective-permute-start.25 = (bf16[2,4,32,512]{3,2,1,0:T(8,128)(2,1)S(1)}, bf16[2,4,32,512]{3,2,1,0:T(8,128)(2,1)S(1)}, u32[]{:S(2)}, u32[]{:S(2)}) collective-permute-start(bf16[2,4,32,512]{3,2,1,0:T(8,128)(2,1)S(1)} %slice.38), channel_id=1, source_target_pairs={{0,2},{2,4},{4,6},{6,0},{8,10},{10,12},{12,14},{14,8},{16,18},{18,... | collective-permute-start | bytes 786440 | tf_op jit(solution)/shard_map/ppermute | solution.py:27
  69.3 11.4 %collective-permute-start.26 = (bf16[2,4,32,512]{3,2,1,0:T(8,128)(2,1)}, bf16[2,4,32,512]{3,2,1,0:T(8,128)(2,1)S(1)}, u32[]{:S(2)}, u32[]{:S(2)}) collective-permute-start(bf16[2,4,32,512]{3,2,1,0:T(8,128)(2,1)} %slice.39), channel_id=1, source_target_pairs={{0,6},{2,0},{4,2},{6,4},{8,14},{10,8},{12,10},{14,12},{16,22},{18,... | collective-permute-start | bytes 786440 | tf_op jit(solution)/shard_map/ppermute | solution.py:27
  70.1 10.6 %collective-permute-start.15 = (bf16[2,4,32,512]{3,2,1,0:T(8,128)(2,1)}, bf16[2,4,32,512]{3,2,1,0:T(8,128)(2,1)S(1)}, u32[]{:S(2)}, u32[]{:S(2)}) collective-permute-start(bf16[2,4,32,512]{3,2,1,0:T(8,128)(2,1)} %slice.36), channel_id=1, source_target_pairs={{0,8},{2,10},{4,12},{6,14},{8,16},{10,18},{12,20},{14,22},{16,24},... | collective-permute-start | bytes 786440 | tf_op jit(solution)/shard_map/ppermute | solution.py:27
  71.8 9.4 %collective-permute-start.16 = (bf16[2,4,32,512]{3,2,1,0:T(8,128)(2,1)}, bf16[2,4,32,512]{3,2,1,0:T(8,128)(2,1)S(1)}, u32[]{:S(2)}, u32[]{:S(2)}) collective-permute-start(bf16[2,4,32,512]{3,2,1,0:T(8,128)(2,1)} %slice.37), channel_id=1, source_target_pairs={{0,24},{2,26},{4,28},{6,30},{8,0},{10,2},{12,4},{14,6},{16,8},{18,... | collective-permute-start | bytes 786440 | tf_op jit(solution)/shard_map/ppermute | solution.py:27
  76.1 12.8 %collective-permute-start.8 = (bf16[2,4,32,512]{3,2,1,0:T(8,128)(2,1)}, bf16[2,4,32,512]{3,2,1,0:T(8,128)(2,1)S(1)}, u32[]{:S(2)}, u32[]{:S(2)}) collective-permute-start(bf16[2,4,32,512]{3,2,1,0:T(8,128)(2,1)} %slice.33), channel_id=1, source_target_pairs={{0,32},{2,34},{4,36},{6,38},{8,40},{10,42},{12,44},{14,46},{16,48}... | collective-permute-start | bytes 786440 | tf_op jit(solution)/shard_map/ppermute | solution.py:27
  77.5 11.8 %collective-permute-start.9 = (bf16[2,4,32,512]{3,2,1,0:T(8,128)(2,1)S(1)}, bf16[2,4,32,512]{3,2,1,0:T(8,128)(2,1)S(1)}, u32[]{:S(2)}, u32[]{:S(2)}) collective-permute-start(bf16[2,4,32,512]{3,2,1,0:T(8,128)(2,1)S(1)} %slice.34), channel_id=1, source_target_pairs={{0,96},{2,98},{4,100},{6,102},{8,104},{10,106},{12,108},{14,110},{... | collective-permute-start | bytes 786440 | tf_op jit(solution)/shard_map/ppermute | solution.py:27
  100.6 20.7 %collective-permute-start.27 = (bf16[512,2048]{1,0:T(8,128)(2,1)}, bf16[512,2048]{1,0:T(8,128)(2,1)}, u32[]{:S(2)}, u32[]{:S(2)}) collective-permute-start(bf16[512,2048]{1,0:T(8,128)(2,1)} %mixer_other.1), channel_id=1, source_target_pairs={{0,1},{1,0},{2,3},{3,2},{4,5},{5,4},{6,7},{7,6},{8,9},{9,8},{10,11... | collective-permute-start | bytes 6291464 | tf_op jit(solution)/shard_map/ppermute | solution.py:316
  (18 other events, 210.3 us)
Sparse Core Ops, SparseCore 0:
  10.3 124.6 all-gather.2

commit v2 on v1

--- a/solution.py
+++ b/solution.py
@@ -78,7 +78,9 @@
 def mixer_body(own, *refs):
     normed_hbm = refs[0]
     for_unit, for_value, for_out = refs[1:6], refs[6:11], refs[11:16]
-    mask_w, bias, gain, shifts, out, rows, w_unit, w_value, w_out, sem_x, sem_u, sem_v, sem_o = refs[16:]
+    mask_w, bias, gain, shifts, out = refs[16:21]
+    early = refs[21] if not own else None
+    rows, w_unit, w_value, w_out, sem_x, sem_u, sem_v, sem_o, sem_e = refs[-9:]
     tp, rep, fs = lax.axis_index("tp"), lax.axis_index("rep"), lax.axis_index("fs")
     z, y, x_at = 2 * rep + fs // 16, fs // RING % RING, fs % RING
     count = rows.shape[0]
@@ -90,30 +92,36 @@
         to = pl.ds(pl.multiple_of(at_z // 2 * part, part), part)
         pltpu.make_async_copy(ref.at[index], w.at[at_z % 2, at_y, :, to], sem).start()
 
-    for piece, low, inner, outer in RELAYED:
-        at_z, at_y = (z + RING - outer) % RING, (y + RING - outer) % RING
-
-        def copies(i, carry, piece=piece, low=low, outer=outer):
-            near_z, near_y = (z + RING - low - i) % RING, (y + RING - low - i) % RING
-            line(for_value[piece], i, w_value, sem_v, near_z, at_y)
-            line(for_unit[piece], i, w_unit, sem_u, at_z, near_y)
-            for r in range(2):
-                pltpu.make_async_copy(
-                    for_out[piece].at[i, pl.ds(2 * r, 2)],
-                    w_out.at[:, near_y, (x_at + RING - outer) % RING, pl.ds(r * part, part)],
-                    sem_o,
-                ).start()
-            return carry
-
-        lax.fori_loop(0, inner, copies, 0)
+    def value_copies(piece, i, near, outer):
+        line(for_value[piece], i, w_value, sem_v, (z + RING - near) % RING, (y + RING - outer) % RING)
+
+    def unit_copies(piece, i, near, outer):
+        line(for_unit[piece], i, w_unit, sem_u, (z + RING - outer) % RING, (y + RING - near) % RING)
+
+    def out_copies(piece, i, near, outer):
+        for r in range(2):
+            pltpu.make_async_copy(
+                for_out[piece].at[i, pl.ds(2 * r, 2)],
+                w_out.at[:, (y + RING - near) % RING, (x_at + RING - outer) % RING, pl.ds(r * part, part)],
+                sem_o,
+            ).start()
+
+    for start_copies in (value_copies, unit_copies, out_copies):
+        for piece, low, inner, outer in RELAYED:
+
+            def step(i, carry, piece=piece, low=low, outer=outer):
+                start_copies(piece, i, low + i, outer)
+                return carry
+
+            lax.fori_loop(0, inner, step, 0)
 
     pltpu.make_async_copy(normed_hbm.at[pl.ds(start, count)], rows, sem_x).wait()
     pltpu.make_async_copy(w_value, w_value, sem_v).wait()
     x = rows[...]
-    model, width = x.shape[1], w_value.shape[-1]
-    value = gelu(dot_nn(x, w_value[...].reshape(model, width)))
+    model, width = x.shape[1], gain.shape[-1]
+    value = gelu(dot_nn(x, w_value[:, :, :, :, :width].reshape(model, width)))
     pltpu.make_async_copy(w_unit, w_unit, sem_u).wait()
-    unit = gelu(dot_nn(x, w_unit[...].reshape(model, width)))
+    unit = gelu(dot_nn(x, w_unit[:, :, :, :, :width].reshape(model, width)))
     groups, block = mask_w.shape[0], mask_w.shape[1]
     per = width // groups
     parts = []
@@ -130,24 +138,104 @@
         parts.append((unit[:, g * per : (g + 1) * per] * jnp.concatenate(mixed, axis=0)).astype(BF16))
     gated = jnp.concatenate(parts, axis=1)
     pltpu.make_async_copy(w_out, w_out, sem_o).wait()
-    out[...] = dot_nt(gated, w_out[...].reshape(model, width)).astype(out.dtype)
+    hands = [] if own else [
+        pltpu.make_async_copy(w.at[:, :, :, :, pl.ds(width, EARLY)], early.at[k], sem_e.at[k])
+        for k, w in enumerate((w_unit, w_value, w_out))
+    ]
+    for hand in hands:
+        hand.start()
+    out[...] = dot_nt(gated, w_out[:, :, :, :, :width].reshape(model, width)).astype(out.dtype)
+    for hand in hands:
+        hand.wait()
 
 
 def mixer(own, normed, pieces, mask_w, bias, gain, shifts, count, dtype):
-    model, width = normed.shape[1], pieces[0].shape[-1]
-    weight = pltpu.VMEM((2, RING, RING, model // 32, width), BF16)
+    model, wide = normed.shape[1], pieces[0].shape[-1]
+    lines = (2, RING, RING, model // 32)
+    weight = pltpu.VMEM((*lines, wide), BF16)
+    shape = jax.ShapeDtypeStruct((count, model), dtype)
+    early = jax.ShapeDtypeStruct((3, *lines, EARLY), BF16)
     return pl.pallas_call(
         functools.partial(mixer_body, own),
-        out_shape=jax.ShapeDtypeStruct((count, model), dtype),
+        out_shape=shape if own else (shape, early),
         in_specs=[ANY] * 16 + [VMEM] * 4,
-        out_specs=VMEM,
-        scratch_shapes=[pltpu.VMEM((count, model), BF16), weight, weight, weight] + [pltpu.SemaphoreType.DMA] * 4,
+        out_specs=VMEM if own else (VMEM, ANY),
+        scratch_shapes=[pltpu.VMEM((count, model), BF16), weight, weight, weight]
+        + [pltpu.SemaphoreType.DMA] * 4 + [pltpu.SemaphoreType.DMA((3,))],
         compiler_params=pltpu.CompilerParams(vmem_limit_bytes=56 * 2**20),
         name="mixer_own" if own else "mixer_other",
     )(normed, *pieces, mask_w, bias, gain, shifts)
 
 
+def early_body(tokens, kept_hbm, arrived_hbm, norm_gain, mine, theirs, acc, normed, rows, kept, arrived, mid, down, sem, sem_w, sem_d):
+    tp = lax.axis_index("tp")
+    count, model = rows.shape
+    start = pl.multiple_of(tp * count, count)
+    steps = count // 4
+    ways = []
+    for k in range(4):
+        line = pl.ds(k * steps, steps)
+        ways.append(
+            [
+                pltpu.make_async_copy(tokens.at[pl.ds(start + k * steps, steps)], rows.at[line], sem.at[k, 0]),
+                pltpu.make_async_copy(kept_hbm.at[line], kept.at[line], sem.at[k, 1]),
+                pltpu.make_async_copy(arrived_hbm.at[line], arrived.at[line], sem.at[k, 2]),
+            ]
+        )
+    weights = [
+        pltpu.make_async_copy(
+            src.at[w], mid.at[:, :, :, :, pl.ds((2 * w + t) * EARLY, EARLY)], sem_w.at[w, t]
+        )
+        for t, src in enumerate((mine, theirs))
+        for w in range(2)
+    ]
+    downs = [
+        pltpu.make_async_copy(src.at[2], down.at[:, :, :, :, pl.ds(t * EARLY, EARLY)], sem_d.at[t])
+        for t, src in enumerate((mine, theirs))
+    ]
+    for copies in (*ways, weights, downs):
+        for copy in copies:
+            copy.start()
+    for k in range(4):
+        line = slice(k * steps, (k + 1) * steps)
+        for copy in ways[k]:
+            copy.wait()
+        h = rows[line].astype(F32) + (kept[line] + arrived[line].astype(F32))
+        h = h.astype(BF16).astype(F32)
+        kept[line] = h
+        scale = lax.rsqrt(jnp.mean(h * h, axis=-1, keepdims=True) + 1e-06)
+        normed[line] = (h * scale * norm_gain[...]).astype(BF16)
+    for copy in weights:
+        copy.wait()
+    both = 2 * EARLY
+    r = dot_nn(normed[...], mid[...].reshape(model, 2 * both))
+    hidden = (jax.nn.silu(r[:, :both]) * r[:, both:]).astype(BF16)
+    for copy in downs:
+        copy.wait()
+    acc[...] = kept[...] + dot_nt(hidden, down[...].reshape(model, both))
+
+
+def early_units(tokens, kept, arrived, gain, mine, theirs):
+    count, model = kept.shape
+    lines = mine.shape[1:-1]
+    row = pltpu.VMEM((count, model), BF16)
+    return pl.pallas_call(
+        early_body,
+        out_shape=(jax.ShapeDtypeStruct((count, model), F32), jax.ShapeDtypeStruct((count, model), BF16)),
+        in_specs=[ANY, ANY, ANY, VMEM, ANY, ANY],
+        out_specs=(VMEM, VMEM),
+        scratch_shapes=[
+            row, pltpu.VMEM((count, model), F32), row,
+            pltpu.VMEM((*lines, 4 * EARLY), BF16), pltpu.VMEM((*lines, 2 * EARLY), BF16),
+            pltpu.SemaphoreType.DMA((4, 3)), pltpu.SemaphoreType.DMA((2, 2)), pltpu.SemaphoreType.DMA((2,)),
+        ],
+        compiler_params=pltpu.CompilerParams(vmem_limit_bytes=56 * 2**20),
+        name="early_units",
+    )(tokens, kept, arrived, gain, mine, theirs)
+
+
 CHUNK = 512
+EARLY = 128
 
 
 def ffn_body(h_hbm, n_hbm, packed, out_hbm, h_mid, normed, mid, down, hidden, out, sem_h, sem_n, sem_w, sem_d, sem_o):
@@ -224,7 +312,7 @@
 
     def back(k, carry):
         cols = pl.ds(pl.multiple_of(k * CHUNK, CHUNK), CHUNK)
-        acc = h_mid[:, cols].astype(F32)
+        acc = h_mid[:, cols]
         for t in range(tps):
             w = down[t, pl.ds(k * lines, lines)].reshape(CHUNK, wide)
             acc = acc + dot_nt(hidden[:, t * wide : (t + 1) * wide], w)
@@ -246,7 +334,7 @@
         in_specs=[ANY] * 3,
         out_specs=ANY,
         scratch_shapes=[
-            row, row, pltpu.VMEM((fs, share, 2 * tps * wide), BF16), pltpu.VMEM((tps, fs, share, wide), BF16),
+            pltpu.VMEM(h_mid.shape, F32), row, pltpu.VMEM((fs, share, 2 * tps * wide), BF16), pltpu.VMEM((tps, fs, share, wide), BF16),
             pltpu.VMEM((h_mid.shape[0], tps * wide), BF16), row,
             pltpu.SemaphoreType.DMA, pltpu.SemaphoreType.DMA, pltpu.SemaphoreType.DMA((-(-tps * wide // CHUNK),)),
             pltpu.SemaphoreType.DMA, pltpu.SemaphoreType.DMA((h_mid.shape[1] // CHUNK,)),
@@ -260,15 +348,15 @@
     rep = lax.axis_index("rep")
     share = gate.shape[0]
     half = share // 2
-    out[:share] = jnp.where(rep == 0, gate[...], up[...])
-    out[share:] = down[pl.ds(pl.multiple_of(rep * half, half), half)]
+    out[:share] = jnp.where(rep == 0, gate[:, EARLY:], up[:, EARLY:])
+    out[share:] = down[pl.ds(pl.multiple_of(rep * half, half), half), EARLY:]
 
 
 def pack(gate, up, down):
     share, wide = gate.shape
     return pl.pallas_call(
         pack_body,
-        out_shape=jax.ShapeDtypeStruct((share + share // 2, wide), gate.dtype),
+        out_shape=jax.ShapeDtypeStruct((share + share // 2, wide - EARLY), gate.dtype),
         in_specs=[VMEM] * 3,
         out_specs=VMEM,
         name="pack",
@@ -293,11 +381,16 @@
     packed = lax.all_gather(packed, EVERY).reshape(tps, reps, fss, *packed.shape)
 
     part = share // 2
-    line = jnp.concatenate([half_rows(w_unit, rep), half_rows(w_value, rep)], axis=0)
+
+    def beside(w, extra):
+        return jnp.concatenate([half_rows(w, rep), half_rows(extra[:, :EARLY], rep)], axis=1)
+
+    line = jnp.concatenate([beside(w_unit, w_gate), beside(w_value, w_up)], axis=0)
     line = in_place(direct_ring(line, 2), fs % RING)
     for_unit = relayed_ring(jnp.stack(passed_ring(line[:, :part], 1, 1)), 0)
     for_value = relayed_ring(jnp.stack(passed_ring(line[:, part:], 0, 1)), 1)
-    for_out = in_place(direct_ring(half_rows(w_mix_out.T, rep), 0), 2 * rep + fs // 16)
+    for_out = beside(w_mix_out.T, w_down.T)
+    for_out = in_place(direct_ring(for_out, 0), 2 * rep + fs // 16)
     for_out = relayed_ring(jnp.stack(passed_ring(for_out, 1, -1)), 2)
 
     groups = spatial.shape[0] // tps
@@ -312,13 +405,14 @@
         mixer, normed=normed, pieces=(*for_unit, *for_value, *for_out), mask_w=mask_w, bias=bias, gain=gain,
         shifts=shifts, count=rows,
     )
-    other = unit(False, dtype=BF16)
-    arrived = lax.ppermute(other, "tp", [(i, (i + 1) % tps) for i in range(tps)])
+    other, early = unit(False, dtype=BF16)
+    swap = [(i, (i + 1) % tps) for i in range(tps)]
+    arrived = lax.ppermute(other, "tp", swap)
+    early_theirs = lax.ppermute(early, "tp", swap)
     kept = unit(True, dtype=F32)
-    residual = lax.dynamic_slice_in_dim(tokens, tp * rows, rows, 0).astype(F32)
-    h_mid = (residual + (kept + arrived.astype(F32))).astype(BF16)
-    normed_mid = rms_scale(h_mid, norm_ffn).astype(BF16)
-    return ffn(h_mid, normed_mid, packed, share)
+    gain = norm_ffn.astype(F32)[None]
+    acc, normed_mid = early_units(tokens, kept, arrived, gain, early, early_theirs)
+    return ffn(acc, normed_mid, packed, share)
 
 
 def solution(mesh):

time: 166 us -> 163 us (0.982)
  other arithmetic: 16.2 us -> 7.09 us
  Pallas kernels: 47.6 us -> 51.4 us
  waiting for transfers between devices: 33.6 us -> 36.3 us
  starting transfers between devices: 45.9 us -> 43.6 us
    ppermute x27, waiting for transfers between devices: 25.8 us -> 36.3 us  [shift(): return lax.ppermute(x, CHIPS, pairs)]
    all_gather x1, waiting for transfers between devices: 7.7 us -> 0.02 us  [on_device(): lax.all_gather(packed, EVERY).reshape(tps, reps, fss, *packed.shape)]
    reduce_sum x2 -> x1, other arithmetic: 7.19 us -> 0.88 us  [rms_scale(): scale = lax.rsqrt(jnp.mean(values * values, axis=-1, keepdims=True) + 1e-06)]
    pallas_call x2 -> x3, Pallas kernels: 22.3 us -> 27.9 us  [the longest x2 18.4 us: mixer(): pl.pallas_call(functools.partial(mixer_body, own), out_shape=shape if own...]
    ppermute x1 -> x2, starting transfers between devices: 9 us -> 4.9 us  [the longest x1 4.81 us: on_device(): arrived = lax.ppermute(other, 'tp', swap)]
    slice x0 -> x3, local copies, waits for them, and re-layouts: none -> 2.16 us  [beside(): extra[:, :EARLY]]
    convert_element_type x1 -> x0, other arithmetic: 1.94 us -> none  [on_device(): normed_mid = rms_scale(h_mid, norm_ffn).astype(BF16)]
    ppermute x27, starting transfers between devices: 36.9 us -> 38.7 us  [shift(): return lax.ppermute(x, CHIPS, pairs)]
  transfers between devices with their start and end apart: 29 -> 30, of which waited for: 10 -> 11; matrix products, arithmetic and copies ran while one was open for 14% -> 9% of each run, Pallas kernels for 13% -> 17%
where the time goes in v2:
time: 163 us; the launch traced here: 162 us
  Pallas kernels  51.4 us (32%)
  starting transfers between devices  43.6 us (27%)
  waiting for transfers between devices  36.3 us (22%)
  between operations  13.9 us (9%)
  local copies, waits for them, and re-layouts  9.8 us (6%)
  other arithmetic  7.09 us (4%)
    ppermute x27, starting transfers between devices, shift(): return lax.ppermute(x, CHIPS, pairs)  38.7 us
    ppermute x27, waiting for transfers between devices, shift(): return lax.ppermute(x, CHIPS, pairs)  36.3 us
    pallas_call x1, Pallas kernels, ffn(): pl.pallas_call(ffn_body, out_shape=jax.ShapeDtypeStruct(h_mid.shape, BF16...  21.7 us
    pallas_call x2, Pallas kernels, mixer(): pl.pallas_call(functools.partial(mixer_body, own), out_shape=shape if own...  18.4 us
    pallas_call x1, Pallas kernels, early_units(): pl.pallas_call(early_body, out_shape=(jax.ShapeDtypeStruct((count, model)...  9.52 us
    ppermute x1, starting transfers between devices, on_device(): arrived = lax.ppermute(other, 'tp', swap)  4.81 us
  transfers between devices with their start and end apart: 30, of which 11 were waited for; matrix products, arithmetic and copies ran while one was open for 9% of the time, Pallas kernels for 17%

profile of v2, /device:TPU:1, one launch (start us, length us, event | category | flops | bytes accessed | tf_op | source)
XLA Modules:
  0.0 162.2 jit_solution(8084746371700920254)
XLA Ops:
  6.5 1.8 %pack.1 = bf16[96,1280]{1,0:T(8,128)(2,1)} custom-call(bf16[64,1408]{1,0:T(8,128)(2,1)} %gate.1, bf16[64,1408]{1,0:T(8,128)(2,1)} %up.1, bf16[64,1408]{1,0:T(8,128)(2,1)} %bitcast.41), custom_call_target="tpu_custom_call" | custom-call | tf_op jit(solution)/shard_map/pack/pallas_call | solution.py:357
  9.2 4.6 %collective-permute-start.17 = (bf16[32,640]{1,0:T(8,128)(2,1)S(1)}, bf16[32,640]{1,0:T(8,128)(2,1)S(1)}, u32[]{:S(2)}, u32[]{:S(2)}) collective-permute-start(bf16[32,640]{1,0:T(8,128)(2,1)S(1)} %pad_maximum_fusion.5), channel_id=1, source_target_pairs={{0,96},{2,98},{4,100},{6,102},{8,104},{10,106},{12,108},{14,110},{... | collective-permute-start | bytes 122888 | tf_op jit(solution)/shard_map/ppermute | solution.py:27
  16.7 2.5 %collective-permute-start = (bf16[64,640]{1,0:T(8,128)(2,1)S(1)}, bf16[64,640]{1,0:T(8,128)(2,1)S(1)}, u32[]{:S(2)}, u32[]{:S(2)}) collective-permute-start(bf16[64,640]{1,0:T(8,128)(2,1)S(1)} %maximum_maximum_fusion), channel_id=1, source_target_pairs={{0,6},{2,0},{4,2},{6,4},{8,14},{10,8},{12,10},{14,12},{16,22},{18,... | collective-permute-start | bytes 245768 | tf_op jit(solution)/shard_map/ppermute | solution.py:27
  20.6 2.8 %collective-permute-start.21 = (bf16[4,32,640]{2,1,0:T(8,128)(2,1)S(1)}, bf16[4,32,640]{2,1,0:T(8,128)(2,1)S(1)}, u32[]{:S(2)}, u32[]{:S(2)}) collective-permute-start(bf16[4,32,640]{2,1,0:T(8,128)(2,1)S(1)} %get-tuple-element.22), channel_id=1, source_target_pairs={{0,24},{2,26},{4,28},{6,30},{8,0},{10,2},{12,4},{14,6},{16,8},{18,... | collective-permute-start | bytes 491528 | tf_op jit(solution)/shard_map/ppermute | solution.py:27
  25.2 1.3 collective-permute-done.21
  26.5 3.4 %collective-permute-start.22 = (bf16[4,32,640]{2,1,0:T(8,128)(2,1)S(1)}, bf16[4,32,640]{2,1,0:T(8,128)(2,1)S(1)}, u32[]{:S(2)}, u32[]{:S(2)}) collective-permute-start(bf16[4,32,640]{2,1,0:T(8,128)(2,1)S(1)} %collective-permute-done.21), channel_id=1, source_target_pairs={{0,24},{2,26},{4,28},{6,30},{8,0},{10,2},{12,4},{14,6},{16,8},{18,... | collective-permute-start | bytes 491528 | tf_op jit(solution)/shard_map/ppermute | solution.py:27
  30.0 2.0 %collective-permute-start.10 = (bf16[4,32,640]{2,1,0:T(8,128)(2,1)S(1)}, bf16[4,32,640]{2,1,0:T(8,128)(2,1)S(1)}, u32[]{:S(2)}, u32[]{:S(2)}) collective-permute-start(bf16[4,32,640]{2,1,0:T(8,128)(2,1)S(1)} %get-tuple-element.15), channel_id=1, source_target_pairs={{0,32},{2,34},{4,36},{6,38},{8,40},{10,42},{12,44},{14,46},{16,48}... | collective-permute-start | bytes 491528 | tf_op jit(solution)/shard_map/ppermute | solution.py:27
  32.6 1.4 collective-permute-start.23
  35.0 2.3 %collective-permute-start.12 = (bf16[4,32,640]{2,1,0:T(8,128)(2,1)S(1)}, bf16[4,32,640]{2,1,0:T(8,128)(2,1)S(1)}, u32[]{:S(2)}, u32[]{:S(2)}) collective-permute-start(bf16[4,32,640]{2,1,0:T(8,128)(2,1)S(1)} %get-tuple-element.15), channel_id=1, source_target_pairs={{0,96},{2,98},{4,100},{6,102},{8,104},{10,106},{12,108},{14,110},{... | collective-permute-start | bytes 491528 | tf_op jit(solution)/shard_map/ppermute | solution.py:27
  37.3 3.2 %collective-permute-start.5 = (bf16[4,32,640]{2,1,0:T(8,128)(2,1)S(1)}, bf16[4,32,640]{2,1,0:T(8,128)(2,1)S(1)}, u32[]{:S(2)}, u32[]{:S(2)}) collective-permute-start(bf16[4,32,640]{2,1,0:T(8,128)(2,1)S(1)} %get-tuple-element.16), channel_id=1, source_target_pairs={{0,24},{2,26},{4,28},{6,30},{8,0},{10,2},{12,4},{14,6},{16,8},{18,... | collective-permute-start | bytes 491528 | tf_op jit(solution)/shard_map/ppermute | solution.py:27
  41.6 4.6 %collective-permute-done.11 = bf16[4,32,640]{2,1,0:T(8,128)(2,1)S(1)} collective-permute-done((bf16[4,32,640]{2,1,0:T(8,128)(2,1)S(1)}, bf16[4,32,640]{2,1,0:T(8,128)(2,1)S(1)}, u32[]{:S(2)}, u32[]{:S(2)}) %collective-permute-start.11) | collective-permute-done | bytes 163872 | tf_op jit(solution)/shard_map/ppermute | solution.py:27
  46.4 2.7 %collective-permute-start.14 = (bf16[4,4,32,640]{3,2,1,0:T(8,128)(2,1)S(1)}, bf16[4,4,32,640]{3,2,1,0:T(8,128)(2,1)}, u32[]{:S(2)}, u32[]{:S(2)}) collective-permute-start(bf16[4,4,32,640]{3,2,1,0:T(8,128)(2,1)S(1)} %pad_maximum_fusion.1.refs_6_), channel_id=1, source_target_pairs={{0,24},{2,26},{4,28},{6,30},{8,0},{10,2},{12,4},{14,6},{16,8},{18,... | collective-permute-start | bytes 1966088 | tf_op jit(solution)/shard_map/ppermute | solution.py:27
  49.3 2.6 %collective-permute-start.7 = (bf16[4,4,32,640]{3,2,1,0:T(8,128)(2,1)S(1)}, bf16[4,4,32,640]{3,2,1,0:T(8,128)(2,1)}, u32[]{:S(2)}, u32[]{:S(2)}) collective-permute-start(bf16[4,4,32,640]{3,2,1,0:T(8,128)(2,1)S(1)} %pad_maximum_fusion.refs_1_), channel_id=1, source_target_pairs={{0,96},{2,98},{4,100},{6,102},{8,104},{10,106},{12,108},{14,110},{... | collective-permute-start | bytes 1966088 | tf_op jit(solution)/shard_map/ppermute | solution.py:27
  52.0 3.0 %fusion.2.refs_0_ = bf16[1024,2048]{1,0:T(8,128)(2,1)} fusion(bf16[1024,2048]{1,0:T(8,128)(2,1)S(1)} %copy-done.2, f32[2048]{0:T(1024)S(1)} %convert_element_type.16, f32[1024]{0:T(1024)S(1)} %add_rsqrt_fusion), kind=kLoop, calls=%fused_computation.4 | loop fusion | flops 8388608 | bytes 8400896 | tf_op jit(solution)/shard_map/convert_element_type | solution.py:402
  55.2 5.6 %collective-permute-done.24.refs_13_ = bf16[4,4,32,640]{3,2,1,0:T(8,128)(2,1)S(1)} collective-permute-done((bf16[4,4,32,640]{3,2,1,0:T(8,128)(2,1)S(1)}, bf16[4,4,32,640]{3,2,1,0:T(8,128)(2,1)S(1)}, u32[]{:S(2)}, u32[]{:S(2)}) %collective-permute-start.24) | collective-permute-done | bytes 655392 | tf_op jit(solution)/shard_map/ppermute | solution.py:27
  61.6 10.6 %collective-permute-done.13.refs_7_ = bf16[4,4,32,640]{3,2,1,0:T(8,128)(2,1)} collective-permute-done((bf16[4,4,32,640]{3,2,1,0:T(8,128)(2,1)S(1)}, bf16[4,4,32,640]{3,2,1,0:T(8,128)(2,1)}, u32[]{:S(2)}, u32[]{:S(2)}) %collective-permute-start.13) | collective-permute-done | bytes 655392 | tf_op jit(solution)/shard_map/ppermute | solution.py:27
  72.2 2.4 %collective-permute-start.26 = (bf16[2,4,32,640]{3,2,1,0:T(8,128)(2,1)S(1)}, bf16[2,4,32,640]{3,2,1,0:T(8,128)(2,1)S(1)}, u32[]{:S(2)}, u32[]{:S(2)}) collective-permute-start(bf16[2,4,32,640]{3,2,1,0:T(8,128)(2,1)S(1)} %slice.52), channel_id=1, source_target_pairs={{0,6},{2,0},{4,2},{6,4},{8,14},{10,8},{12,10},{14,12},{16,22},{18,... | collective-permute-start | bytes 983048 | tf_op jit(solution)/shard_map/ppermute | solution.py:27
  74.6 1.0 slice.48
  75.7 1.0 slice.49
  76.7 2.7 %collective-permute-start.16 = (bf16[2,4,32,640]{3,2,1,0:T(8,128)(2,1)S(1)}, bf16[2,4,32,640]{3,2,1,0:T(8,128)(2,1)S(1)}, u32[]{:S(2)}, u32[]{:S(2)}) collective-permute-start(bf16[2,4,32,640]{3,2,1,0:T(8,128)(2,1)S(1)} %slice.49), channel_id=1, source_target_pairs={{0,24},{2,26},{4,28},{6,30},{8,0},{10,2},{12,4},{14,6},{16,8},{18,... | collective-permute-start | bytes 983048 | tf_op jit(solution)/shard_map/ppermute | solution.py:27
  79.5 1.0 slice.45
  80.6 1.0 slice.46
  81.6 2.7 %collective-permute-start.9 = (bf16[2,4,32,640]{3,2,1,0:T(8,128)(2,1)S(1)}, bf16[2,4,32,640]{3,2,1,0:T(8,128)(2,1)S(1)}, u32[]{:S(2)}, u32[]{:S(2)}) collective-permute-start(bf16[2,4,32,640]{3,2,1,0:T(8,128)(2,1)S(1)} %slice.46), channel_id=1, source_target_pairs={{0,96},{2,98},{4,100},{6,102},{8,104},{10,106},{12,108},{14,110},{... | collective-permute-start | bytes 983048 | tf_op jit(solution)/shard_map/ppermute | solution.py:27
  85.6 6.3 %collective-permute-done.15.refs_9_ = bf16[2,4,32,640]{3,2,1,0:T(8,128)(2,1)S(1)} collective-permute-done((bf16[2,4,32,640]{3,2,1,0:T(8,128)(2,1)S(1)}, bf16[2,4,32,640]{3,2,1,0:T(8,128)(2,1)S(1)}, u32[]{:S(2)}, u32[]{:S(2)}) %collective-permute-start.15) | collective-permute-done | bytes 327712 | tf_op jit(solution)/shard_map/ppermute | solution.py:27
  91.9 1.0 collective-permute-done.16.refs_10_
  92.9 4.5 %collective-permute-done.8.refs_4_ = bf16[2,4,32,640]{3,2,1,0:T(8,128)(2,1)S(1)} collective-permute-done((bf16[2,4,32,640]{3,2,1,0:T(8,128)(2,1)S(1)}, bf16[2,4,32,640]{3,2,1,0:T(8,128)(2,1)S(1)}, u32[]{:S(2)}, u32[]{:S(2)}) %collective-permute-start.8) | collective-permute-done | bytes 327712 | tf_op jit(solution)/shard_map/ppermute | solution.py:27
  98.3 8.9 %mixer_other.1 = (bf16[512,2048]{1,0:T(8,128)(2,1)}, bf16[3,2,4,4,64,128]{5,4,3,2,1,0:T(8,128)(2,1)}) custom-call(bf16[1024,2048]{1,0:T(8,128)(2,1)} %fusion.2.refs_0_, bf16[4,4,32,640]{3,2,1,0:T(8,128)(2,1)} %copy-done.5, bf16[4,4,32,640]{3,2,1,0:T(8,128)(2,1)} %collective-permute-done.6.refs_2_, bf16[4,4,32,640]{3,2,1,0:T(8,128)(2,1)} %collective-permute-done.7.refs_3_, ...), custom_call_target="tpu_custom_call" | custom-call | tf_op jit(solution)/shard_map/mixer_other/pallas_call | solution.py:158
  107.2 4.8 %collective-permute-start.27 = (bf16[512,2048]{1,0:T(8,128)(2,1)}, bf16[512,2048]{1,0:T(8,128)(2,1)S(1)}, u32[]{:S(2)}, u32[]{:S(2)}) collective-permute-start(bf16[512,2048]{1,0:T(8,128)(2,1)} %get-tuple-element.9), channel_id=1, source_target_pairs={{0,1},{1,0},{2,3},{3,2},{4,5},{5,4},{6,7},{7,6},{8,9},{9,8},{10,11... | collective-permute-start | bytes 6291464 | tf_op jit(solution)/shard_map/ppermute | solution.py:410
  112.7 9.5 %mixer_own.1.kept_hbm = f32[512,2048]{1,0:T(8,128)} custom-call(bf16[1024,2048]{1,0:T(8,128)(2,1)} %fusion.2.refs_0_, bf16[4,4,32,640]{3,2,1,0:T(8,128)(2,1)} %copy-done.5, bf16[4,4,32,640]{3,2,1,0:T(8,128)(2,1)} %collective-permute-done.6.refs_2_, bf16[4,4,32,640]{3,2,1,0:T(8,128)(2,1)} %collective-permute-done.7.refs_3_, ...), custom_call_target="tpu_custom_call" | custom-call | tf_op jit(solution)/shard_map/mixer_own/pallas_call | solution.py:158
  122.2 1.1 copy-done.9
  124.0 9.5 %early_units.1 = (f32[512,2048]{1,0:T(8,128)}, bf16[512,2048]{1,0:T(8,128)(2,1)}) custom-call(bf16[1024,2048]{1,0:T(8,128)(2,1)} %tokens.1, f32[512,2048]{1,0:T(8,128)} %mixer_own.1.kept_hbm, bf16[512,2048]{1,0:T(8,128)(2,1)} %copy-done.8, f32[1,2048]{1,0:T(1,128)} %bitcast.52, bf16[3,2,4,4,64,128]{5,4,3,2,1,0:T(8,128)(2,1)} %get-tuple-element.10.mine, ...), custom_call_target="tpu_custom_call" | custom-call | tf_op jit(solution)/shard_map/early_units/pallas_call | solution.py:222
  133.6 21.7 %ffn.1 = bf16[512,2048]{1,0:T(8,128)(2,1)} custom-call(f32[512,2048]{1,0:T(8,128)} %get-tuple-element.11.h_hbm, bf16[512,2048]{1,0:T(8,128)(2,1)} %get-tuple-element.12.n_hbm, bf16[2,2,32,96,1280]{4,3,2,1,0:T(8,128)(2,1)} %bitcast.40), custom_call_target="tpu_custom_call" | custom-call | tf_op jit(solution)/shard_map/ffn/pallas_call | solution.py:331
  (114 shorter events, 14.3 us)
Async XLA Ops:
  6.5 127.0 %all-gather.3.cloned.1.call-start = ((), (), s32[]{:S(2)}) async-start(), calls=%async_computation | async-start | bytes 31703040 | tf_op jit(solution)/shard_map/all_gather | solution.py:381
  9.2 10.7 %collective-permute-start.17 = (bf16[32,640]{1,0:T(8,128)(2,1)S(1)}, bf16[32,640]{1,0:T(8,128)(2,1)S(1)}, u32[]{:S(2)}, u32[]{:S(2)}) collective-permute-start(bf16[32,640]{1,0:T(8,128)(2,1)S(1)} %pad_maximum_fusion.5), channel_id=1, source_target_pairs={{0,96},{2,98},{4,100},{6,102},{8,104},{10,106},{12,108},{14,110},{... | collective-permute-start | bytes 122888 | tf_op jit(solution)/shard_map/ppermute | solution.py:27
  13.8 6.6 %collective-permute-start.18 = (bf16[32,640]{1,0:T(8,128)(2,1)S(1)}, bf16[32,640]{1,0:T(8,128)(2,1)S(1)}, u32[]{:S(2)}, u32[]{:S(2)}) collective-permute-start(bf16[32,640]{1,0:T(8,128)(2,1)S(1)} %pad_maximum_fusion.5), channel_id=1, source_target_pairs={{0,64},{2,66},{4,68},{6,70},{8,72},{10,74},{12,76},{14,78},{16,80}... | collective-permute-start | bytes 122888 | tf_op jit(solution)/shard_map/ppermute | solution.py:27
  13.8 6.6 %collective-permute-start.19 = (bf16[32,640]{1,0:T(8,128)(2,1)S(1)}, bf16[32,640]{1,0:T(8,128)(2,1)S(1)}, u32[]{:S(2)}, u32[]{:S(2)}) collective-permute-start(bf16[32,640]{1,0:T(8,128)(2,1)S(1)} %pad_maximum_fusion.5), channel_id=1, source_target_pairs={{0,32},{2,34},{4,36},{6,38},{8,40},{10,42},{12,44},{14,46},{16,48}... | collective-permute-start | bytes 122888 | tf_op jit(solution)/shard_map/ppermute | solution.py:27
  16.7 6.6 %collective-permute-start = (bf16[64,640]{1,0:T(8,128)(2,1)S(1)}, bf16[64,640]{1,0:T(8,128)(2,1)S(1)}, u32[]{:S(2)}, u32[]{:S(2)}) collective-permute-start(bf16[64,640]{1,0:T(8,128)(2,1)S(1)} %maximum_maximum_fusion), channel_id=1, source_target_pairs={{0,6},{2,0},{4,2},{6,4},{8,14},{10,8},{12,10},{14,12},{16,22},{18,... | collective-permute-start | bytes 245768 | tf_op jit(solution)/shard_map/ppermute | solution.py:27
  19.3 4.9 %collective-permute-start.1 = (bf16[64,640]{1,0:T(8,128)(2,1)S(1)}, bf16[64,640]{1,0:T(8,128)(2,1)S(1)}, u32[]{:S(2)}, u32[]{:S(2)}) collective-permute-start(bf16[64,640]{1,0:T(8,128)(2,1)S(1)} %maximum_maximum_fusion), channel_id=1, source_target_pairs={{0,4},{2,6},{4,0},{6,2},{8,12},{10,14},{12,8},{14,10},{16,20},{18,... | collective-permute-start | bytes 245768 | tf_op jit(solution)/shard_map/ppermute | solution.py:27
  19.8 5.1 %collective-permute-start.2 = (bf16[64,640]{1,0:T(8,128)(2,1)S(1)}, bf16[64,640]{1,0:T(8,128)(2,1)S(1)}, u32[]{:S(2)}, u32[]{:S(2)}) collective-permute-start(bf16[64,640]{1,0:T(8,128)(2,1)S(1)} %maximum_maximum_fusion), channel_id=1, source_target_pairs={{0,2},{2,4},{4,6},{6,0},{8,10},{10,12},{12,14},{14,8},{16,18},{18,... | collective-permute-start | bytes 245768 | tf_op jit(solution)/shard_map/ppermute | solution.py:27
  20.6 5.9 %collective-permute-start.21 = (bf16[4,32,640]{2,1,0:T(8,128)(2,1)S(1)}, bf16[4,32,640]{2,1,0:T(8,128)(2,1)S(1)}, u32[]{:S(2)}, u32[]{:S(2)}) collective-permute-start(bf16[4,32,640]{2,1,0:T(8,128)(2,1)S(1)} %get-tuple-element.22), channel_id=1, source_target_pairs={{0,24},{2,26},{4,28},{6,30},{8,0},{10,2},{12,4},{14,6},{16,8},{18,... | collective-permute-start | bytes 491528 | tf_op jit(solution)/shard_map/ppermute | solution.py:27
  23.4 8.6 %collective-permute-start.20 = (bf16[4,32,640]{2,1,0:T(8,128)(2,1)S(1)}, bf16[4,32,640]{2,1,0:T(8,128)(2,1)S(1)}, u32[]{:S(2)}, u32[]{:S(2)}) collective-permute-start(bf16[4,32,640]{2,1,0:T(8,128)(2,1)S(1)} %get-tuple-element.22), channel_id=1, source_target_pairs={{0,8},{2,10},{4,12},{6,14},{8,16},{10,18},{12,20},{14,22},{16,24},... | collective-permute-start | bytes 491528 | tf_op jit(solution)/shard_map/ppermute | solution.py:27
  26.5 6.0 %collective-permute-start.22 = (bf16[4,32,640]{2,1,0:T(8,128)(2,1)S(1)}, bf16[4,32,640]{2,1,0:T(8,128)(2,1)S(1)}, u32[]{:S(2)}, u32[]{:S(2)}) collective-permute-start(bf16[4,32,640]{2,1,0:T(8,128)(2,1)S(1)} %collective-permute-done.21), channel_id=1, source_target_pairs={{0,24},{2,26},{4,28},{6,30},{8,0},{10,2},{12,4},{14,6},{16,8},{18,... | collective-permute-start | bytes 491528 | tf_op jit(solution)/shard_map/ppermute | solution.py:27
  30.0 10.5 %collective-permute-start.10 = (bf16[4,32,640]{2,1,0:T(8,128)(2,1)S(1)}, bf16[4,32,640]{2,1,0:T(8,128)(2,1)S(1)}, u32[]{:S(2)}, u32[]{:S(2)}) collective-permute-start(bf16[4,32,640]{2,1,0:T(8,128)(2,1)S(1)} %get-tuple-element.15), channel_id=1, source_target_pairs={{0,32},{2,34},{4,36},{6,38},{8,40},{10,42},{12,44},{14,46},{16,48}... | collective-permute-start | bytes 491528 | tf_op jit(solution)/shard_map/ppermute | solution.py:27
  32.0 8.5 %collective-permute-start.3 = (bf16[4,32,640]{2,1,0:T(8,128)(2,1)S(1)}, bf16[4,32,640]{2,1,0:T(8,128)(2,1)S(1)}, u32[]{:S(2)}, u32[]{:S(2)}) collective-permute-start(bf16[4,32,640]{2,1,0:T(8,128)(2,1)S(1)} %get-tuple-element.16), channel_id=1, source_target_pairs={{0,8},{2,10},{4,12},{6,14},{8,16},{10,18},{12,20},{14,22},{16,24},... | collective-permute-start | bytes 491528 | tf_op jit(solution)/shard_map/ppermute | solution.py:27
  32.6 16.7 %collective-permute-start.23 = (bf16[4,4,32,640]{3,2,1,0:T(8,128)(2,1)S(1)}, bf16[4,4,32,640]{3,2,1,0:T(8,128)(2,1)S(1)}, u32[]{:S(2)}, u32[]{:S(2)}) collective-permute-start(bf16[4,4,32,640]{3,2,1,0:T(8,128)(2,1)S(1)} %pad_maximum_fusion.2.refs_11_), channel_id=1, source_target_pairs={{0,2},{2,4},{4,6},{6,0},{8,10},{10,12},{12,14},{14,8},{16,18},{18,... | collective-permute-start | bytes 1966088 | tf_op jit(solution)/shard_map/ppermute | solution.py:27
  35.0 5.7 %collective-permute-start.12 = (bf16[4,32,640]{2,1,0:T(8,128)(2,1)S(1)}, bf16[4,32,640]{2,1,0:T(8,128)(2,1)S(1)}, u32[]{:S(2)}, u32[]{:S(2)}) collective-permute-start(bf16[4,32,640]{2,1,0:T(8,128)(2,1)S(1)} %get-tuple-element.15), channel_id=1, source_target_pairs={{0,96},{2,98},{4,100},{6,102},{8,104},{10,106},{12,108},{14,110},{... | collective-permute-start | bytes 491528 | tf_op jit(solution)/shard_map/ppermute | solution.py:27
  37.3 9.1 %collective-permute-start.5 = (bf16[4,32,640]{2,1,0:T(8,128)(2,1)S(1)}, bf16[4,32,640]{2,1,0:T(8,128)(2,1)S(1)}, u32[]{:S(2)}, u32[]{:S(2)}) collective-permute-start(bf16[4,32,640]{2,1,0:T(8,128)(2,1)S(1)} %get-tuple-element.16), channel_id=1, source_target_pairs={{0,24},{2,26},{4,28},{6,30},{8,0},{10,2},{12,4},{14,6},{16,8},{18,... | collective-permute-start | bytes 491528 | tf_op jit(solution)/shard_map/ppermute | solution.py:27
  40.5 5.7 %collective-permute-start.11 = (bf16[4,32,640]{2,1,0:T(8,128)(2,1)S(1)}, bf16[4,32,640]{2,1,0:T(8,128)(2,1)S(1)}, u32[]{:S(2)}, u32[]{:S(2)}) collective-permute-start(bf16[4,32,640]{2,1,0:T(8,128)(2,1)S(1)} %collective-permute-done.10), channel_id=1, source_target_pairs={{0,32},{2,34},{4,36},{6,38},{8,40},{10,42},{12,44},{14,46},{16,48}... | collective-permute-start | bytes 491528 | tf_op jit(solution)/shard_map/ppermute | solution.py:27
  40.5 8.5 %collective-permute-start.4 = (bf16[4,32,640]{2,1,0:T(8,128)(2,1)S(1)}, bf16[4,32,640]{2,1,0:T(8,128)(2,1)S(1)}, u32[]{:S(2)}, u32[]{:S(2)}) collective-permute-start(bf16[4,32,640]{2,1,0:T(8,128)(2,1)S(1)} %collective-permute-done.3), channel_id=1, source_target_pairs={{0,8},{2,10},{4,12},{6,14},{8,16},{10,18},{12,20},{14,22},{16,24},... | collective-permute-start | bytes 491528 | tf_op jit(solution)/shard_map/ppermute | solution.py:27
  40.6 20.2 %collective-permute-start.24 = (bf16[4,4,32,640]{3,2,1,0:T(8,128)(2,1)S(1)}, bf16[4,4,32,640]{3,2,1,0:T(8,128)(2,1)S(1)}, u32[]{:S(2)}, u32[]{:S(2)}) collective-permute-start(bf16[4,4,32,640]{3,2,1,0:T(8,128)(2,1)S(1)} %pad_maximum_fusion.2.refs_11_), channel_id=1, source_target_pairs={{0,6},{2,0},{4,2},{6,4},{8,14},{10,8},{12,10},{14,12},{16,22},{18,... | collective-permute-start | bytes 1966088 | tf_op jit(solution)/shard_map/ppermute | solution.py:27
  46.3 25.9 %collective-permute-start.13 = (bf16[4,4,32,640]{3,2,1,0:T(8,128)(2,1)S(1)}, bf16[4,4,32,640]{3,2,1,0:T(8,128)(2,1)}, u32[]{:S(2)}, u32[]{:S(2)}) collective-permute-start(bf16[4,4,32,640]{3,2,1,0:T(8,128)(2,1)S(1)} %pad_maximum_fusion.1.refs_6_), channel_id=1, source_target_pairs={{0,8},{2,10},{4,12},{6,14},{8,16},{10,18},{12,20},{14,22},{16,24},... | collective-permute-start | bytes 1966088 | tf_op jit(solution)/shard_map/ppermute | solution.py:27
  46.4 29.2 %collective-permute-start.14 = (bf16[4,4,32,640]{3,2,1,0:T(8,128)(2,1)S(1)}, bf16[4,4,32,640]{3,2,1,0:T(8,128)(2,1)}, u32[]{:S(2)}, u32[]{:S(2)}) collective-permute-start(bf16[4,4,32,640]{3,2,1,0:T(8,128)(2,1)S(1)} %pad_maximum_fusion.1.refs_6_), channel_id=1, source_target_pairs={{0,24},{2,26},{4,28},{6,30},{8,0},{10,2},{12,4},{14,6},{16,8},{18,... | collective-permute-start | bytes 1966088 | tf_op jit(solution)/shard_map/ppermute | solution.py:27
  49.2 35.1 %copy-start.19 = (bf16[1024]{0:T(1024)(128)(2,1)S(1)}, bf16[1024]{0:T(1024)(128)(2,1)}, u32[]{:S(2)}) copy-start(bf16[1024]{0:T(1024)(128)(2,1)} %param.20) | copy-start | bytes 6148
  49.2 27.5 %collective-permute-start.6 = (bf16[4,4,32,640]{3,2,1,0:T(8,128)(2,1)S(1)}, bf16[4,4,32,640]{3,2,1,0:T(8,128)(2,1)}, u32[]{:S(2)}, u32[]{:S(2)}) collective-permute-start(bf16[4,4,32,640]{3,2,1,0:T(8,128)(2,1)S(1)} %pad_maximum_fusion.refs_1_), channel_id=1, source_target_pairs={{0,32},{2,34},{4,36},{6,38},{8,40},{10,42},{12,44},{14,46},{16,48}... | collective-permute-start | bytes 1966088 | tf_op jit(solution)/shard_map/ppermute | solution.py:27
  49.3 31.2 %collective-permute-start.7 = (bf16[4,4,32,640]{3,2,1,0:T(8,128)(2,1)S(1)}, bf16[4,4,32,640]{3,2,1,0:T(8,128)(2,1)}, u32[]{:S(2)}, u32[]{:S(2)}) collective-permute-start(bf16[4,4,32,640]{3,2,1,0:T(8,128)(2,1)S(1)} %pad_maximum_fusion.refs_1_), channel_id=1, source_target_pairs={{0,96},{2,98},{4,100},{6,102},{8,104},{10,106},{12,108},{14,110},{... | collective-permute-start | bytes 1966088 | tf_op jit(solution)/shard_map/ppermute | solution.py:27
  60.8 36.8 %copy-start.7 = (bf16[4,4,32,640]{3,2,1,0:T(8,128)(2,1)}, bf16[4,4,32,640]{3,2,1,0:T(8,128)(2,1)S(1)}, u32[]{:S(2)}) copy-start(bf16[4,4,32,640]{3,2,1,0:T(8,128)(2,1)S(1)} %collective-permute-done.24.refs_13_) | copy-start | bytes 1966084
  60.8 20.8 %collective-permute-start.25 = (bf16[2,4,32,640]{3,2,1,0:T(8,128)(2,1)S(1)}, bf16[2,4,32,640]{3,2,1,0:T(8,128)(2,1)S(1)}, u32[]{:S(2)}, u32[]{:S(2)}) collective-permute-start(bf16[2,4,32,640]{3,2,1,0:T(8,128)(2,1)S(1)} %slice.51), channel_id=1, source_target_pairs={{0,2},{2,4},{4,6},{6,0},{8,10},{10,12},{12,14},{14,8},{16,18},{18,... | collective-permute-start | bytes 983048 | tf_op jit(solution)/shard_map/ppermute | solution.py:27
  72.2 13.4 %collective-permute-start.26 = (bf16[2,4,32,640]{3,2,1,0:T(8,128)(2,1)S(1)}, bf16[2,4,32,640]{3,2,1,0:T(8,128)(2,1)S(1)}, u32[]{:S(2)}, u32[]{:S(2)}) collective-permute-start(bf16[2,4,32,640]{3,2,1,0:T(8,128)(2,1)S(1)} %slice.52), channel_id=1, source_target_pairs={{0,6},{2,0},{4,2},{6,4},{8,14},{10,8},{12,10},{14,12},{16,22},{18,... | collective-permute-start | bytes 983048 | tf_op jit(solution)/shard_map/ppermute | solution.py:27
  75.6 16.3 %collective-permute-start.15 = (bf16[2,4,32,640]{3,2,1,0:T(8,128)(2,1)S(1)}, bf16[2,4,32,640]{3,2,1,0:T(8,128)(2,1)S(1)}, u32[]{:S(2)}, u32[]{:S(2)}) collective-permute-start(bf16[2,4,32,640]{3,2,1,0:T(8,128)(2,1)S(1)} %slice.48), channel_id=1, source_target_pairs={{0,8},{2,10},{4,12},{6,14},{8,16},{10,18},{12,20},{14,22},{16,24},... | collective-permute-start | bytes 983048 | tf_op jit(solution)/shard_map/ppermute | solution.py:27
  76.7 16.2 %collective-permute-start.16 = (bf16[2,4,32,640]{3,2,1,0:T(8,128)(2,1)S(1)}, bf16[2,4,32,640]{3,2,1,0:T(8,128)(2,1)S(1)}, u32[]{:S(2)}, u32[]{:S(2)}) collective-permute-start(bf16[2,4,32,640]{3,2,1,0:T(8,128)(2,1)S(1)} %slice.49), channel_id=1, source_target_pairs={{0,24},{2,26},{4,28},{6,30},{8,0},{10,2},{12,4},{14,6},{16,8},{18,... | collective-permute-start | bytes 983048 | tf_op jit(solution)/shard_map/ppermute | solution.py:27
  80.5 16.9 %collective-permute-start.8 = (bf16[2,4,32,640]{3,2,1,0:T(8,128)(2,1)S(1)}, bf16[2,4,32,640]{3,2,1,0:T(8,128)(2,1)S(1)}, u32[]{:S(2)}, u32[]{:S(2)}) collective-permute-start(bf16[2,4,32,640]{3,2,1,0:T(8,128)(2,1)S(1)} %slice.45), channel_id=1, source_target_pairs={{0,32},{2,34},{4,36},{6,38},{8,40},{10,42},{12,44},{14,46},{16,48}... | collective-permute-start | bytes 983048 | tf_op jit(solution)/shard_map/ppermute | solution.py:27
  81.6 16.0 %collective-permute-start.9 = (bf16[2,4,32,640]{3,2,1,0:T(8,128)(2,1)S(1)}, bf16[2,4,32,640]{3,2,1,0:T(8,128)(2,1)S(1)}, u32[]{:S(2)}, u32[]{:S(2)}) collective-permute-start(bf16[2,4,32,640]{3,2,1,0:T(8,128)(2,1)S(1)} %slice.46), channel_id=1, source_target_pairs={{0,96},{2,98},{4,100},{6,102},{8,104},{10,106},{12,108},{14,110},{... | collective-permute-start | bytes 983048 | tf_op jit(solution)/shard_map/ppermute | solution.py:27
  107.2 15.0 %collective-permute-start.27 = (bf16[512,2048]{1,0:T(8,128)(2,1)}, bf16[512,2048]{1,0:T(8,128)(2,1)S(1)}, u32[]{:S(2)}, u32[]{:S(2)}) collective-permute-start(bf16[512,2048]{1,0:T(8,128)(2,1)} %get-tuple-element.9), channel_id=1, source_target_pairs={{0,1},{1,0},{2,3},{3,2},{4,5},{5,4},{6,7},{7,6},{8,9},{9,8},{10,11... | collective-permute-start | bytes 6291464 | tf_op jit(solution)/shard_map/ppermute | solution.py:410
  112.0 10.2 %collective-permute-start.28 = (bf16[3,2,4,4,64,128]{5,4,3,2,1,0:T(8,128)(2,1)}, bf16[3,2,4,4,64,128]{5,4,3,2,1,0:T(8,128)(2,1)S(1)}, u32[]{:S(2)}, u32[]{:S(2)}) collective-permute-start(bf16[3,2,4,4,64,128]{5,4,3,2,1,0:T(8,128)(2,1)} %get-tuple-element.10.mine), channel_id=1, source_target_pairs={{0,1},{1,0},{2,3},{3,2},{4,5},{5,4},{6,7},{7,6},{8,9},{9,8},{10,11... | collective-permute-start | bytes 4718600 | tf_op jit(solution)/shard_map/ppermute | solution.py:411
  (20 other events, 210.5 us)
Sparse Core Ops, SparseCore 0:
  10.2 121.9 all-gather.2

commit v3 on v1

--- a/solution.py
+++ b/solution.py
@@ -90,22 +90,28 @@
         to = pl.ds(pl.multiple_of(at_z // 2 * part, part), part)
         pltpu.make_async_copy(ref.at[index], w.at[at_z % 2, at_y, :, to], sem).start()
 
-    for piece, low, inner, outer in RELAYED:
-        at_z, at_y = (z + RING - outer) % RING, (y + RING - outer) % RING
-
-        def copies(i, carry, piece=piece, low=low, outer=outer):
-            near_z, near_y = (z + RING - low - i) % RING, (y + RING - low - i) % RING
-            line(for_value[piece], i, w_value, sem_v, near_z, at_y)
-            line(for_unit[piece], i, w_unit, sem_u, at_z, near_y)
-            for r in range(2):
-                pltpu.make_async_copy(
-                    for_out[piece].at[i, pl.ds(2 * r, 2)],
-                    w_out.at[:, near_y, (x_at + RING - outer) % RING, pl.ds(r * part, part)],
-                    sem_o,
-                ).start()
-            return carry
-
-        lax.fori_loop(0, inner, copies, 0)
+    def value_copies(piece, i, near, outer):
+        line(for_value[piece], i, w_value, sem_v, (z + RING - near) % RING, (y + RING - outer) % RING)
+
+    def unit_copies(piece, i, near, outer):
+        line(for_unit[piece], i, w_unit, sem_u, (z + RING - outer) % RING, (y + RING - near) % RING)
+
+    def out_copies(piece, i, near, outer):
+        for r in range(2):
+            pltpu.make_async_copy(
+                for_out[piece].at[i, pl.ds(2 * r, 2)],
+                w_out.at[:, (y + RING - near) % RING, (x_at + RING - outer) % RING, pl.ds(r * part, part)],
+                sem_o,
+            ).start()
+
+    for start_copies in (value_copies, unit_copies, out_copies):
+        for piece, low, inner, outer in RELAYED:
+
+            def step(i, carry, piece=piece, low=low, outer=outer):
+                start_copies(piece, i, low + i, outer)
+                return carry
+
+            lax.fori_loop(0, inner, step, 0)
 
     pltpu.make_async_copy(normed_hbm.at[pl.ds(start, count)], rows, sem_x).wait()
     pltpu.make_async_copy(w_value, w_value, sem_v).wait()

time: 166 us -> 166 us (level)
  Pallas kernels: 47.6 us -> 45.1 us
  waiting for transfers between devices: 33.6 us -> 36 us
    pallas_call x2, Pallas kernels: 22.3 us -> 19.8 us  [mixer(): pl.pallas_call(functools.partial(mixer_body, own), out_shape=jax.ShapeDty...]
    all_gather x1, waiting for transfers between devices: 7.7 us -> 10.1 us  [on_device(): lax.all_gather(packed, EVERY).reshape(tps, reps, fss, *packed.shape)]
  transfers between devices with their start and end apart: 29 -> 29, of which waited for: 10 -> 10; matrix products, arithmetic and copies ran while one was open for 14% -> 15% of each run, Pallas kernels for 13% -> 12%
where the time goes in v3:
time: 166 us; the launch traced here: 165 us
  starting transfers between devices  45.7 us (28%)
  Pallas kernels  45.1 us (27%)
  waiting for transfers between devices  36 us (22%)
  other arithmetic  16.4 us (10%)
  between operations  13.7 us (8%)
  local copies, waits for them, and re-layouts  8.39 us (5%)
    ppermute x27, starting transfers between devices, shift(): return lax.ppermute(x, CHIPS, pairs)  36.9 us
    ppermute x27, waiting for transfers between devices, shift(): return lax.ppermute(x, CHIPS, pairs)  25.8 us
    pallas_call x1, Pallas kernels, ffn(): pl.pallas_call(ffn_body, out_shape=jax.ShapeDtypeStruct(h_mid.shape, BF16...  23.5 us
    pallas_call x2, Pallas kernels, mixer(): pl.pallas_call(functools.partial(mixer_body, own), out_shape=jax.ShapeDty...  19.8 us
    all_gather x1, waiting for transfers between devices, on_device(): lax.all_gather(packed, EVERY).reshape(tps, reps, fss, *packed.shape)  10.1 us
    ppermute x1, starting transfers between devices, on_device(): lax.ppermute(other, 'tp', [(i, (i + 1) % tps) for i in range(tps)])  8.86 us
    reduce_sum x2, other arithmetic, rms_scale(): scale = lax.rsqrt(jnp.mean(values * values, axis=-1, keepdims=True) + 1e-06)  7.38 us
    slice x3, local copies, waits for them, and re-layouts, relayed_ring(): ahead[half:]  3.43 us
  transfers between devices with their start and end apart: 29, of which 10 were waited for; matrix products, arithmetic and copies ran while one was open for 15% of the time, Pallas kernels for 12%

profile of v3, /device:TPU:1, one launch (start us, length us, event | category | flops | bytes accessed | tf_op | source)
XLA Modules:
  0.0 165.4 jit_solution(1437313445548711177)
XLA Ops:
  6.5 1.8 %pack.1 = bf16[96,1408]{1,0:T(8,128)(2,1)} custom-call(bf16[64,1408]{1,0:T(8,128)(2,1)} %gate.1, bf16[64,1408]{1,0:T(8,128)(2,1)} %up.1, bf16[64,1408]{1,0:T(8,128)(2,1)} %bitcast.42), custom_call_target="tpu_custom_call" | custom-call | tf_op jit(solution)/shard_map/pack/pallas_call | solution.py:275
  9.2 4.6 %collective-permute-start.17 = (bf16[32,512]{1,0:T(8,128)(2,1)S(1)}, bf16[32,512]{1,0:T(8,128)(2,1)S(1)}, u32[]{:S(2)}, u32[]{:S(2)}) collective-permute-start(bf16[32,512]{1,0:T(8,128)(2,1)S(1)} %dynamic-slice_bitcast_fusion), channel_id=1, source_target_pairs={{0,96},{2,98},{4,100},{6,102},{8,104},{10,106},{12,108},{14,110},{... | collective-permute-start | bytes 98312 | tf_op jit(solution)/shard_map/ppermute | solution.py:27
  15.3 2.5 %collective-permute-start = (bf16[64,512]{1,0:T(8,128)(2,1)S(1)}, bf16[64,512]{1,0:T(8,128)(2,1)S(1)}, u32[]{:S(2)}, u32[]{:S(2)}) collective-permute-start(bf16[64,512]{1,0:T(8,128)(2,1)S(1)} %pad_maximum_fusion.5), channel_id=1, source_target_pairs={{0,6},{2,0},{4,2},{6,4},{8,14},{10,8},{12,10},{14,12},{16,22},{18,... | collective-permute-start | bytes 196616 | tf_op jit(solution)/shard_map/ppermute | solution.py:27
  19.8 2.8 %collective-permute-start.21 = (bf16[4,32,512]{2,1,0:T(8,128)(2,1)S(1)}, bf16[4,32,512]{2,1,0:T(8,128)(2,1)S(1)}, u32[]{:S(2)}, u32[]{:S(2)}) collective-permute-start(bf16[4,32,512]{2,1,0:T(8,128)(2,1)S(1)} %get-tuple-element.15), channel_id=1, source_target_pairs={{0,24},{2,26},{4,28},{6,30},{8,0},{10,2},{12,4},{14,6},{16,8},{18,... | collective-permute-start | bytes 393224 | tf_op jit(solution)/shard_map/ppermute | solution.py:27
  23.3 1.2 collective-permute-done.21
  24.5 3.4 %collective-permute-start.22 = (bf16[4,32,512]{2,1,0:T(8,128)(2,1)S(1)}, bf16[4,32,512]{2,1,0:T(8,128)(2,1)S(1)}, u32[]{:S(2)}, u32[]{:S(2)}) collective-permute-start(bf16[4,32,512]{2,1,0:T(8,128)(2,1)S(1)} %collective-permute-done.21), channel_id=1, source_target_pairs={{0,24},{2,26},{4,28},{6,30},{8,0},{10,2},{12,4},{14,6},{16,8},{18,... | collective-permute-start | bytes 393224 | tf_op jit(solution)/shard_map/ppermute | solution.py:27
  28.0 2.0 %collective-permute-start.10 = (bf16[4,32,512]{2,1,0:T(8,128)(2,1)S(1)}, bf16[4,32,512]{2,1,0:T(8,128)(2,1)S(1)}, u32[]{:S(2)}, u32[]{:S(2)}) collective-permute-start(bf16[4,32,512]{2,1,0:T(8,128)(2,1)S(1)} %get-tuple-element.9), channel_id=1, source_target_pairs={{0,32},{2,34},{4,36},{6,38},{8,40},{10,42},{12,44},{14,46},{16,48}... | collective-permute-start | bytes 393224 | tf_op jit(solution)/shard_map/ppermute | solution.py:27
  30.3 2.0 %collective-permute-start.23 = (bf16[4,4,32,512]{3,2,1,0:T(8,128)(2,1)S(1)}, bf16[4,4,32,512]{3,2,1,0:T(8,128)(2,1)S(1)}, u32[]{:S(2)}, u32[]{:S(2)}) collective-permute-start(bf16[4,4,32,512]{3,2,1,0:T(8,128)(2,1)S(1)} %pad_maximum_fusion.2.refs_11_), channel_id=1, source_target_pairs={{0,2},{2,4},{4,6},{6,0},{8,10},{10,12},{12,14},{14,8},{16,18},{18,... | collective-permute-start | bytes 1572872 | tf_op jit(solution)/shard_map/ppermute | solution.py:27
  32.3 3.1 %fusion = f32[1024]{0:T(1024)S(1)} fusion(bf16[1024,2048]{1,0:T(8,128)(2,1)} %param.13), kind=kLoop, calls=%fused_computation.2 | loop fusion | flops 6290432 | bytes 4198400 | tf_op jit(solution)/shard_map/reduce_sum | solution.py:62
  35.4 1.1 collective-permute-start.12
  36.5 3.2 %collective-permute-start.5 = (bf16[4,32,512]{2,1,0:T(8,128)(2,1)S(1)}, bf16[4,32,512]{2,1,0:T(8,128)(2,1)S(1)}, u32[]{:S(2)}, u32[]{:S(2)}) collective-permute-start(bf16[4,32,512]{2,1,0:T(8,128)(2,1)S(1)} %get-tuple-element.10), channel_id=1, source_target_pairs={{0,24},{2,26},{4,28},{6,30},{8,0},{10,2},{12,4},{14,6},{16,8},{18,... | collective-permute-start | bytes 393224 | tf_op jit(solution)/shard_map/ppermute | solution.py:27
  39.7 1.5 collective-permute-start.11
  41.3 1.1 collective-permute-start.24
  42.3 2.7 %collective-permute-done.11 = bf16[4,32,512]{2,1,0:T(8,128)(2,1)S(1)} collective-permute-done((bf16[4,32,512]{2,1,0:T(8,128)(2,1)S(1)}, bf16[4,32,512]{2,1,0:T(8,128)(2,1)S(1)}, u32[]{:S(2)}, u32[]{:S(2)}) %collective-permute-start.11) | collective-permute-done | bytes 131104 | tf_op jit(solution)/shard_map/ppermute | solution.py:27
  45.2 2.7 %collective-permute-start.14 = (bf16[4,4,32,512]{3,2,1,0:T(8,128)(2,1)S(1)}, bf16[4,4,32,512]{3,2,1,0:T(8,128)(2,1)}, u32[]{:S(2)}, u32[]{:S(2)}) collective-permute-start(bf16[4,4,32,512]{3,2,1,0:T(8,128)(2,1)S(1)} %pad_maximum_fusion.1.refs_6_), channel_id=1, source_target_pairs={{0,24},{2,26},{4,28},{6,30},{8,0},{10,2},{12,4},{14,6},{16,8},{18,... | collective-permute-start | bytes 1572872 | tf_op jit(solution)/shard_map/ppermute | solution.py:27
  48.3 2.4 %collective-permute-start.7 = (bf16[4,4,32,512]{3,2,1,0:T(8,128)(2,1)S(1)}, bf16[4,4,32,512]{3,2,1,0:T(8,128)(2,1)}, u32[]{:S(2)}, u32[]{:S(2)}) collective-permute-start(bf16[4,4,32,512]{3,2,1,0:T(8,128)(2,1)S(1)} %pad_maximum_fusion.refs_1_), channel_id=1, source_target_pairs={{0,96},{2,98},{4,100},{6,102},{8,104},{10,106},{12,108},{14,110},{... | collective-permute-start | bytes 1572872 | tf_op jit(solution)/shard_map/ppermute | solution.py:27
  50.7 3.0 %fusion.2.refs_0_ = bf16[1024,2048]{1,0:T(8,128)(2,1)} fusion(bf16[1024,2048]{1,0:T(8,128)(2,1)S(1)} %copy-done.2, f32[2048]{0:T(1024)S(1)} %convert_element_type.34, f32[1024]{0:T(1024)S(1)} %add_rsqrt_fusion), kind=kLoop, calls=%fused_computation.4 | loop fusion | flops 8388608 | bytes 8400896 | tf_op jit(solution)/shard_map/convert_element_type | solution.py:315
  53.7 3.3 %collective-permute-done.24.refs_13_ = bf16[4,4,32,512]{3,2,1,0:T(8,128)(2,1)S(1)} collective-permute-done((bf16[4,4,32,512]{3,2,1,0:T(8,128)(2,1)S(1)}, bf16[4,4,32,512]{3,2,1,0:T(8,128)(2,1)S(1)}, u32[]{:S(2)}, u32[]{:S(2)}) %collective-permute-start.24) | collective-permute-done | bytes 524320 | tf_op jit(solution)/shard_map/ppermute | solution.py:27
  57.8 1.5 dynamic-slice_select_fusion.refs_16_
  60.0 9.3 %collective-permute-done.13.refs_7_ = bf16[4,4,32,512]{3,2,1,0:T(8,128)(2,1)S(1)} collective-permute-done((bf16[4,4,32,512]{3,2,1,0:T(8,128)(2,1)S(1)}, bf16[4,4,32,512]{3,2,1,0:T(8,128)(2,1)S(1)}, u32[]{:S(2)}, u32[]{:S(2)}) %collective-permute-start.13) | collective-permute-done | bytes 524320 | tf_op jit(solution)/shard_map/ppermute | solution.py:27
  70.1 1.7 slice.37
  71.8 2.7 %collective-permute-start.16 = (bf16[2,4,32,512]{3,2,1,0:T(8,128)(2,1)}, bf16[2,4,32,512]{3,2,1,0:T(8,128)(2,1)S(1)}, u32[]{:S(2)}, u32[]{:S(2)}) collective-permute-start(bf16[2,4,32,512]{3,2,1,0:T(8,128)(2,1)} %slice.37), channel_id=1, source_target_pairs={{0,24},{2,26},{4,28},{6,30},{8,0},{10,2},{12,4},{14,6},{16,8},{18,... | collective-permute-start | bytes 786440 | tf_op jit(solution)/shard_map/ppermute | solution.py:27
  74.4 1.7 %slice.33 = bf16[2,4,32,512]{3,2,1,0:T(8,128)(2,1)} slice(bf16[4,4,32,512]{3,2,1,0:T(8,128)(2,1)} %collective-permute-done.6.refs_2_), slice={[0:2], [0:4], [0:32], [0:512]} | slice | bytes 524288 | tf_op jit(solution)/shard_map/slice | solution.py:43
  77.5 2.4 %collective-permute-start.9 = (bf16[2,4,32,512]{3,2,1,0:T(8,128)(2,1)S(1)}, bf16[2,4,32,512]{3,2,1,0:T(8,128)(2,1)S(1)}, u32[]{:S(2)}, u32[]{:S(2)}) collective-permute-start(bf16[2,4,32,512]{3,2,1,0:T(8,128)(2,1)S(1)} %slice.34), channel_id=1, source_target_pairs={{0,96},{2,98},{4,100},{6,102},{8,104},{10,106},{12,108},{14,110},{... | collective-permute-start | bytes 786440 | tf_op jit(solution)/shard_map/ppermute | solution.py:27
  81.1 7.8 %collective-permute-done.8.refs_4_ = bf16[2,4,32,512]{3,2,1,0:T(8,128)(2,1)S(1)} collective-permute-done((bf16[2,4,32,512]{3,2,1,0:T(8,128)(2,1)}, bf16[2,4,32,512]{3,2,1,0:T(8,128)(2,1)S(1)}, u32[]{:S(2)}, u32[]{:S(2)}) %collective-permute-start.8) | collective-permute-done | bytes 262176 | tf_op jit(solution)/shard_map/ppermute | solution.py:27
  90.0 9.2 %mixer_other.1 = bf16[512,2048]{1,0:T(8,128)(2,1)} custom-call(bf16[1024,2048]{1,0:T(8,128)(2,1)} %fusion.2.refs_0_, bf16[4,4,32,512]{3,2,1,0:T(8,128)(2,1)} %copy-done.7, bf16[4,4,32,512]{3,2,1,0:T(8,128)(2,1)} %collective-permute-done.6.refs_2_, bf16[4,4,32,512]{3,2,1,0:T(8,128)(2,1)} %collective-permute-done.7.refs_3_, ...), custom_call_target="tpu_custom_call" | custom-call | tf_op jit(solution)/shard_map/mixer_other/pallas_call | solution.py:145
  99.2 8.9 %collective-permute-start.27 = (bf16[512,2048]{1,0:T(8,128)(2,1)}, bf16[512,2048]{1,0:T(8,128)(2,1)}, u32[]{:S(2)}, u32[]{:S(2)}) collective-permute-start(bf16[512,2048]{1,0:T(8,128)(2,1)} %mixer_other.1), channel_id=1, source_target_pairs={{0,1},{1,0},{2,3},{3,2},{4,5},{5,4},{6,7},{7,6},{8,9},{9,8},{10,11... | collective-permute-start | bytes 6291464 | tf_op jit(solution)/shard_map/ppermute | solution.py:322
  108.0 10.6 %mixer_own.1 = f32[512,2048]{1,0:T(8,128)} custom-call(bf16[1024,2048]{1,0:T(8,128)(2,1)} %fusion.2.refs_0_, bf16[4,4,32,512]{3,2,1,0:T(8,128)(2,1)} %copy-done.7, bf16[4,4,32,512]{3,2,1,0:T(8,128)(2,1)} %collective-permute-done.6.refs_2_, bf16[4,4,32,512]{3,2,1,0:T(8,128)(2,1)} %collective-permute-done.7.refs_3_, bf16[2,4,32,512]{3,2,1,0:T(8,128)(2,1)} %copy-done.15, ...), custom_call_target="tpu_custom_call" | custom-call | tf_op jit(solution)/shard_map/mixer_own/pallas_call | solution.py:145
  118.6 4.3 %fusion.3 = (f32[512]{0:T(512)S(1)}, bf16[512,2048]{1,0:T(8,128)(2,1)S(1)}) fusion(f32[512,2048]{1,0:T(8,128)} %mixer_own.1, bf16[512,2048]{1,0:T(8,128)(2,1)} %collective-permute-done.27, bf16[1024,2048]{1,0:T(8,128)(2,1)S(1)} %copy-done.3, s32[]{:T(128)S(6)} %select_n.211), kind=kLoop, calls=%fused_computation.7 | loop fusion | flops 8388096 | bytes 10487812 | tf_op jit(solution)/shard_map/reduce_sum | solution.py:62
  122.9 2.0 %fusion.5.n_hbm = bf16[512,2048]{1,0:T(8,128)(2,1)} fusion(bf16[512,2048]{1,0:T(8,128)(2,1)S(1)} %get-tuple-element.6.h_hbm, f32[2048]{0:T(1024)S(1)} %convert_element_type.39, f32[512]{0:T(512)S(1)} %add_rsqrt_fusion.1), kind=kLoop, calls=%fused_computation.9 | loop fusion | flops 4194304 | bytes 4204544 | tf_op jit(solution)/shard_map/convert_element_type | solution.py:326
  124.9 10.1 %all-gather.3.cloned.1.call-done = bf16[12288,1408]{1,0:T(8,128)(2,1)} async-done(((bf16[96,1408]{1,0:T(8,128)(2,1)}), bf16[12288,1408]{1,0:T(8,128)(2,1)}) %all-gather.3.cloned.1.call-update) | async-done | bytes 34603024 | tf_op jit(solution)/shard_map/all_gather | solution.py:299
  135.0 23.5 %ffn.1 = bf16[512,2048]{1,0:T(8,128)(2,1)} custom-call(bf16[512,2048]{1,0:T(8,128)(2,1)} %copy-done.4, bf16[512,2048]{1,0:T(8,128)(2,1)} %fusion.5.n_hbm, bf16[2,2,32,96,1408]{4,3,2,1,0:T(8,128)(2,1)} %bitcast.41), custom_call_target="tpu_custom_call" | custom-call | tf_op jit(solution)/shard_map/ffn/pallas_call | solution.py:249
  (105 shorter events, 11.9 us)
Async XLA Ops:
  6.5 73.4 %copy-start = (bf16[4,128]{1,0:T(4,128)(2,1)S(1)}, bf16[4,128]{1,0:T(4,128)(2,1)}, u32[]{:S(2)}) copy-start(bf16[4,128]{1,0:T(4,128)(2,1)} %param.18) | copy-start | bytes 3076
  6.5 128.5 %all-gather.3.cloned.1.call-start = ((), (), s32[]{:S(2)}) async-start(), calls=%async_computation | async-start | bytes 34873344 | tf_op jit(solution)/shard_map/all_gather | solution.py:299
  9.2 9.1 %collective-permute-start.17 = (bf16[32,512]{1,0:T(8,128)(2,1)S(1)}, bf16[32,512]{1,0:T(8,128)(2,1)S(1)}, u32[]{:S(2)}, u32[]{:S(2)}) collective-permute-start(bf16[32,512]{1,0:T(8,128)(2,1)S(1)} %dynamic-slice_bitcast_fusion), channel_id=1, source_target_pairs={{0,96},{2,98},{4,100},{6,102},{8,104},{10,106},{12,108},{14,110},{... | collective-permute-start | bytes 98312 | tf_op jit(solution)/shard_map/ppermute | solution.py:27
  13.8 5.2 %collective-permute-start.18 = (bf16[32,512]{1,0:T(8,128)(2,1)S(1)}, bf16[32,512]{1,0:T(8,128)(2,1)S(1)}, u32[]{:S(2)}, u32[]{:S(2)}) collective-permute-start(bf16[32,512]{1,0:T(8,128)(2,1)S(1)} %dynamic-slice_bitcast_fusion), channel_id=1, source_target_pairs={{0,64},{2,66},{4,68},{6,70},{8,72},{10,74},{12,76},{14,78},{16,80}... | collective-permute-start | bytes 98312 | tf_op jit(solution)/shard_map/ppermute | solution.py:27
  13.8 5.2 %collective-permute-start.19 = (bf16[32,512]{1,0:T(8,128)(2,1)S(1)}, bf16[32,512]{1,0:T(8,128)(2,1)S(1)}, u32[]{:S(2)}, u32[]{:S(2)}) collective-permute-start(bf16[32,512]{1,0:T(8,128)(2,1)S(1)} %dynamic-slice_bitcast_fusion), channel_id=1, source_target_pairs={{0,32},{2,34},{4,36},{6,38},{8,40},{10,42},{12,44},{14,46},{16,48}... | collective-permute-start | bytes 98312 | tf_op jit(solution)/shard_map/ppermute | solution.py:27
  15.3 7.3 %collective-permute-start = (bf16[64,512]{1,0:T(8,128)(2,1)S(1)}, bf16[64,512]{1,0:T(8,128)(2,1)S(1)}, u32[]{:S(2)}, u32[]{:S(2)}) collective-permute-start(bf16[64,512]{1,0:T(8,128)(2,1)S(1)} %pad_maximum_fusion.5), channel_id=1, source_target_pairs={{0,6},{2,0},{4,2},{6,4},{8,14},{10,8},{12,10},{14,12},{16,22},{18,... | collective-permute-start | bytes 196616 | tf_op jit(solution)/shard_map/ppermute | solution.py:27
  17.8 4.8 %collective-permute-start.1 = (bf16[64,512]{1,0:T(8,128)(2,1)S(1)}, bf16[64,512]{1,0:T(8,128)(2,1)S(1)}, u32[]{:S(2)}, u32[]{:S(2)}) collective-permute-start(bf16[64,512]{1,0:T(8,128)(2,1)S(1)} %pad_maximum_fusion.5), channel_id=1, source_target_pairs={{0,4},{2,6},{4,0},{6,2},{8,12},{10,14},{12,8},{14,10},{16,20},{18,... | collective-permute-start | bytes 196616 | tf_op jit(solution)/shard_map/ppermute | solution.py:27
  18.3 4.8 %collective-permute-start.2 = (bf16[64,512]{1,0:T(8,128)(2,1)S(1)}, bf16[64,512]{1,0:T(8,128)(2,1)S(1)}, u32[]{:S(2)}, u32[]{:S(2)}) collective-permute-start(bf16[64,512]{1,0:T(8,128)(2,1)S(1)} %pad_maximum_fusion.5), channel_id=1, source_target_pairs={{0,2},{2,4},{4,6},{6,0},{8,10},{10,12},{12,14},{14,8},{16,18},{18,... | collective-permute-start | bytes 196616 | tf_op jit(solution)/shard_map/ppermute | solution.py:27
  19.8 4.8 %collective-permute-start.21 = (bf16[4,32,512]{2,1,0:T(8,128)(2,1)S(1)}, bf16[4,32,512]{2,1,0:T(8,128)(2,1)S(1)}, u32[]{:S(2)}, u32[]{:S(2)}) collective-permute-start(bf16[4,32,512]{2,1,0:T(8,128)(2,1)S(1)} %get-tuple-element.15), channel_id=1, source_target_pairs={{0,24},{2,26},{4,28},{6,30},{8,0},{10,2},{12,4},{14,6},{16,8},{18,... | collective-permute-start | bytes 393224 | tf_op jit(solution)/shard_map/ppermute | solution.py:27
  22.6 7.4 %collective-permute-start.20 = (bf16[4,32,512]{2,1,0:T(8,128)(2,1)S(1)}, bf16[4,32,512]{2,1,0:T(8,128)(2,1)S(1)}, u32[]{:S(2)}, u32[]{:S(2)}) collective-permute-start(bf16[4,32,512]{2,1,0:T(8,128)(2,1)S(1)} %get-tuple-element.15), channel_id=1, source_target_pairs={{0,8},{2,10},{4,12},{6,14},{8,16},{10,18},{12,20},{14,22},{16,24},... | collective-permute-start | bytes 393224 | tf_op jit(solution)/shard_map/ppermute | solution.py:27
  23.3 27.4 %copy-start.2 = (bf16[1024,2048]{1,0:T(8,128)(2,1)S(1)}, bf16[1024,2048]{1,0:T(8,128)(2,1)}, u32[]{:S(2)}) copy-start(bf16[1024,2048]{1,0:T(8,128)(2,1)} %param.13) | copy-start | bytes 12582916
  24.5 5.7 %collective-permute-start.22 = (bf16[4,32,512]{2,1,0:T(8,128)(2,1)S(1)}, bf16[4,32,512]{2,1,0:T(8,128)(2,1)S(1)}, u32[]{:S(2)}, u32[]{:S(2)}) collective-permute-start(bf16[4,32,512]{2,1,0:T(8,128)(2,1)S(1)} %collective-permute-done.21), channel_id=1, source_target_pairs={{0,24},{2,26},{4,28},{6,30},{8,0},{10,2},{12,4},{14,6},{16,8},{18,... | collective-permute-start | bytes 393224 | tf_op jit(solution)/shard_map/ppermute | solution.py:27
  28.0 11.7 %collective-permute-start.10 = (bf16[4,32,512]{2,1,0:T(8,128)(2,1)S(1)}, bf16[4,32,512]{2,1,0:T(8,128)(2,1)S(1)}, u32[]{:S(2)}, u32[]{:S(2)}) collective-permute-start(bf16[4,32,512]{2,1,0:T(8,128)(2,1)S(1)} %get-tuple-element.9), channel_id=1, source_target_pairs={{0,32},{2,34},{4,36},{6,38},{8,40},{10,42},{12,44},{14,46},{16,48}... | collective-permute-start | bytes 393224 | tf_op jit(solution)/shard_map/ppermute | solution.py:27
  30.0 11.2 %collective-permute-start.3 = (bf16[4,32,512]{2,1,0:T(8,128)(2,1)S(1)}, bf16[4,32,512]{2,1,0:T(8,128)(2,1)S(1)}, u32[]{:S(2)}, u32[]{:S(2)}) collective-permute-start(bf16[4,32,512]{2,1,0:T(8,128)(2,1)S(1)} %get-tuple-element.10), channel_id=1, source_target_pairs={{0,8},{2,10},{4,12},{6,14},{8,16},{10,18},{12,20},{14,22},{16,24},... | collective-permute-start | bytes 393224 | tf_op jit(solution)/shard_map/ppermute | solution.py:27
  30.3 18.0 %collective-permute-start.23 = (bf16[4,4,32,512]{3,2,1,0:T(8,128)(2,1)S(1)}, bf16[4,4,32,512]{3,2,1,0:T(8,128)(2,1)S(1)}, u32[]{:S(2)}, u32[]{:S(2)}) collective-permute-start(bf16[4,4,32,512]{3,2,1,0:T(8,128)(2,1)S(1)} %pad_maximum_fusion.2.refs_11_), channel_id=1, source_target_pairs={{0,2},{2,4},{4,6},{6,0},{8,10},{10,12},{12,14},{14,8},{16,18},{18,... | collective-permute-start | bytes 1572872 | tf_op jit(solution)/shard_map/ppermute | solution.py:27
  35.4 5.8 %collective-permute-start.12 = (bf16[4,32,512]{2,1,0:T(8,128)(2,1)S(1)}, bf16[4,32,512]{2,1,0:T(8,128)(2,1)S(1)}, u32[]{:S(2)}, u32[]{:S(2)}) collective-permute-start(bf16[4,32,512]{2,1,0:T(8,128)(2,1)S(1)} %get-tuple-element.9), channel_id=1, source_target_pairs={{0,96},{2,98},{4,100},{6,102},{8,104},{10,106},{12,108},{14,110},{... | collective-permute-start | bytes 393224 | tf_op jit(solution)/shard_map/ppermute | solution.py:27
  36.5 8.7 %collective-permute-start.5 = (bf16[4,32,512]{2,1,0:T(8,128)(2,1)S(1)}, bf16[4,32,512]{2,1,0:T(8,128)(2,1)S(1)}, u32[]{:S(2)}, u32[]{:S(2)}) collective-permute-start(bf16[4,32,512]{2,1,0:T(8,128)(2,1)S(1)} %get-tuple-element.10), channel_id=1, source_target_pairs={{0,24},{2,26},{4,28},{6,30},{8,0},{10,2},{12,4},{14,6},{16,8},{18,... | collective-permute-start | bytes 393224 | tf_op jit(solution)/shard_map/ppermute | solution.py:27
  39.7 5.3 %collective-permute-start.11 = (bf16[4,32,512]{2,1,0:T(8,128)(2,1)S(1)}, bf16[4,32,512]{2,1,0:T(8,128)(2,1)S(1)}, u32[]{:S(2)}, u32[]{:S(2)}) collective-permute-start(bf16[4,32,512]{2,1,0:T(8,128)(2,1)S(1)} %collective-permute-done.10), channel_id=1, source_target_pairs={{0,32},{2,34},{4,36},{6,38},{8,40},{10,42},{12,44},{14,46},{16,48}... | collective-permute-start | bytes 393224 | tf_op jit(solution)/shard_map/ppermute | solution.py:27
  41.2 6.6 %collective-permute-start.4 = (bf16[4,32,512]{2,1,0:T(8,128)(2,1)S(1)}, bf16[4,32,512]{2,1,0:T(8,128)(2,1)S(1)}, u32[]{:S(2)}, u32[]{:S(2)}) collective-permute-start(bf16[4,32,512]{2,1,0:T(8,128)(2,1)S(1)} %collective-permute-done.3), channel_id=1, source_target_pairs={{0,8},{2,10},{4,12},{6,14},{8,16},{10,18},{12,20},{14,22},{16,24},... | collective-permute-start | bytes 393224 | tf_op jit(solution)/shard_map/ppermute | solution.py:27
  41.3 15.8 %collective-permute-start.24 = (bf16[4,4,32,512]{3,2,1,0:T(8,128)(2,1)S(1)}, bf16[4,4,32,512]{3,2,1,0:T(8,128)(2,1)S(1)}, u32[]{:S(2)}, u32[]{:S(2)}) collective-permute-start(bf16[4,4,32,512]{3,2,1,0:T(8,128)(2,1)S(1)} %pad_maximum_fusion.2.refs_11_), channel_id=1, source_target_pairs={{0,6},{2,0},{4,2},{6,4},{8,14},{10,8},{12,10},{14,12},{16,22},{18,... | collective-permute-start | bytes 1572872 | tf_op jit(solution)/shard_map/ppermute | solution.py:27
  45.1 24.2 %collective-permute-start.13 = (bf16[4,4,32,512]{3,2,1,0:T(8,128)(2,1)S(1)}, bf16[4,4,32,512]{3,2,1,0:T(8,128)(2,1)S(1)}, u32[]{:S(2)}, u32[]{:S(2)}) collective-permute-start(bf16[4,4,32,512]{3,2,1,0:T(8,128)(2,1)S(1)} %pad_maximum_fusion.1.refs_6_), channel_id=1, source_target_pairs={{0,8},{2,10},{4,12},{6,14},{8,16},{10,18},{12,20},{14,22},{16,24},... | collective-permute-start | bytes 1572872 | tf_op jit(solution)/shard_map/ppermute | solution.py:27
  45.2 24.9 %collective-permute-start.14 = (bf16[4,4,32,512]{3,2,1,0:T(8,128)(2,1)S(1)}, bf16[4,4,32,512]{3,2,1,0:T(8,128)(2,1)}, u32[]{:S(2)}, u32[]{:S(2)}) collective-permute-start(bf16[4,4,32,512]{3,2,1,0:T(8,128)(2,1)S(1)} %pad_maximum_fusion.1.refs_6_), channel_id=1, source_target_pairs={{0,24},{2,26},{4,28},{6,30},{8,0},{10,2},{12,4},{14,6},{16,8},{18,... | collective-permute-start | bytes 1572872 | tf_op jit(solution)/shard_map/ppermute | solution.py:27
  48.0 23.8 %collective-permute-start.6 = (bf16[4,4,32,512]{3,2,1,0:T(8,128)(2,1)S(1)}, bf16[4,4,32,512]{3,2,1,0:T(8,128)(2,1)}, u32[]{:S(2)}, u32[]{:S(2)}) collective-permute-start(bf16[4,4,32,512]{3,2,1,0:T(8,128)(2,1)S(1)} %pad_maximum_fusion.refs_1_), channel_id=1, source_target_pairs={{0,32},{2,34},{4,36},{6,38},{8,40},{10,42},{12,44},{14,46},{16,48}... | collective-permute-start | bytes 1572872 | tf_op jit(solution)/shard_map/ppermute | solution.py:27
  48.3 27.8 %collective-permute-start.7 = (bf16[4,4,32,512]{3,2,1,0:T(8,128)(2,1)S(1)}, bf16[4,4,32,512]{3,2,1,0:T(8,128)(2,1)}, u32[]{:S(2)}, u32[]{:S(2)}) collective-permute-start(bf16[4,4,32,512]{3,2,1,0:T(8,128)(2,1)S(1)} %pad_maximum_fusion.refs_1_), channel_id=1, source_target_pairs={{0,96},{2,98},{4,100},{6,102},{8,104},{10,106},{12,108},{14,110},{... | collective-permute-start | bytes 1572872 | tf_op jit(solution)/shard_map/ppermute | solution.py:27
  57.0 32.2 %copy-start.9 = (bf16[4,4,32,512]{3,2,1,0:T(8,128)(2,1)}, bf16[4,4,32,512]{3,2,1,0:T(8,128)(2,1)S(1)}, u32[]{:S(2)}) copy-start(bf16[4,4,32,512]{3,2,1,0:T(8,128)(2,1)S(1)} %collective-permute-done.24.refs_13_) | copy-start | bytes 1572868
  57.0 20.4 %collective-permute-start.25 = (bf16[2,4,32,512]{3,2,1,0:T(8,128)(2,1)S(1)}, bf16[2,4,32,512]{3,2,1,0:T(8,128)(2,1)S(1)}, u32[]{:S(2)}, u32[]{:S(2)}) collective-permute-start(bf16[2,4,32,512]{3,2,1,0:T(8,128)(2,1)S(1)} %slice.38), channel_id=1, source_target_pairs={{0,2},{2,4},{4,6},{6,0},{8,10},{10,12},{12,14},{14,8},{16,18},{18,... | collective-permute-start | bytes 786440 | tf_op jit(solution)/shard_map/ppermute | solution.py:27
  69.3 11.4 %collective-permute-start.26 = (bf16[2,4,32,512]{3,2,1,0:T(8,128)(2,1)}, bf16[2,4,32,512]{3,2,1,0:T(8,128)(2,1)S(1)}, u32[]{:S(2)}, u32[]{:S(2)}) collective-permute-start(bf16[2,4,32,512]{3,2,1,0:T(8,128)(2,1)} %slice.39), channel_id=1, source_target_pairs={{0,6},{2,0},{4,2},{6,4},{8,14},{10,8},{12,10},{14,12},{16,22},{18,... | collective-permute-start | bytes 786440 | tf_op jit(solution)/shard_map/ppermute | solution.py:27
  70.1 10.6 %collective-permute-start.15 = (bf16[2,4,32,512]{3,2,1,0:T(8,128)(2,1)}, bf16[2,4,32,512]{3,2,1,0:T(8,128)(2,1)S(1)}, u32[]{:S(2)}, u32[]{:S(2)}) collective-permute-start(bf16[2,4,32,512]{3,2,1,0:T(8,128)(2,1)} %slice.36), channel_id=1, source_target_pairs={{0,8},{2,10},{4,12},{6,14},{8,16},{10,18},{12,20},{14,22},{16,24},... | collective-permute-start | bytes 786440 | tf_op jit(solution)/shard_map/ppermute | solution.py:27
  71.8 9.4 %collective-permute-start.16 = (bf16[2,4,32,512]{3,2,1,0:T(8,128)(2,1)}, bf16[2,4,32,512]{3,2,1,0:T(8,128)(2,1)S(1)}, u32[]{:S(2)}, u32[]{:S(2)}) collective-permute-start(bf16[2,4,32,512]{3,2,1,0:T(8,128)(2,1)} %slice.37), channel_id=1, source_target_pairs={{0,24},{2,26},{4,28},{6,30},{8,0},{10,2},{12,4},{14,6},{16,8},{18,... | collective-permute-start | bytes 786440 | tf_op jit(solution)/shard_map/ppermute | solution.py:27
  76.1 12.8 %collective-permute-start.8 = (bf16[2,4,32,512]{3,2,1,0:T(8,128)(2,1)}, bf16[2,4,32,512]{3,2,1,0:T(8,128)(2,1)S(1)}, u32[]{:S(2)}, u32[]{:S(2)}) collective-permute-start(bf16[2,4,32,512]{3,2,1,0:T(8,128)(2,1)} %slice.33), channel_id=1, source_target_pairs={{0,32},{2,34},{4,36},{6,38},{8,40},{10,42},{12,44},{14,46},{16,48}... | collective-permute-start | bytes 786440 | tf_op jit(solution)/shard_map/ppermute | solution.py:27
  77.5 11.8 %collective-permute-start.9 = (bf16[2,4,32,512]{3,2,1,0:T(8,128)(2,1)S(1)}, bf16[2,4,32,512]{3,2,1,0:T(8,128)(2,1)S(1)}, u32[]{:S(2)}, u32[]{:S(2)}) collective-permute-start(bf16[2,4,32,512]{3,2,1,0:T(8,128)(2,1)S(1)} %slice.34), channel_id=1, source_target_pairs={{0,96},{2,98},{4,100},{6,102},{8,104},{10,106},{12,108},{14,110},{... | collective-permute-start | bytes 786440 | tf_op jit(solution)/shard_map/ppermute | solution.py:27
  99.2 19.4 %collective-permute-start.27 = (bf16[512,2048]{1,0:T(8,128)(2,1)}, bf16[512,2048]{1,0:T(8,128)(2,1)}, u32[]{:S(2)}, u32[]{:S(2)}) collective-permute-start(bf16[512,2048]{1,0:T(8,128)(2,1)} %mixer_other.1), channel_id=1, source_target_pairs={{0,1},{1,0},{2,3},{3,2},{4,5},{5,4},{6,7},{7,6},{8,9},{9,8},{10,11... | collective-permute-start | bytes 6291464 | tf_op jit(solution)/shard_map/ppermute | solution.py:322
  (18 other events, 210.1 us)
Sparse Core Ops, SparseCore 0:
  10.3 124.6 all-gather.2

commit v4 on v3

--- a/solution.py
+++ b/solution.py
@@ -210,15 +210,8 @@
         r = dot_nn(normed[...], w[...].reshape(model, 2 * size))
         hidden[:, pl.ds(at, size)] = (jax.nn.silu(r[:, :size]) * r[:, size:]).astype(BF16)
 
-    if first:
-        up_to(0, 0, first)
-
-    def whole(j, carry):
-        at = pl.multiple_of(first + j * CHUNK, 128)
-        up_to(j + (first > 0), at, CHUNK)
-        return carry
-
-    lax.fori_loop(0, tps * wide // CHUNK, whole, 0)
+    for j, (at, size) in enumerate(zip(starts, sizes)):
+        up_to(j, at, size)
     pltpu.make_async_copy(down, down, sem_d).wait()
     mids.wait()
 
@@ -318,11 +311,11 @@
         mixer, normed=normed, pieces=(*for_unit, *for_value, *for_out), mask_w=mask_w, bias=bias, gain=gain,
         shifts=shifts, count=rows,
     )
-    other = unit(False, dtype=BF16)
+    other = unit(False, dtype=F32)
     arrived = lax.ppermute(other, "tp", [(i, (i + 1) % tps) for i in range(tps)])
     kept = unit(True, dtype=F32)
     residual = lax.dynamic_slice_in_dim(tokens, tp * rows, rows, 0).astype(F32)
-    h_mid = (residual + (kept + arrived.astype(F32))).astype(BF16)
+    h_mid = (residual + (kept + arrived)).astype(BF16)
     normed_mid = rms_scale(h_mid, norm_ffn).astype(BF16)
     return ffn(h_mid, normed_mid, packed, share)
 

time: 166 us -> 166 us (level)
    all_gather x1, waiting for transfers between devices: 10.1 us -> 7.64 us  [on_device(): lax.all_gather(packed, EVERY).reshape(tps, reps, fss, *packed.shape)]
  transfers between devices with their start and end apart: 29 -> 29, of which waited for: 10 -> 10; matrix products, arithmetic and copies ran while one was open for 15% -> 14% of each run, Pallas kernels for 12% -> 12%
where the time goes in v4:
time: 166 us; the launch traced here: 165 us
  starting transfers between devices  46.2 us (28%)
  Pallas kernels  45.3 us (27%)
  waiting for transfers between devices  35.6 us (21%)
  other arithmetic  16.8 us (10%)
  between operations  13.8 us (8%)
  local copies, waits for them, and re-layouts  7.53 us (5%)
    ppermute x27, starting transfers between devices, shift(): return lax.ppermute(x, CHIPS, pairs)  37.1 us
    ppermute x27, waiting for transfers between devices, shift(): return lax.ppermute(x, CHIPS, pairs)  26.5 us
    pallas_call x1, Pallas kernels, ffn(): pl.pallas_call(ffn_body, out_shape=jax.ShapeDtypeStruct(h_mid.shape, BF16...  23.4 us
    pallas_call x2, Pallas kernels, mixer(): pl.pallas_call(functools.partial(mixer_body, own), out_shape=jax.ShapeDty...  20 us
    ppermute x1, starting transfers between devices, on_device(): lax.ppermute(other, 'tp', [(i, (i + 1) % tps) for i in range(tps)])  9.12 us
    reduce_sum x2, other arithmetic, rms_scale(): scale = lax.rsqrt(jnp.mean(values * values, axis=-1, keepdims=True) + 1e-06)  7.82 us
    all_gather x1, waiting for transfers between devices, on_device(): lax.all_gather(packed, EVERY).reshape(tps, reps, fss, *packed.shape)  7.64 us
    slice x3, local copies, waits for them, and re-layouts, relayed_ring(): ahead[half:]  3.35 us
  transfers between devices with their start and end apart: 29, of which 10 were waited for; matrix products, arithmetic and copies ran while one was open for 14% of the time, Pallas kernels for 12%

profile of v4, /device:TPU:1, one launch (start us, length us, event | category | flops | bytes accessed | tf_op | source)
XLA Modules:
  0.0 165.2 jit_solution(8896812760076285913)
XLA Ops:
  6.5 1.8 %pack.1 = bf16[96,1408]{1,0:T(8,128)(2,1)} custom-call(bf16[64,1408]{1,0:T(8,128)(2,1)} %gate.1, bf16[64,1408]{1,0:T(8,128)(2,1)} %up.1, bf16[64,1408]{1,0:T(8,128)(2,1)} %bitcast.42), custom_call_target="tpu_custom_call" | custom-call | tf_op jit(solution)/shard_map/pack/pallas_call | solution.py:268
  9.2 4.6 %collective-permute-start.17 = (bf16[32,512]{1,0:T(8,128)(2,1)S(1)}, bf16[32,512]{1,0:T(8,128)(2,1)S(1)}, u32[]{:S(2)}, u32[]{:S(2)}) collective-permute-start(bf16[32,512]{1,0:T(8,128)(2,1)S(1)} %dynamic-slice_bitcast_fusion), channel_id=1, source_target_pairs={{0,96},{2,98},{4,100},{6,102},{8,104},{10,106},{12,108},{14,110},{... | collective-permute-start | bytes 98312 | tf_op jit(solution)/shard_map/ppermute | solution.py:27
  15.2 2.5 %collective-permute-start = (bf16[64,512]{1,0:T(8,128)(2,1)S(1)}, bf16[64,512]{1,0:T(8,128)(2,1)S(1)}, u32[]{:S(2)}, u32[]{:S(2)}) collective-permute-start(bf16[64,512]{1,0:T(8,128)(2,1)S(1)} %pad_maximum_fusion.5), channel_id=1, source_target_pairs={{0,6},{2,0},{4,2},{6,4},{8,14},{10,8},{12,10},{14,12},{16,22},{18,... | collective-permute-start | bytes 196616 | tf_op jit(solution)/shard_map/ppermute | solution.py:27
  19.8 2.8 %collective-permute-start.21 = (bf16[4,32,512]{2,1,0:T(8,128)(2,1)S(1)}, bf16[4,32,512]{2,1,0:T(8,128)(2,1)S(1)}, u32[]{:S(2)}, u32[]{:S(2)}) collective-permute-start(bf16[4,32,512]{2,1,0:T(8,128)(2,1)S(1)} %get-tuple-element.15), channel_id=1, source_target_pairs={{0,24},{2,26},{4,28},{6,30},{8,0},{10,2},{12,4},{14,6},{16,8},{18,... | collective-permute-start | bytes 393224 | tf_op jit(solution)/shard_map/ppermute | solution.py:27
  24.5 3.4 %collective-permute-start.22 = (bf16[4,32,512]{2,1,0:T(8,128)(2,1)S(1)}, bf16[4,32,512]{2,1,0:T(8,128)(2,1)S(1)}, u32[]{:S(2)}, u32[]{:S(2)}) collective-permute-start(bf16[4,32,512]{2,1,0:T(8,128)(2,1)S(1)} %collective-permute-done.21), channel_id=1, source_target_pairs={{0,24},{2,26},{4,28},{6,30},{8,0},{10,2},{12,4},{14,6},{16,8},{18,... | collective-permute-start | bytes 393224 | tf_op jit(solution)/shard_map/ppermute | solution.py:27
  28.0 2.0 %collective-permute-start.10 = (bf16[4,32,512]{2,1,0:T(8,128)(2,1)S(1)}, bf16[4,32,512]{2,1,0:T(8,128)(2,1)S(1)}, u32[]{:S(2)}, u32[]{:S(2)}) collective-permute-start(bf16[4,32,512]{2,1,0:T(8,128)(2,1)S(1)} %get-tuple-element.9), channel_id=1, source_target_pairs={{0,32},{2,34},{4,36},{6,38},{8,40},{10,42},{12,44},{14,46},{16,48}... | collective-permute-start | bytes 393224 | tf_op jit(solution)/shard_map/ppermute | solution.py:27
  30.3 1.9 %collective-permute-start.23 = (bf16[4,4,32,512]{3,2,1,0:T(8,128)(2,1)S(1)}, bf16[4,4,32,512]{3,2,1,0:T(8,128)(2,1)S(1)}, u32[]{:S(2)}, u32[]{:S(2)}) collective-permute-start(bf16[4,4,32,512]{3,2,1,0:T(8,128)(2,1)S(1)} %pad_maximum_fusion.2.refs_11_), channel_id=1, source_target_pairs={{0,2},{2,4},{4,6},{6,0},{8,10},{10,12},{12,14},{14,8},{16,18},{18,... | collective-permute-start | bytes 1572872 | tf_op jit(solution)/shard_map/ppermute | solution.py:27
  32.3 3.1 %fusion = f32[1024]{0:T(1024)S(1)} fusion(bf16[1024,2048]{1,0:T(8,128)(2,1)} %param.13), kind=kLoop, calls=%fused_computation.2 | loop fusion | flops 6290432 | bytes 4198400 | tf_op jit(solution)/shard_map/reduce_sum | solution.py:62
  36.5 3.2 %collective-permute-start.5 = (bf16[4,32,512]{2,1,0:T(8,128)(2,1)S(1)}, bf16[4,32,512]{2,1,0:T(8,128)(2,1)S(1)}, u32[]{:S(2)}, u32[]{:S(2)}) collective-permute-start(bf16[4,32,512]{2,1,0:T(8,128)(2,1)S(1)} %get-tuple-element.10), channel_id=1, source_target_pairs={{0,24},{2,26},{4,28},{6,30},{8,0},{10,2},{12,4},{14,6},{16,8},{18,... | collective-permute-start | bytes 393224 | tf_op jit(solution)/shard_map/ppermute | solution.py:27
  39.7 1.5 collective-permute-start.11
  42.3 2.7 %collective-permute-done.11 = bf16[4,32,512]{2,1,0:T(8,128)(2,1)S(1)} collective-permute-done((bf16[4,32,512]{2,1,0:T(8,128)(2,1)S(1)}, bf16[4,32,512]{2,1,0:T(8,128)(2,1)S(1)}, u32[]{:S(2)}, u32[]{:S(2)}) %collective-permute-start.11) | collective-permute-done | bytes 131104 | tf_op jit(solution)/shard_map/ppermute | solution.py:27
  45.2 2.7 %collective-permute-start.14 = (bf16[4,4,32,512]{3,2,1,0:T(8,128)(2,1)S(1)}, bf16[4,4,32,512]{3,2,1,0:T(8,128)(2,1)}, u32[]{:S(2)}, u32[]{:S(2)}) collective-permute-start(bf16[4,4,32,512]{3,2,1,0:T(8,128)(2,1)S(1)} %pad_maximum_fusion.1.refs_6_), channel_id=1, source_target_pairs={{0,24},{2,26},{4,28},{6,30},{8,0},{10,2},{12,4},{14,6},{16,8},{18,... | collective-permute-start | bytes 1572872 | tf_op jit(solution)/shard_map/ppermute | solution.py:27
  48.3 2.4 %collective-permute-start.7 = (bf16[4,4,32,512]{3,2,1,0:T(8,128)(2,1)S(1)}, bf16[4,4,32,512]{3,2,1,0:T(8,128)(2,1)}, u32[]{:S(2)}, u32[]{:S(2)}) collective-permute-start(bf16[4,4,32,512]{3,2,1,0:T(8,128)(2,1)S(1)} %pad_maximum_fusion.refs_1_), channel_id=1, source_target_pairs={{0,96},{2,98},{4,100},{6,102},{8,104},{10,106},{12,108},{14,110},{... | collective-permute-start | bytes 1572872 | tf_op jit(solution)/shard_map/ppermute | solution.py:27
  50.7 3.0 %fusion.2.refs_0_ = bf16[1024,2048]{1,0:T(8,128)(2,1)} fusion(bf16[1024,2048]{1,0:T(8,128)(2,1)S(1)} %copy-done.2, f32[2048]{0:T(1024)S(1)} %convert_element_type.31, f32[1024]{0:T(1024)S(1)} %add_rsqrt_fusion), kind=kLoop, calls=%fused_computation.4 | loop fusion | flops 8388608 | bytes 8400896 | tf_op jit(solution)/shard_map/convert_element_type | solution.py:308
  53.7 3.3 %collective-permute-done.24.refs_13_ = bf16[4,4,32,512]{3,2,1,0:T(8,128)(2,1)S(1)} collective-permute-done((bf16[4,4,32,512]{3,2,1,0:T(8,128)(2,1)S(1)}, bf16[4,4,32,512]{3,2,1,0:T(8,128)(2,1)S(1)}, u32[]{:S(2)}, u32[]{:S(2)}) %collective-permute-start.24) | collective-permute-done | bytes 524320 | tf_op jit(solution)/shard_map/ppermute | solution.py:27
  57.8 1.5 dynamic-slice_select_fusion.refs_16_
  59.3 10.0 %collective-permute-done.13.refs_7_ = bf16[4,4,32,512]{3,2,1,0:T(8,128)(2,1)S(1)} collective-permute-done((bf16[4,4,32,512]{3,2,1,0:T(8,128)(2,1)S(1)}, bf16[4,4,32,512]{3,2,1,0:T(8,128)(2,1)S(1)}, u32[]{:S(2)}, u32[]{:S(2)}) %collective-permute-start.13) | collective-permute-done | bytes 524320 | tf_op jit(solution)/shard_map/ppermute | solution.py:27
  69.6 1.7 %slice.37 = bf16[2,4,32,512]{3,2,1,0:T(8,128)(2,1)} slice(bf16[4,4,32,512]{3,2,1,0:T(8,128)(2,1)} %collective-permute-done.14.refs_8_), slice={[2:4], [0:4], [0:32], [0:512]} | slice | bytes 524288 | tf_op jit(solution)/shard_map/slice | solution.py:43
  71.3 2.7 %collective-permute-start.16 = (bf16[2,4,32,512]{3,2,1,0:T(8,128)(2,1)}, bf16[2,4,32,512]{3,2,1,0:T(8,128)(2,1)S(1)}, u32[]{:S(2)}, u32[]{:S(2)}) collective-permute-start(bf16[2,4,32,512]{3,2,1,0:T(8,128)(2,1)} %slice.37), channel_id=1, source_target_pairs={{0,24},{2,26},{4,28},{6,30},{8,0},{10,2},{12,4},{14,6},{16,8},{18,... | collective-permute-start | bytes 786440 | tf_op jit(solution)/shard_map/ppermute | solution.py:27
  73.9 1.7 %slice.33 = bf16[2,4,32,512]{3,2,1,0:T(8,128)(2,1)} slice(bf16[4,4,32,512]{3,2,1,0:T(8,128)(2,1)} %collective-permute-done.6.refs_2_), slice={[0:2], [0:4], [0:32], [0:512]} | slice | bytes 524288 | tf_op jit(solution)/shard_map/slice | solution.py:43
  75.6 1.7 %slice.34 = bf16[2,4,32,512]{3,2,1,0:T(8,128)(2,1)} slice(bf16[4,4,32,512]{3,2,1,0:T(8,128)(2,1)} %collective-permute-done.7.refs_3_), slice={[2:4], [0:4], [0:32], [0:512]} | slice | bytes 524288 | tf_op jit(solution)/shard_map/slice | solution.py:43
  77.3 2.7 %collective-permute-start.9 = (bf16[2,4,32,512]{3,2,1,0:T(8,128)(2,1)}, bf16[2,4,32,512]{3,2,1,0:T(8,128)(2,1)S(1)}, u32[]{:S(2)}, u32[]{:S(2)}) collective-permute-start(bf16[2,4,32,512]{3,2,1,0:T(8,128)(2,1)} %slice.34), channel_id=1, source_target_pairs={{0,96},{2,98},{4,100},{6,102},{8,104},{10,106},{12,108},{14,110},{... | collective-permute-start | bytes 786440 | tf_op jit(solution)/shard_map/ppermute | solution.py:27
  80.7 6.7 %collective-permute-done.8.refs_4_ = bf16[2,4,32,512]{3,2,1,0:T(8,128)(2,1)S(1)} collective-permute-done((bf16[2,4,32,512]{3,2,1,0:T(8,128)(2,1)}, bf16[2,4,32,512]{3,2,1,0:T(8,128)(2,1)S(1)}, u32[]{:S(2)}, u32[]{:S(2)}) %collective-permute-start.8) | collective-permute-done | bytes 262176 | tf_op jit(solution)/shard_map/ppermute | solution.py:27
  87.4 1.9 %collective-permute-done.9.refs_5_ = bf16[2,4,32,512]{3,2,1,0:T(8,128)(2,1)S(1)} collective-permute-done((bf16[2,4,32,512]{3,2,1,0:T(8,128)(2,1)}, bf16[2,4,32,512]{3,2,1,0:T(8,128)(2,1)S(1)}, u32[]{:S(2)}, u32[]{:S(2)}) %collective-permute-start.9) | collective-permute-done | bytes 262176 | tf_op jit(solution)/shard_map/ppermute | solution.py:27
  90.0 10.0 %mixer_other.1 = f32[512,2048]{1,0:T(8,128)} custom-call(bf16[1024,2048]{1,0:T(8,128)(2,1)} %fusion.2.refs_0_, bf16[4,4,32,512]{3,2,1,0:T(8,128)(2,1)} %copy-done.7, bf16[4,4,32,512]{3,2,1,0:T(8,128)(2,1)} %collective-permute-done.6.refs_2_, bf16[4,4,32,512]{3,2,1,0:T(8,128)(2,1)} %collective-permute-done.7.refs_3_, bf16[2,4,32,512]{3,2,1,0:T(8,128)(2,1)} %copy-done.15, ...), custom_call_target="tpu_custom_call" | custom-call | tf_op jit(solution)/shard_map/mixer_other/pallas_call | solution.py:145
  100.0 9.1 %collective-permute-start.27 = (f32[512,2048]{1,0:T(8,128)}, f32[512,2048]{1,0:T(8,128)}, u32[]{:S(2)}, u32[]{:S(2)}) collective-permute-start(f32[512,2048]{1,0:T(8,128)} %mixer_other.1), channel_id=1, source_target_pairs={{0,1},{1,0},{2,3},{3,2},{4,5},{5,4},{6,7},{7,6},{8,9},{9,8},{10,11... | collective-permute-start | bytes 12582920 | tf_op jit(solution)/shard_map/ppermute | solution.py:315
  109.2 10.0 %mixer_own.1 = f32[512,2048]{1,0:T(8,128)} custom-call(bf16[1024,2048]{1,0:T(8,128)(2,1)} %fusion.2.refs_0_, bf16[4,4,32,512]{3,2,1,0:T(8,128)(2,1)} %copy-done.7, bf16[4,4,32,512]{3,2,1,0:T(8,128)(2,1)} %collective-permute-done.6.refs_2_, bf16[4,4,32,512]{3,2,1,0:T(8,128)(2,1)} %collective-permute-done.7.refs_3_, bf16[2,4,32,512]{3,2,1,0:T(8,128)(2,1)} %copy-done.15, ...), custom_call_target="tpu_custom_call" | custom-call | tf_op jit(solution)/shard_map/mixer_own/pallas_call | solution.py:145
  119.2 1.4 collective-permute-done.27
  120.6 4.7 %fusion.3 = (f32[512]{0:T(512)S(1)}, bf16[512,2048]{1,0:T(8,128)(2,1)S(1)}) fusion(f32[512,2048]{1,0:T(8,128)} %mixer_own.1, f32[512,2048]{1,0:T(8,128)} %collective-permute-done.27, bf16[1024,2048]{1,0:T(8,128)(2,1)S(1)} %copy-done.3, s32[]{:T(128)S(6)} %select_n.211), kind=kLoop, calls=%fused_computation.7 | loop fusion | flops 7339520 | bytes 12584964 | tf_op jit(solution)/shard_map/reduce_sum | solution.py:62
  125.3 1.9 %fusion.5.n_hbm = bf16[512,2048]{1,0:T(8,128)(2,1)} fusion(bf16[512,2048]{1,0:T(8,128)(2,1)S(1)} %get-tuple-element.6.h_hbm, f32[2048]{0:T(1024)S(1)} %convert_element_type.35, f32[512]{0:T(512)S(1)} %add_rsqrt_fusion.1), kind=kLoop, calls=%fused_computation.9 | loop fusion | flops 4194304 | bytes 4204544 | tf_op jit(solution)/shard_map/convert_element_type | solution.py:319
  127.2 7.6 %all-gather.3.cloned.1.call-done = bf16[12288,1408]{1,0:T(8,128)(2,1)} async-done(((bf16[96,1408]{1,0:T(8,128)(2,1)}), bf16[12288,1408]{1,0:T(8,128)(2,1)}) %all-gather.3.cloned.1.call-update) | async-done | bytes 34603024 | tf_op jit(solution)/shard_map/all_gather | solution.py:292
  134.9 23.4 %ffn.1 = bf16[512,2048]{1,0:T(8,128)(2,1)} custom-call(bf16[512,2048]{1,0:T(8,128)(2,1)} %copy-done.4, bf16[512,2048]{1,0:T(8,128)(2,1)} %fusion.5.n_hbm, bf16[2,2,32,96,1408]{4,3,2,1,0:T(8,128)(2,1)} %bitcast.41), custom_call_target="tpu_custom_call" | custom-call | tf_op jit(solution)/shard_map/ffn/pallas_call | solution.py:242
  (105 shorter events, 12.0 us)
Async XLA Ops:
  6.5 73.4 %copy-start = (bf16[4,128]{1,0:T(4,128)(2,1)S(1)}, bf16[4,128]{1,0:T(4,128)(2,1)}, u32[]{:S(2)}) copy-start(bf16[4,128]{1,0:T(4,128)(2,1)} %param.18) | copy-start | bytes 3076
  6.5 128.3 %all-gather.3.cloned.1.call-start = ((), (), s32[]{:S(2)}) async-start(), calls=%async_computation | async-start | bytes 34873344 | tf_op jit(solution)/shard_map/all_gather | solution.py:292
  9.2 9.1 %collective-permute-start.17 = (bf16[32,512]{1,0:T(8,128)(2,1)S(1)}, bf16[32,512]{1,0:T(8,128)(2,1)S(1)}, u32[]{:S(2)}, u32[]{:S(2)}) collective-permute-start(bf16[32,512]{1,0:T(8,128)(2,1)S(1)} %dynamic-slice_bitcast_fusion), channel_id=1, source_target_pairs={{0,96},{2,98},{4,100},{6,102},{8,104},{10,106},{12,108},{14,110},{... | collective-permute-start | bytes 98312 | tf_op jit(solution)/shard_map/ppermute | solution.py:27
  13.7 5.2 %collective-permute-start.18 = (bf16[32,512]{1,0:T(8,128)(2,1)S(1)}, bf16[32,512]{1,0:T(8,128)(2,1)S(1)}, u32[]{:S(2)}, u32[]{:S(2)}) collective-permute-start(bf16[32,512]{1,0:T(8,128)(2,1)S(1)} %dynamic-slice_bitcast_fusion), channel_id=1, source_target_pairs={{0,64},{2,66},{4,68},{6,70},{8,72},{10,74},{12,76},{14,78},{16,80}... | collective-permute-start | bytes 98312 | tf_op jit(solution)/shard_map/ppermute | solution.py:27
  13.7 5.2 %collective-permute-start.19 = (bf16[32,512]{1,0:T(8,128)(2,1)S(1)}, bf16[32,512]{1,0:T(8,128)(2,1)S(1)}, u32[]{:S(2)}, u32[]{:S(2)}) collective-permute-start(bf16[32,512]{1,0:T(8,128)(2,1)S(1)} %dynamic-slice_bitcast_fusion), channel_id=1, source_target_pairs={{0,32},{2,34},{4,36},{6,38},{8,40},{10,42},{12,44},{14,46},{16,48}... | collective-permute-start | bytes 98312 | tf_op jit(solution)/shard_map/ppermute | solution.py:27
  15.2 7.3 %collective-permute-start = (bf16[64,512]{1,0:T(8,128)(2,1)S(1)}, bf16[64,512]{1,0:T(8,128)(2,1)S(1)}, u32[]{:S(2)}, u32[]{:S(2)}) collective-permute-start(bf16[64,512]{1,0:T(8,128)(2,1)S(1)} %pad_maximum_fusion.5), channel_id=1, source_target_pairs={{0,6},{2,0},{4,2},{6,4},{8,14},{10,8},{12,10},{14,12},{16,22},{18,... | collective-permute-start | bytes 196616 | tf_op jit(solution)/shard_map/ppermute | solution.py:27
  17.8 4.8 %collective-permute-start.1 = (bf16[64,512]{1,0:T(8,128)(2,1)S(1)}, bf16[64,512]{1,0:T(8,128)(2,1)S(1)}, u32[]{:S(2)}, u32[]{:S(2)}) collective-permute-start(bf16[64,512]{1,0:T(8,128)(2,1)S(1)} %pad_maximum_fusion.5), channel_id=1, source_target_pairs={{0,4},{2,6},{4,0},{6,2},{8,12},{10,14},{12,8},{14,10},{16,20},{18,... | collective-permute-start | bytes 196616 | tf_op jit(solution)/shard_map/ppermute | solution.py:27
  18.3 4.8 %collective-permute-start.2 = (bf16[64,512]{1,0:T(8,128)(2,1)S(1)}, bf16[64,512]{1,0:T(8,128)(2,1)S(1)}, u32[]{:S(2)}, u32[]{:S(2)}) collective-permute-start(bf16[64,512]{1,0:T(8,128)(2,1)S(1)} %pad_maximum_fusion.5), channel_id=1, source_target_pairs={{0,2},{2,4},{4,6},{6,0},{8,10},{10,12},{12,14},{14,8},{16,18},{18,... | collective-permute-start | bytes 196616 | tf_op jit(solution)/shard_map/ppermute | solution.py:27
  19.8 4.8 %collective-permute-start.21 = (bf16[4,32,512]{2,1,0:T(8,128)(2,1)S(1)}, bf16[4,32,512]{2,1,0:T(8,128)(2,1)S(1)}, u32[]{:S(2)}, u32[]{:S(2)}) collective-permute-start(bf16[4,32,512]{2,1,0:T(8,128)(2,1)S(1)} %get-tuple-element.15), channel_id=1, source_target_pairs={{0,24},{2,26},{4,28},{6,30},{8,0},{10,2},{12,4},{14,6},{16,8},{18,... | collective-permute-start | bytes 393224 | tf_op jit(solution)/shard_map/ppermute | solution.py:27
  22.6 7.4 %collective-permute-start.20 = (bf16[4,32,512]{2,1,0:T(8,128)(2,1)S(1)}, bf16[4,32,512]{2,1,0:T(8,128)(2,1)S(1)}, u32[]{:S(2)}, u32[]{:S(2)}) collective-permute-start(bf16[4,32,512]{2,1,0:T(8,128)(2,1)S(1)} %get-tuple-element.15), channel_id=1, source_target_pairs={{0,8},{2,10},{4,12},{6,14},{8,16},{10,18},{12,20},{14,22},{16,24},... | collective-permute-start | bytes 393224 | tf_op jit(solution)/shard_map/ppermute | solution.py:27
  23.3 27.4 %copy-start.2 = (bf16[1024,2048]{1,0:T(8,128)(2,1)S(1)}, bf16[1024,2048]{1,0:T(8,128)(2,1)}, u32[]{:S(2)}) copy-start(bf16[1024,2048]{1,0:T(8,128)(2,1)} %param.13) | copy-start | bytes 12582916
  24.5 5.7 %collective-permute-start.22 = (bf16[4,32,512]{2,1,0:T(8,128)(2,1)S(1)}, bf16[4,32,512]{2,1,0:T(8,128)(2,1)S(1)}, u32[]{:S(2)}, u32[]{:S(2)}) collective-permute-start(bf16[4,32,512]{2,1,0:T(8,128)(2,1)S(1)} %collective-permute-done.21), channel_id=1, source_target_pairs={{0,24},{2,26},{4,28},{6,30},{8,0},{10,2},{12,4},{14,6},{16,8},{18,... | collective-permute-start | bytes 393224 | tf_op jit(solution)/shard_map/ppermute | solution.py:27
  28.0 11.7 %collective-permute-start.10 = (bf16[4,32,512]{2,1,0:T(8,128)(2,1)S(1)}, bf16[4,32,512]{2,1,0:T(8,128)(2,1)S(1)}, u32[]{:S(2)}, u32[]{:S(2)}) collective-permute-start(bf16[4,32,512]{2,1,0:T(8,128)(2,1)S(1)} %get-tuple-element.9), channel_id=1, source_target_pairs={{0,32},{2,34},{4,36},{6,38},{8,40},{10,42},{12,44},{14,46},{16,48}... | collective-permute-start | bytes 393224 | tf_op jit(solution)/shard_map/ppermute | solution.py:27
  30.0 11.2 %collective-permute-start.3 = (bf16[4,32,512]{2,1,0:T(8,128)(2,1)S(1)}, bf16[4,32,512]{2,1,0:T(8,128)(2,1)S(1)}, u32[]{:S(2)}, u32[]{:S(2)}) collective-permute-start(bf16[4,32,512]{2,1,0:T(8,128)(2,1)S(1)} %get-tuple-element.10), channel_id=1, source_target_pairs={{0,8},{2,10},{4,12},{6,14},{8,16},{10,18},{12,20},{14,22},{16,24},... | collective-permute-start | bytes 393224 | tf_op jit(solution)/shard_map/ppermute | solution.py:27
  30.3 18.0 %collective-permute-start.23 = (bf16[4,4,32,512]{3,2,1,0:T(8,128)(2,1)S(1)}, bf16[4,4,32,512]{3,2,1,0:T(8,128)(2,1)S(1)}, u32[]{:S(2)}, u32[]{:S(2)}) collective-permute-start(bf16[4,4,32,512]{3,2,1,0:T(8,128)(2,1)S(1)} %pad_maximum_fusion.2.refs_11_), channel_id=1, source_target_pairs={{0,2},{2,4},{4,6},{6,0},{8,10},{10,12},{12,14},{14,8},{16,18},{18,... | collective-permute-start | bytes 1572872 | tf_op jit(solution)/shard_map/ppermute | solution.py:27
  35.4 5.8 %collective-permute-start.12 = (bf16[4,32,512]{2,1,0:T(8,128)(2,1)S(1)}, bf16[4,32,512]{2,1,0:T(8,128)(2,1)S(1)}, u32[]{:S(2)}, u32[]{:S(2)}) collective-permute-start(bf16[4,32,512]{2,1,0:T(8,128)(2,1)S(1)} %get-tuple-element.9), channel_id=1, source_target_pairs={{0,96},{2,98},{4,100},{6,102},{8,104},{10,106},{12,108},{14,110},{... | collective-permute-start | bytes 393224 | tf_op jit(solution)/shard_map/ppermute | solution.py:27
  36.5 8.6 %collective-permute-start.5 = (bf16[4,32,512]{2,1,0:T(8,128)(2,1)S(1)}, bf16[4,32,512]{2,1,0:T(8,128)(2,1)S(1)}, u32[]{:S(2)}, u32[]{:S(2)}) collective-permute-start(bf16[4,32,512]{2,1,0:T(8,128)(2,1)S(1)} %get-tuple-element.10), channel_id=1, source_target_pairs={{0,24},{2,26},{4,28},{6,30},{8,0},{10,2},{12,4},{14,6},{16,8},{18,... | collective-permute-start | bytes 393224 | tf_op jit(solution)/shard_map/ppermute | solution.py:27
  39.7 5.3 %collective-permute-start.11 = (bf16[4,32,512]{2,1,0:T(8,128)(2,1)S(1)}, bf16[4,32,512]{2,1,0:T(8,128)(2,1)S(1)}, u32[]{:S(2)}, u32[]{:S(2)}) collective-permute-start(bf16[4,32,512]{2,1,0:T(8,128)(2,1)S(1)} %collective-permute-done.10), channel_id=1, source_target_pairs={{0,32},{2,34},{4,36},{6,38},{8,40},{10,42},{12,44},{14,46},{16,48}... | collective-permute-start | bytes 393224 | tf_op jit(solution)/shard_map/ppermute | solution.py:27
  41.2 6.7 %collective-permute-start.4 = (bf16[4,32,512]{2,1,0:T(8,128)(2,1)S(1)}, bf16[4,32,512]{2,1,0:T(8,128)(2,1)S(1)}, u32[]{:S(2)}, u32[]{:S(2)}) collective-permute-start(bf16[4,32,512]{2,1,0:T(8,128)(2,1)S(1)} %collective-permute-done.3), channel_id=1, source_target_pairs={{0,8},{2,10},{4,12},{6,14},{8,16},{10,18},{12,20},{14,22},{16,24},... | collective-permute-start | bytes 393224 | tf_op jit(solution)/shard_map/ppermute | solution.py:27
  41.2 15.8 %collective-permute-start.24 = (bf16[4,4,32,512]{3,2,1,0:T(8,128)(2,1)S(1)}, bf16[4,4,32,512]{3,2,1,0:T(8,128)(2,1)S(1)}, u32[]{:S(2)}, u32[]{:S(2)}) collective-permute-start(bf16[4,4,32,512]{3,2,1,0:T(8,128)(2,1)S(1)} %pad_maximum_fusion.2.refs_11_), channel_id=1, source_target_pairs={{0,6},{2,0},{4,2},{6,4},{8,14},{10,8},{12,10},{14,12},{16,22},{18,... | collective-permute-start | bytes 1572872 | tf_op jit(solution)/shard_map/ppermute | solution.py:27
  45.1 24.2 %collective-permute-start.13 = (bf16[4,4,32,512]{3,2,1,0:T(8,128)(2,1)S(1)}, bf16[4,4,32,512]{3,2,1,0:T(8,128)(2,1)S(1)}, u32[]{:S(2)}, u32[]{:S(2)}) collective-permute-start(bf16[4,4,32,512]{3,2,1,0:T(8,128)(2,1)S(1)} %pad_maximum_fusion.1.refs_6_), channel_id=1, source_target_pairs={{0,8},{2,10},{4,12},{6,14},{8,16},{10,18},{12,20},{14,22},{16,24},... | collective-permute-start | bytes 1572872 | tf_op jit(solution)/shard_map/ppermute | solution.py:27
  45.2 24.1 %collective-permute-start.14 = (bf16[4,4,32,512]{3,2,1,0:T(8,128)(2,1)S(1)}, bf16[4,4,32,512]{3,2,1,0:T(8,128)(2,1)}, u32[]{:S(2)}, u32[]{:S(2)}) collective-permute-start(bf16[4,4,32,512]{3,2,1,0:T(8,128)(2,1)S(1)} %pad_maximum_fusion.1.refs_6_), channel_id=1, source_target_pairs={{0,24},{2,26},{4,28},{6,30},{8,0},{10,2},{12,4},{14,6},{16,8},{18,... | collective-permute-start | bytes 1572872 | tf_op jit(solution)/shard_map/ppermute | solution.py:27
  47.9 23.3 %collective-permute-start.6 = (bf16[4,4,32,512]{3,2,1,0:T(8,128)(2,1)S(1)}, bf16[4,4,32,512]{3,2,1,0:T(8,128)(2,1)}, u32[]{:S(2)}, u32[]{:S(2)}) collective-permute-start(bf16[4,4,32,512]{3,2,1,0:T(8,128)(2,1)S(1)} %pad_maximum_fusion.refs_1_), channel_id=1, source_target_pairs={{0,32},{2,34},{4,36},{6,38},{8,40},{10,42},{12,44},{14,46},{16,48}... | collective-permute-start | bytes 1572872 | tf_op jit(solution)/shard_map/ppermute | solution.py:27
  48.3 27.3 %collective-permute-start.7 = (bf16[4,4,32,512]{3,2,1,0:T(8,128)(2,1)S(1)}, bf16[4,4,32,512]{3,2,1,0:T(8,128)(2,1)}, u32[]{:S(2)}, u32[]{:S(2)}) collective-permute-start(bf16[4,4,32,512]{3,2,1,0:T(8,128)(2,1)S(1)} %pad_maximum_fusion.refs_1_), channel_id=1, source_target_pairs={{0,96},{2,98},{4,100},{6,102},{8,104},{10,106},{12,108},{14,110},{... | collective-permute-start | bytes 1572872 | tf_op jit(solution)/shard_map/ppermute | solution.py:27
  57.0 32.3 %copy-start.9 = (bf16[4,4,32,512]{3,2,1,0:T(8,128)(2,1)}, bf16[4,4,32,512]{3,2,1,0:T(8,128)(2,1)S(1)}, u32[]{:S(2)}) copy-start(bf16[4,4,32,512]{3,2,1,0:T(8,128)(2,1)S(1)} %collective-permute-done.24.refs_13_) | copy-start | bytes 1572868
  57.0 20.2 %collective-permute-start.25 = (bf16[2,4,32,512]{3,2,1,0:T(8,128)(2,1)S(1)}, bf16[2,4,32,512]{3,2,1,0:T(8,128)(2,1)S(1)}, u32[]{:S(2)}, u32[]{:S(2)}) collective-permute-start(bf16[2,4,32,512]{3,2,1,0:T(8,128)(2,1)S(1)} %slice.38), channel_id=1, source_target_pairs={{0,2},{2,4},{4,6},{6,0},{8,10},{10,12},{12,14},{14,8},{16,18},{18,... | collective-permute-start | bytes 786440 | tf_op jit(solution)/shard_map/ppermute | solution.py:27
  69.3 11.4 %collective-permute-start.26 = (bf16[2,4,32,512]{3,2,1,0:T(8,128)(2,1)S(1)}, bf16[2,4,32,512]{3,2,1,0:T(8,128)(2,1)S(1)}, u32[]{:S(2)}, u32[]{:S(2)}) collective-permute-start(bf16[2,4,32,512]{3,2,1,0:T(8,128)(2,1)S(1)} %slice.39), channel_id=1, source_target_pairs={{0,6},{2,0},{4,2},{6,4},{8,14},{10,8},{12,10},{14,12},{16,22},{18,... | collective-permute-start | bytes 786440 | tf_op jit(solution)/shard_map/ppermute | solution.py:27
  69.3 11.4 %collective-permute-start.15 = (bf16[2,4,32,512]{3,2,1,0:T(8,128)(2,1)S(1)}, bf16[2,4,32,512]{3,2,1,0:T(8,128)(2,1)S(1)}, u32[]{:S(2)}, u32[]{:S(2)}) collective-permute-start(bf16[2,4,32,512]{3,2,1,0:T(8,128)(2,1)S(1)} %slice.36), channel_id=1, source_target_pairs={{0,8},{2,10},{4,12},{6,14},{8,16},{10,18},{12,20},{14,22},{16,24},... | collective-permute-start | bytes 786440 | tf_op jit(solution)/shard_map/ppermute | solution.py:27
  71.3 9.5 %collective-permute-start.16 = (bf16[2,4,32,512]{3,2,1,0:T(8,128)(2,1)}, bf16[2,4,32,512]{3,2,1,0:T(8,128)(2,1)S(1)}, u32[]{:S(2)}, u32[]{:S(2)}) collective-permute-start(bf16[2,4,32,512]{3,2,1,0:T(8,128)(2,1)} %slice.37), channel_id=1, source_target_pairs={{0,24},{2,26},{4,28},{6,30},{8,0},{10,2},{12,4},{14,6},{16,8},{18,... | collective-permute-start | bytes 786440 | tf_op jit(solution)/shard_map/ppermute | solution.py:27
  75.6 11.8 %collective-permute-start.8 = (bf16[2,4,32,512]{3,2,1,0:T(8,128)(2,1)}, bf16[2,4,32,512]{3,2,1,0:T(8,128)(2,1)S(1)}, u32[]{:S(2)}, u32[]{:S(2)}) collective-permute-start(bf16[2,4,32,512]{3,2,1,0:T(8,128)(2,1)} %slice.33), channel_id=1, source_target_pairs={{0,32},{2,34},{4,36},{6,38},{8,40},{10,42},{12,44},{14,46},{16,48}... | collective-permute-start | bytes 786440 | tf_op jit(solution)/shard_map/ppermute | solution.py:27
  77.3 12.0 %collective-permute-start.9 = (bf16[2,4,32,512]{3,2,1,0:T(8,128)(2,1)}, bf16[2,4,32,512]{3,2,1,0:T(8,128)(2,1)S(1)}, u32[]{:S(2)}, u32[]{:S(2)}) collective-permute-start(bf16[2,4,32,512]{3,2,1,0:T(8,128)(2,1)} %slice.34), channel_id=1, source_target_pairs={{0,96},{2,98},{4,100},{6,102},{8,104},{10,106},{12,108},{14,110},{... | collective-permute-start | bytes 786440 | tf_op jit(solution)/shard_map/ppermute | solution.py:27
  100.0 20.5 %collective-permute-start.27 = (f32[512,2048]{1,0:T(8,128)}, f32[512,2048]{1,0:T(8,128)}, u32[]{:S(2)}, u32[]{:S(2)}) collective-permute-start(f32[512,2048]{1,0:T(8,128)} %mixer_other.1), channel_id=1, source_target_pairs={{0,1},{1,0},{2,3},{3,2},{4,5},{5,4},{6,7},{7,6},{8,9},{9,8},{10,11... | collective-permute-start | bytes 12582920 | tf_op jit(solution)/shard_map/ppermute | solution.py:315
  (18 other events, 211.5 us)
Sparse Core Ops, SparseCore 0:
  10.3 124.4 all-gather.2

commit v5 on v3

--- a/solution.py
+++ b/solution.py
@@ -157,7 +157,7 @@
 
 
 def ffn_body(h_hbm, n_hbm, packed, out_hbm, h_mid, normed, mid, down, hidden, out, sem_h, sem_n, sem_w, sem_d, sem_o):
-    tps, share, wide = packed.shape[0], down.shape[2], packed.shape[-1]
+    tps, share, wide = packed.shape[0], down.shape[1], packed.shape[-1]
     _, model = out.shape
     first = tps * wide % CHUNK
     starts = [0] * (first > 0) + list(range(first, tps * wide, CHUNK))
@@ -185,7 +185,7 @@
         half = share // 2
         return [
             pltpu.make_async_copy(
-                packed.at[t, r, :, pl.ds(share, half)], down.at[t, :, pl.ds(r * half, half)], sem_d
+                packed.at[t, r, :, pl.ds(share, half)], down.at[:, pl.ds(r * half, half), pl.ds(t * wide, wide)], sem_d
             )
             for r in range(2)
         ]
@@ -214,8 +214,7 @@
         up_to(0, 0, first)
 
     def whole(j, carry):
-        at = pl.multiple_of(first + j * CHUNK, 128)
-        up_to(j + (first > 0), at, CHUNK)
+        up_to(j + (first > 0), pl.multiple_of(first + j * CHUNK, 128), CHUNK)
         return carry
 
     lax.fori_loop(0, tps * wide // CHUNK, whole, 0)
@@ -223,22 +222,16 @@
     mids.wait()
 
     def leave(k):
-        cols = pl.ds(pl.multiple_of(k * CHUNK, CHUNK), CHUNK)
+        cols = pl.ds(k * CHUNK, CHUNK)
         return pltpu.make_async_copy(out.at[:, cols], out_hbm.at[:, cols], sem_o.at[k])
 
     lines = CHUNK // share
 
-    def back(k, carry):
-        cols = pl.ds(pl.multiple_of(k * CHUNK, CHUNK), CHUNK)
-        acc = h_mid[:, cols].astype(F32)
-        for t in range(tps):
-            w = down[t, pl.ds(k * lines, lines)].reshape(CHUNK, wide)
-            acc = acc + dot_nt(hidden[:, t * wide : (t + 1) * wide], w)
-        out[:, cols] = acc.astype(BF16)
+    for k in range(model // CHUNK):
+        cols = slice(k * CHUNK, (k + 1) * CHUNK)
+        w = down[k * lines : (k + 1) * lines].reshape(CHUNK, tps * wide)
+        out[:, cols] = (h_mid[:, cols].astype(F32) + dot_nt(hidden[...], w)).astype(BF16)
         leave(k).start()
-        return carry
-
-    lax.fori_loop(0, model // CHUNK, back, 0)
     for k in range(model // CHUNK):
         leave(k).wait()
 
@@ -252,7 +245,7 @@
         in_specs=[ANY] * 3,
         out_specs=ANY,
         scratch_shapes=[
-            row, row, pltpu.VMEM((fs, share, 2 * tps * wide), BF16), pltpu.VMEM((tps, fs, share, wide), BF16),
+            row, row, pltpu.VMEM((fs, share, 2 * tps * wide), BF16), pltpu.VMEM((fs, share, tps * wide), BF16),
             pltpu.VMEM((h_mid.shape[0], tps * wide), BF16), row,
             pltpu.SemaphoreType.DMA, pltpu.SemaphoreType.DMA, pltpu.SemaphoreType.DMA((-(-tps * wide // CHUNK),)),
             pltpu.SemaphoreType.DMA, pltpu.SemaphoreType.DMA((h_mid.shape[1] // CHUNK,)),
@@ -318,11 +311,11 @@
         mixer, normed=normed, pieces=(*for_unit, *for_value, *for_out), mask_w=mask_w, bias=bias, gain=gain,
         shifts=shifts, count=rows,
     )
-    other = unit(False, dtype=BF16)
+    other = unit(False, dtype=F32)
     arrived = lax.ppermute(other, "tp", [(i, (i + 1) % tps) for i in range(tps)])
     kept = unit(True, dtype=F32)
     residual = lax.dynamic_slice_in_dim(tokens, tp * rows, rows, 0).astype(F32)
-    h_mid = (residual + (kept + arrived.astype(F32))).astype(BF16)
+    h_mid = (residual + (kept + arrived)).astype(BF16)
     normed_mid = rms_scale(h_mid, norm_ffn).astype(BF16)
     return ffn(h_mid, normed_mid, packed, share)
 

time: 166 us -> 165 us (level)
    all_gather x1, waiting for transfers between devices: 10.1 us -> 7.62 us  [on_device(): lax.all_gather(packed, EVERY).reshape(tps, reps, fss, *packed.shape)]
  transfers between devices with their start and end apart: 29 -> 29, of which waited for: 10 -> 10; matrix products, arithmetic and copies ran while one was open for 15% -> 14% of each run, Pallas kernels for 12% -> 12%
where the time goes in v5:
time: 165 us; the launch traced here: 164 us
  starting transfers between devices  46.4 us (28%)
  Pallas kernels  44.2 us (27%)
  waiting for transfers between devices  35.5 us (22%)
  other arithmetic  16.7 us (10%)
  between operations  13.8 us (8%)
  local copies, waits for them, and re-layouts  7.53 us (5%)
    ppermute x27, starting transfers between devices, shift(): return lax.ppermute(x, CHIPS, pairs)  37.1 us
    ppermute x27, waiting for transfers between devices, shift(): return lax.ppermute(x, CHIPS, pairs)  26.5 us
    pallas_call x1, Pallas kernels, ffn(): pl.pallas_call(ffn_body, out_shape=jax.ShapeDtypeStruct(h_mid.shape, BF16...  22.4 us
    pallas_call x2, Pallas kernels, mixer(): pl.pallas_call(functools.partial(mixer_body, own), out_shape=jax.ShapeDty...  20 us
    ppermute x1, starting transfers between devices, on_device(): lax.ppermute(other, 'tp', [(i, (i + 1) % tps) for i in range(tps)])  9.34 us
    reduce_sum x2, other arithmetic, rms_scale(): scale = lax.rsqrt(jnp.mean(values * values, axis=-1, keepdims=True) + 1e-06)  7.72 us
    all_gather x1, waiting for transfers between devices, on_device(): lax.all_gather(packed, EVERY).reshape(tps, reps, fss, *packed.shape)  7.62 us
    slice x3, local copies, waits for them, and re-layouts, relayed_ring(): ahead[half:]  3.35 us
  transfers between devices with their start and end apart: 29, of which 10 were waited for; matrix products, arithmetic and copies ran while one was open for 14% of the time, Pallas kernels for 12%

profile of v5, /device:TPU:1, one launch (start us, length us, event | category | flops | bytes accessed | tf_op | source)
XLA Modules:
  0.0 164.1 jit_solution(7051168157988454910)
XLA Ops:
  6.5 1.8 %pack.1 = bf16[96,1408]{1,0:T(8,128)(2,1)} custom-call(bf16[64,1408]{1,0:T(8,128)(2,1)} %gate.1, bf16[64,1408]{1,0:T(8,128)(2,1)} %up.1, bf16[64,1408]{1,0:T(8,128)(2,1)} %bitcast.42), custom_call_target="tpu_custom_call" | custom-call | tf_op jit(solution)/shard_map/pack/pallas_call | solution.py:268
  9.2 4.6 %collective-permute-start.17 = (bf16[32,512]{1,0:T(8,128)(2,1)S(1)}, bf16[32,512]{1,0:T(8,128)(2,1)S(1)}, u32[]{:S(2)}, u32[]{:S(2)}) collective-permute-start(bf16[32,512]{1,0:T(8,128)(2,1)S(1)} %dynamic-slice_bitcast_fusion), channel_id=1, source_target_pairs={{0,96},{2,98},{4,100},{6,102},{8,104},{10,106},{12,108},{14,110},{... | collective-permute-start | bytes 98312 | tf_op jit(solution)/shard_map/ppermute | solution.py:27
  15.2 2.5 %collective-permute-start = (bf16[64,512]{1,0:T(8,128)(2,1)S(1)}, bf16[64,512]{1,0:T(8,128)(2,1)S(1)}, u32[]{:S(2)}, u32[]{:S(2)}) collective-permute-start(bf16[64,512]{1,0:T(8,128)(2,1)S(1)} %pad_maximum_fusion.5), channel_id=1, source_target_pairs={{0,6},{2,0},{4,2},{6,4},{8,14},{10,8},{12,10},{14,12},{16,22},{18,... | collective-permute-start | bytes 196616 | tf_op jit(solution)/shard_map/ppermute | solution.py:27
  19.8 2.8 %collective-permute-start.21 = (bf16[4,32,512]{2,1,0:T(8,128)(2,1)S(1)}, bf16[4,32,512]{2,1,0:T(8,128)(2,1)S(1)}, u32[]{:S(2)}, u32[]{:S(2)}) collective-permute-start(bf16[4,32,512]{2,1,0:T(8,128)(2,1)S(1)} %get-tuple-element.15), channel_id=1, source_target_pairs={{0,24},{2,26},{4,28},{6,30},{8,0},{10,2},{12,4},{14,6},{16,8},{18,... | collective-permute-start | bytes 393224 | tf_op jit(solution)/shard_map/ppermute | solution.py:27
  24.5 3.4 %collective-permute-start.22 = (bf16[4,32,512]{2,1,0:T(8,128)(2,1)S(1)}, bf16[4,32,512]{2,1,0:T(8,128)(2,1)S(1)}, u32[]{:S(2)}, u32[]{:S(2)}) collective-permute-start(bf16[4,32,512]{2,1,0:T(8,128)(2,1)S(1)} %collective-permute-done.21), channel_id=1, source_target_pairs={{0,24},{2,26},{4,28},{6,30},{8,0},{10,2},{12,4},{14,6},{16,8},{18,... | collective-permute-start | bytes 393224 | tf_op jit(solution)/shard_map/ppermute | solution.py:27
  28.0 2.0 %collective-permute-start.10 = (bf16[4,32,512]{2,1,0:T(8,128)(2,1)S(1)}, bf16[4,32,512]{2,1,0:T(8,128)(2,1)S(1)}, u32[]{:S(2)}, u32[]{:S(2)}) collective-permute-start(bf16[4,32,512]{2,1,0:T(8,128)(2,1)S(1)} %get-tuple-element.9), channel_id=1, source_target_pairs={{0,32},{2,34},{4,36},{6,38},{8,40},{10,42},{12,44},{14,46},{16,48}... | collective-permute-start | bytes 393224 | tf_op jit(solution)/shard_map/ppermute | solution.py:27
  30.3 1.9 %collective-permute-start.23 = (bf16[4,4,32,512]{3,2,1,0:T(8,128)(2,1)S(1)}, bf16[4,4,32,512]{3,2,1,0:T(8,128)(2,1)S(1)}, u32[]{:S(2)}, u32[]{:S(2)}) collective-permute-start(bf16[4,4,32,512]{3,2,1,0:T(8,128)(2,1)S(1)} %pad_maximum_fusion.2.refs_11_), channel_id=1, source_target_pairs={{0,2},{2,4},{4,6},{6,0},{8,10},{10,12},{12,14},{14,8},{16,18},{18,... | collective-permute-start | bytes 1572872 | tf_op jit(solution)/shard_map/ppermute | solution.py:27
  32.3 3.1 %fusion = f32[1024]{0:T(1024)S(1)} fusion(bf16[1024,2048]{1,0:T(8,128)(2,1)} %param.13), kind=kLoop, calls=%fused_computation.2 | loop fusion | flops 6290432 | bytes 4198400 | tf_op jit(solution)/shard_map/reduce_sum | solution.py:62
  36.5 3.2 %collective-permute-start.5 = (bf16[4,32,512]{2,1,0:T(8,128)(2,1)S(1)}, bf16[4,32,512]{2,1,0:T(8,128)(2,1)S(1)}, u32[]{:S(2)}, u32[]{:S(2)}) collective-permute-start(bf16[4,32,512]{2,1,0:T(8,128)(2,1)S(1)} %get-tuple-element.10), channel_id=1, source_target_pairs={{0,24},{2,26},{4,28},{6,30},{8,0},{10,2},{12,4},{14,6},{16,8},{18,... | collective-permute-start | bytes 393224 | tf_op jit(solution)/shard_map/ppermute | solution.py:27
  39.7 1.5 collective-permute-start.11
  42.3 2.7 %collective-permute-done.11 = bf16[4,32,512]{2,1,0:T(8,128)(2,1)S(1)} collective-permute-done((bf16[4,32,512]{2,1,0:T(8,128)(2,1)S(1)}, bf16[4,32,512]{2,1,0:T(8,128)(2,1)S(1)}, u32[]{:S(2)}, u32[]{:S(2)}) %collective-permute-start.11) | collective-permute-done | bytes 131104 | tf_op jit(solution)/shard_map/ppermute | solution.py:27
  45.2 2.7 %collective-permute-start.14 = (bf16[4,4,32,512]{3,2,1,0:T(8,128)(2,1)S(1)}, bf16[4,4,32,512]{3,2,1,0:T(8,128)(2,1)}, u32[]{:S(2)}, u32[]{:S(2)}) collective-permute-start(bf16[4,4,32,512]{3,2,1,0:T(8,128)(2,1)S(1)} %pad_maximum_fusion.1.refs_6_), channel_id=1, source_target_pairs={{0,24},{2,26},{4,28},{6,30},{8,0},{10,2},{12,4},{14,6},{16,8},{18,... | collective-permute-start | bytes 1572872 | tf_op jit(solution)/shard_map/ppermute | solution.py:27
  48.3 2.4 %collective-permute-start.7 = (bf16[4,4,32,512]{3,2,1,0:T(8,128)(2,1)S(1)}, bf16[4,4,32,512]{3,2,1,0:T(8,128)(2,1)}, u32[]{:S(2)}, u32[]{:S(2)}) collective-permute-start(bf16[4,4,32,512]{3,2,1,0:T(8,128)(2,1)S(1)} %pad_maximum_fusion.refs_1_), channel_id=1, source_target_pairs={{0,96},{2,98},{4,100},{6,102},{8,104},{10,106},{12,108},{14,110},{... | collective-permute-start | bytes 1572872 | tf_op jit(solution)/shard_map/ppermute | solution.py:27
  50.7 3.0 %fusion.2.refs_0_ = bf16[1024,2048]{1,0:T(8,128)(2,1)} fusion(bf16[1024,2048]{1,0:T(8,128)(2,1)S(1)} %copy-done.2, f32[2048]{0:T(1024)S(1)} %convert_element_type.31, f32[1024]{0:T(1024)S(1)} %add_rsqrt_fusion), kind=kLoop, calls=%fused_computation.4 | loop fusion | flops 8388608 | bytes 8400896 | tf_op jit(solution)/shard_map/convert_element_type | solution.py:308
  53.7 3.3 %collective-permute-done.24.refs_13_ = bf16[4,4,32,512]{3,2,1,0:T(8,128)(2,1)S(1)} collective-permute-done((bf16[4,4,32,512]{3,2,1,0:T(8,128)(2,1)S(1)}, bf16[4,4,32,512]{3,2,1,0:T(8,128)(2,1)S(1)}, u32[]{:S(2)}, u32[]{:S(2)}) %collective-permute-start.24) | collective-permute-done | bytes 524320 | tf_op jit(solution)/shard_map/ppermute | solution.py:27
  57.8 1.5 dynamic-slice_select_fusion.refs_16_
  59.3 10.0 %collective-permute-done.13.refs_7_ = bf16[4,4,32,512]{3,2,1,0:T(8,128)(2,1)S(1)} collective-permute-done((bf16[4,4,32,512]{3,2,1,0:T(8,128)(2,1)S(1)}, bf16[4,4,32,512]{3,2,1,0:T(8,128)(2,1)S(1)}, u32[]{:S(2)}, u32[]{:S(2)}) %collective-permute-start.13) | collective-permute-done | bytes 524320 | tf_op jit(solution)/shard_map/ppermute | solution.py:27
  69.6 1.7 %slice.37 = bf16[2,4,32,512]{3,2,1,0:T(8,128)(2,1)} slice(bf16[4,4,32,512]{3,2,1,0:T(8,128)(2,1)} %collective-permute-done.14.refs_8_), slice={[2:4], [0:4], [0:32], [0:512]} | slice | bytes 524288 | tf_op jit(solution)/shard_map/slice | solution.py:43
  71.3 2.7 %collective-permute-start.16 = (bf16[2,4,32,512]{3,2,1,0:T(8,128)(2,1)}, bf16[2,4,32,512]{3,2,1,0:T(8,128)(2,1)S(1)}, u32[]{:S(2)}, u32[]{:S(2)}) collective-permute-start(bf16[2,4,32,512]{3,2,1,0:T(8,128)(2,1)} %slice.37), channel_id=1, source_target_pairs={{0,24},{2,26},{4,28},{6,30},{8,0},{10,2},{12,4},{14,6},{16,8},{18,... | collective-permute-start | bytes 786440 | tf_op jit(solution)/shard_map/ppermute | solution.py:27
  73.9 1.7 %slice.33 = bf16[2,4,32,512]{3,2,1,0:T(8,128)(2,1)} slice(bf16[4,4,32,512]{3,2,1,0:T(8,128)(2,1)} %collective-permute-done.6.refs_2_), slice={[0:2], [0:4], [0:32], [0:512]} | slice | bytes 524288 | tf_op jit(solution)/shard_map/slice | solution.py:43
  75.6 1.7 %slice.34 = bf16[2,4,32,512]{3,2,1,0:T(8,128)(2,1)} slice(bf16[4,4,32,512]{3,2,1,0:T(8,128)(2,1)} %collective-permute-done.7.refs_3_), slice={[2:4], [0:4], [0:32], [0:512]} | slice | bytes 524288 | tf_op jit(solution)/shard_map/slice | solution.py:43
  77.3 2.7 %collective-permute-start.9 = (bf16[2,4,32,512]{3,2,1,0:T(8,128)(2,1)}, bf16[2,4,32,512]{3,2,1,0:T(8,128)(2,1)S(1)}, u32[]{:S(2)}, u32[]{:S(2)}) collective-permute-start(bf16[2,4,32,512]{3,2,1,0:T(8,128)(2,1)} %slice.34), channel_id=1, source_target_pairs={{0,96},{2,98},{4,100},{6,102},{8,104},{10,106},{12,108},{14,110},{... | collective-permute-start | bytes 786440 | tf_op jit(solution)/shard_map/ppermute | solution.py:27
  80.7 6.7 %collective-permute-done.8.refs_4_ = bf16[2,4,32,512]{3,2,1,0:T(8,128)(2,1)S(1)} collective-permute-done((bf16[2,4,32,512]{3,2,1,0:T(8,128)(2,1)}, bf16[2,4,32,512]{3,2,1,0:T(8,128)(2,1)S(1)}, u32[]{:S(2)}, u32[]{:S(2)}) %collective-permute-start.8) | collective-permute-done | bytes 262176 | tf_op jit(solution)/shard_map/ppermute | solution.py:27
  87.4 1.9 %collective-permute-done.9.refs_5_ = bf16[2,4,32,512]{3,2,1,0:T(8,128)(2,1)S(1)} collective-permute-done((bf16[2,4,32,512]{3,2,1,0:T(8,128)(2,1)}, bf16[2,4,32,512]{3,2,1,0:T(8,128)(2,1)S(1)}, u32[]{:S(2)}, u32[]{:S(2)}) %collective-permute-start.9) | collective-permute-done | bytes 262176 | tf_op jit(solution)/shard_map/ppermute | solution.py:27
  90.0 10.0 %mixer_other.1 = f32[512,2048]{1,0:T(8,128)} custom-call(bf16[1024,2048]{1,0:T(8,128)(2,1)} %fusion.2.refs_0_, bf16[4,4,32,512]{3,2,1,0:T(8,128)(2,1)} %copy-done.7, bf16[4,4,32,512]{3,2,1,0:T(8,128)(2,1)} %collective-permute-done.6.refs_2_, bf16[4,4,32,512]{3,2,1,0:T(8,128)(2,1)} %collective-permute-done.7.refs_3_, bf16[2,4,32,512]{3,2,1,0:T(8,128)(2,1)} %copy-done.15, ...), custom_call_target="tpu_custom_call" | custom-call | tf_op jit(solution)/shard_map/mixer_other/pallas_call | solution.py:145
  100.0 9.3 %collective-permute-start.27 = (f32[512,2048]{1,0:T(8,128)}, f32[512,2048]{1,0:T(8,128)}, u32[]{:S(2)}, u32[]{:S(2)}) collective-permute-start(f32[512,2048]{1,0:T(8,128)} %mixer_other.1), channel_id=1, source_target_pairs={{0,1},{1,0},{2,3},{3,2},{4,5},{5,4},{6,7},{7,6},{8,9},{9,8},{10,11... | collective-permute-start | bytes 12582920 | tf_op jit(solution)/shard_map/ppermute | solution.py:315
  109.4 9.9 %mixer_own.1 = f32[512,2048]{1,0:T(8,128)} custom-call(bf16[1024,2048]{1,0:T(8,128)(2,1)} %fusion.2.refs_0_, bf16[4,4,32,512]{3,2,1,0:T(8,128)(2,1)} %copy-done.7, bf16[4,4,32,512]{3,2,1,0:T(8,128)(2,1)} %collective-permute-done.6.refs_2_, bf16[4,4,32,512]{3,2,1,0:T(8,128)(2,1)} %collective-permute-done.7.refs_3_, bf16[2,4,32,512]{3,2,1,0:T(8,128)(2,1)} %copy-done.15, ...), custom_call_target="tpu_custom_call" | custom-call | tf_op jit(solution)/shard_map/mixer_own/pallas_call | solution.py:145
  119.3 1.3 collective-permute-done.27
  120.7 4.6 %fusion.3 = (f32[512]{0:T(512)S(1)}, bf16[512,2048]{1,0:T(8,128)(2,1)S(1)}) fusion(f32[512,2048]{1,0:T(8,128)} %mixer_own.1, f32[512,2048]{1,0:T(8,128)} %collective-permute-done.27, bf16[1024,2048]{1,0:T(8,128)(2,1)S(1)} %copy-done.3, s32[]{:T(128)S(6)} %select_n.211), kind=kLoop, calls=%fused_computation.7 | loop fusion | flops 7339520 | bytes 12584964 | tf_op jit(solution)/shard_map/reduce_sum | solution.py:62
  125.3 1.9 %fusion.5.n_hbm = bf16[512,2048]{1,0:T(8,128)(2,1)} fusion(bf16[512,2048]{1,0:T(8,128)(2,1)S(1)} %get-tuple-element.6.h_hbm, f32[2048]{0:T(1024)S(1)} %convert_element_type.35, f32[512]{0:T(512)S(1)} %add_rsqrt_fusion.1), kind=kLoop, calls=%fused_computation.9 | loop fusion | flops 4194304 | bytes 4204544 | tf_op jit(solution)/shard_map/convert_element_type | solution.py:319
  127.2 7.6 %all-gather.3.cloned.1.call-done = bf16[12288,1408]{1,0:T(8,128)(2,1)} async-done(((bf16[96,1408]{1,0:T(8,128)(2,1)}), bf16[12288,1408]{1,0:T(8,128)(2,1)}) %all-gather.3.cloned.1.call-update) | async-done | bytes 34603024 | tf_op jit(solution)/shard_map/all_gather | solution.py:292
  134.9 22.4 %ffn.1 = bf16[512,2048]{1,0:T(8,128)(2,1)} custom-call(bf16[512,2048]{1,0:T(8,128)(2,1)} %copy-done.4, bf16[512,2048]{1,0:T(8,128)(2,1)} %fusion.5.n_hbm, bf16[2,2,32,96,1408]{4,3,2,1,0:T(8,128)(2,1)} %bitcast.41), custom_call_target="tpu_custom_call" | custom-call | tf_op jit(solution)/shard_map/ffn/pallas_call | solution.py:242
  (105 shorter events, 12.0 us)
Async XLA Ops:
  6.5 73.4 %copy-start = (bf16[4,128]{1,0:T(4,128)(2,1)S(1)}, bf16[4,128]{1,0:T(4,128)(2,1)}, u32[]{:S(2)}) copy-start(bf16[4,128]{1,0:T(4,128)(2,1)} %param.18) | copy-start | bytes 3076
  6.5 128.3 %all-gather.3.cloned.1.call-start = ((), (), s32[]{:S(2)}) async-start(), calls=%async_computation | async-start | bytes 34873344 | tf_op jit(solution)/shard_map/all_gather | solution.py:292
  9.2 9.1 %collective-permute-start.17 = (bf16[32,512]{1,0:T(8,128)(2,1)S(1)}, bf16[32,512]{1,0:T(8,128)(2,1)S(1)}, u32[]{:S(2)}, u32[]{:S(2)}) collective-permute-start(bf16[32,512]{1,0:T(8,128)(2,1)S(1)} %dynamic-slice_bitcast_fusion), channel_id=1, source_target_pairs={{0,96},{2,98},{4,100},{6,102},{8,104},{10,106},{12,108},{14,110},{... | collective-permute-start | bytes 98312 | tf_op jit(solution)/shard_map/ppermute | solution.py:27
  13.7 5.2 %collective-permute-start.18 = (bf16[32,512]{1,0:T(8,128)(2,1)S(1)}, bf16[32,512]{1,0:T(8,128)(2,1)S(1)}, u32[]{:S(2)}, u32[]{:S(2)}) collective-permute-start(bf16[32,512]{1,0:T(8,128)(2,1)S(1)} %dynamic-slice_bitcast_fusion), channel_id=1, source_target_pairs={{0,64},{2,66},{4,68},{6,70},{8,72},{10,74},{12,76},{14,78},{16,80}... | collective-permute-start | bytes 98312 | tf_op jit(solution)/shard_map/ppermute | solution.py:27
  13.7 5.2 %collective-permute-start.19 = (bf16[32,512]{1,0:T(8,128)(2,1)S(1)}, bf16[32,512]{1,0:T(8,128)(2,1)S(1)}, u32[]{:S(2)}, u32[]{:S(2)}) collective-permute-start(bf16[32,512]{1,0:T(8,128)(2,1)S(1)} %dynamic-slice_bitcast_fusion), channel_id=1, source_target_pairs={{0,32},{2,34},{4,36},{6,38},{8,40},{10,42},{12,44},{14,46},{16,48}... | collective-permute-start | bytes 98312 | tf_op jit(solution)/shard_map/ppermute | solution.py:27
  15.2 7.3 %collective-permute-start = (bf16[64,512]{1,0:T(8,128)(2,1)S(1)}, bf16[64,512]{1,0:T(8,128)(2,1)S(1)}, u32[]{:S(2)}, u32[]{:S(2)}) collective-permute-start(bf16[64,512]{1,0:T(8,128)(2,1)S(1)} %pad_maximum_fusion.5), channel_id=1, source_target_pairs={{0,6},{2,0},{4,2},{6,4},{8,14},{10,8},{12,10},{14,12},{16,22},{18,... | collective-permute-start | bytes 196616 | tf_op jit(solution)/shard_map/ppermute | solution.py:27
  17.8 4.8 %collective-permute-start.1 = (bf16[64,512]{1,0:T(8,128)(2,1)S(1)}, bf16[64,512]{1,0:T(8,128)(2,1)S(1)}, u32[]{:S(2)}, u32[]{:S(2)}) collective-permute-start(bf16[64,512]{1,0:T(8,128)(2,1)S(1)} %pad_maximum_fusion.5), channel_id=1, source_target_pairs={{0,4},{2,6},{4,0},{6,2},{8,12},{10,14},{12,8},{14,10},{16,20},{18,... | collective-permute-start | bytes 196616 | tf_op jit(solution)/shard_map/ppermute | solution.py:27
  18.3 4.8 %collective-permute-start.2 = (bf16[64,512]{1,0:T(8,128)(2,1)S(1)}, bf16[64,512]{1,0:T(8,128)(2,1)S(1)}, u32[]{:S(2)}, u32[]{:S(2)}) collective-permute-start(bf16[64,512]{1,0:T(8,128)(2,1)S(1)} %pad_maximum_fusion.5), channel_id=1, source_target_pairs={{0,2},{2,4},{4,6},{6,0},{8,10},{10,12},{12,14},{14,8},{16,18},{18,... | collective-permute-start | bytes 196616 | tf_op jit(solution)/shard_map/ppermute | solution.py:27
  19.8 4.8 %collective-permute-start.21 = (bf16[4,32,512]{2,1,0:T(8,128)(2,1)S(1)}, bf16[4,32,512]{2,1,0:T(8,128)(2,1)S(1)}, u32[]{:S(2)}, u32[]{:S(2)}) collective-permute-start(bf16[4,32,512]{2,1,0:T(8,128)(2,1)S(1)} %get-tuple-element.15), channel_id=1, source_target_pairs={{0,24},{2,26},{4,28},{6,30},{8,0},{10,2},{12,4},{14,6},{16,8},{18,... | collective-permute-start | bytes 393224 | tf_op jit(solution)/shard_map/ppermute | solution.py:27
  22.6 7.4 %collective-permute-start.20 = (bf16[4,32,512]{2,1,0:T(8,128)(2,1)S(1)}, bf16[4,32,512]{2,1,0:T(8,128)(2,1)S(1)}, u32[]{:S(2)}, u32[]{:S(2)}) collective-permute-start(bf16[4,32,512]{2,1,0:T(8,128)(2,1)S(1)} %get-tuple-element.15), channel_id=1, source_target_pairs={{0,8},{2,10},{4,12},{6,14},{8,16},{10,18},{12,20},{14,22},{16,24},... | collective-permute-start | bytes 393224 | tf_op jit(solution)/shard_map/ppermute | solution.py:27
  23.3 27.4 %copy-start.2 = (bf16[1024,2048]{1,0:T(8,128)(2,1)S(1)}, bf16[1024,2048]{1,0:T(8,128)(2,1)}, u32[]{:S(2)}) copy-start(bf16[1024,2048]{1,0:T(8,128)(2,1)} %param.13) | copy-start | bytes 12582916
  24.5 5.7 %collective-permute-start.22 = (bf16[4,32,512]{2,1,0:T(8,128)(2,1)S(1)}, bf16[4,32,512]{2,1,0:T(8,128)(2,1)S(1)}, u32[]{:S(2)}, u32[]{:S(2)}) collective-permute-start(bf16[4,32,512]{2,1,0:T(8,128)(2,1)S(1)} %collective-permute-done.21), channel_id=1, source_target_pairs={{0,24},{2,26},{4,28},{6,30},{8,0},{10,2},{12,4},{14,6},{16,8},{18,... | collective-permute-start | bytes 393224 | tf_op jit(solution)/shard_map/ppermute | solution.py:27
  28.0 11.7 %collective-permute-start.10 = (bf16[4,32,512]{2,1,0:T(8,128)(2,1)S(1)}, bf16[4,32,512]{2,1,0:T(8,128)(2,1)S(1)}, u32[]{:S(2)}, u32[]{:S(2)}) collective-permute-start(bf16[4,32,512]{2,1,0:T(8,128)(2,1)S(1)} %get-tuple-element.9), channel_id=1, source_target_pairs={{0,32},{2,34},{4,36},{6,38},{8,40},{10,42},{12,44},{14,46},{16,48}... | collective-permute-start | bytes 393224 | tf_op jit(solution)/shard_map/ppermute | solution.py:27
  30.0 11.2 %collective-permute-start.3 = (bf16[4,32,512]{2,1,0:T(8,128)(2,1)S(1)}, bf16[4,32,512]{2,1,0:T(8,128)(2,1)S(1)}, u32[]{:S(2)}, u32[]{:S(2)}) collective-permute-start(bf16[4,32,512]{2,1,0:T(8,128)(2,1)S(1)} %get-tuple-element.10), channel_id=1, source_target_pairs={{0,8},{2,10},{4,12},{6,14},{8,16},{10,18},{12,20},{14,22},{16,24},... | collective-permute-start | bytes 393224 | tf_op jit(solution)/shard_map/ppermute | solution.py:27
  30.3 18.0 %collective-permute-start.23 = (bf16[4,4,32,512]{3,2,1,0:T(8,128)(2,1)S(1)}, bf16[4,4,32,512]{3,2,1,0:T(8,128)(2,1)S(1)}, u32[]{:S(2)}, u32[]{:S(2)}) collective-permute-start(bf16[4,4,32,512]{3,2,1,0:T(8,128)(2,1)S(1)} %pad_maximum_fusion.2.refs_11_), channel_id=1, source_target_pairs={{0,2},{2,4},{4,6},{6,0},{8,10},{10,12},{12,14},{14,8},{16,18},{18,... | collective-permute-start | bytes 1572872 | tf_op jit(solution)/shard_map/ppermute | solution.py:27
  35.4 5.8 %collective-permute-start.12 = (bf16[4,32,512]{2,1,0:T(8,128)(2,1)S(1)}, bf16[4,32,512]{2,1,0:T(8,128)(2,1)S(1)}, u32[]{:S(2)}, u32[]{:S(2)}) collective-permute-start(bf16[4,32,512]{2,1,0:T(8,128)(2,1)S(1)} %get-tuple-element.9), channel_id=1, source_target_pairs={{0,96},{2,98},{4,100},{6,102},{8,104},{10,106},{12,108},{14,110},{... | collective-permute-start | bytes 393224 | tf_op jit(solution)/shard_map/ppermute | solution.py:27
  36.5 8.6 %collective-permute-start.5 = (bf16[4,32,512]{2,1,0:T(8,128)(2,1)S(1)}, bf16[4,32,512]{2,1,0:T(8,128)(2,1)S(1)}, u32[]{:S(2)}, u32[]{:S(2)}) collective-permute-start(bf16[4,32,512]{2,1,0:T(8,128)(2,1)S(1)} %get-tuple-element.10), channel_id=1, source_target_pairs={{0,24},{2,26},{4,28},{6,30},{8,0},{10,2},{12,4},{14,6},{16,8},{18,... | collective-permute-start | bytes 393224 | tf_op jit(solution)/shard_map/ppermute | solution.py:27
  39.7 5.3 %collective-permute-start.11 = (bf16[4,32,512]{2,1,0:T(8,128)(2,1)S(1)}, bf16[4,32,512]{2,1,0:T(8,128)(2,1)S(1)}, u32[]{:S(2)}, u32[]{:S(2)}) collective-permute-start(bf16[4,32,512]{2,1,0:T(8,128)(2,1)S(1)} %collective-permute-done.10), channel_id=1, source_target_pairs={{0,32},{2,34},{4,36},{6,38},{8,40},{10,42},{12,44},{14,46},{16,48}... | collective-permute-start | bytes 393224 | tf_op jit(solution)/shard_map/ppermute | solution.py:27
  41.2 6.7 %collective-permute-start.4 = (bf16[4,32,512]{2,1,0:T(8,128)(2,1)S(1)}, bf16[4,32,512]{2,1,0:T(8,128)(2,1)S(1)}, u32[]{:S(2)}, u32[]{:S(2)}) collective-permute-start(bf16[4,32,512]{2,1,0:T(8,128)(2,1)S(1)} %collective-permute-done.3), channel_id=1, source_target_pairs={{0,8},{2,10},{4,12},{6,14},{8,16},{10,18},{12,20},{14,22},{16,24},... | collective-permute-start | bytes 393224 | tf_op jit(solution)/shard_map/ppermute | solution.py:27
  41.2 15.8 %collective-permute-start.24 = (bf16[4,4,32,512]{3,2,1,0:T(8,128)(2,1)S(1)}, bf16[4,4,32,512]{3,2,1,0:T(8,128)(2,1)S(1)}, u32[]{:S(2)}, u32[]{:S(2)}) collective-permute-start(bf16[4,4,32,512]{3,2,1,0:T(8,128)(2,1)S(1)} %pad_maximum_fusion.2.refs_11_), channel_id=1, source_target_pairs={{0,6},{2,0},{4,2},{6,4},{8,14},{10,8},{12,10},{14,12},{16,22},{18,... | collective-permute-start | bytes 1572872 | tf_op jit(solution)/shard_map/ppermute | solution.py:27
  45.1 24.2 %collective-permute-start.13 = (bf16[4,4,32,512]{3,2,1,0:T(8,128)(2,1)S(1)}, bf16[4,4,32,512]{3,2,1,0:T(8,128)(2,1)S(1)}, u32[]{:S(2)}, u32[]{:S(2)}) collective-permute-start(bf16[4,4,32,512]{3,2,1,0:T(8,128)(2,1)S(1)} %pad_maximum_fusion.1.refs_6_), channel_id=1, source_target_pairs={{0,8},{2,10},{4,12},{6,14},{8,16},{10,18},{12,20},{14,22},{16,24},... | collective-permute-start | bytes 1572872 | tf_op jit(solution)/shard_map/ppermute | solution.py:27
  45.2 24.1 %collective-permute-start.14 = (bf16[4,4,32,512]{3,2,1,0:T(8,128)(2,1)S(1)}, bf16[4,4,32,512]{3,2,1,0:T(8,128)(2,1)}, u32[]{:S(2)}, u32[]{:S(2)}) collective-permute-start(bf16[4,4,32,512]{3,2,1,0:T(8,128)(2,1)S(1)} %pad_maximum_fusion.1.refs_6_), channel_id=1, source_target_pairs={{0,24},{2,26},{4,28},{6,30},{8,0},{10,2},{12,4},{14,6},{16,8},{18,... | collective-permute-start | bytes 1572872 | tf_op jit(solution)/shard_map/ppermute | solution.py:27
  47.9 23.3 %collective-permute-start.6 = (bf16[4,4,32,512]{3,2,1,0:T(8,128)(2,1)S(1)}, bf16[4,4,32,512]{3,2,1,0:T(8,128)(2,1)}, u32[]{:S(2)}, u32[]{:S(2)}) collective-permute-start(bf16[4,4,32,512]{3,2,1,0:T(8,128)(2,1)S(1)} %pad_maximum_fusion.refs_1_), channel_id=1, source_target_pairs={{0,32},{2,34},{4,36},{6,38},{8,40},{10,42},{12,44},{14,46},{16,48}... | collective-permute-start | bytes 1572872 | tf_op jit(solution)/shard_map/ppermute | solution.py:27
  48.3 27.3 %collective-permute-start.7 = (bf16[4,4,32,512]{3,2,1,0:T(8,128)(2,1)S(1)}, bf16[4,4,32,512]{3,2,1,0:T(8,128)(2,1)}, u32[]{:S(2)}, u32[]{:S(2)}) collective-permute-start(bf16[4,4,32,512]{3,2,1,0:T(8,128)(2,1)S(1)} %pad_maximum_fusion.refs_1_), channel_id=1, source_target_pairs={{0,96},{2,98},{4,100},{6,102},{8,104},{10,106},{12,108},{14,110},{... | collective-permute-start | bytes 1572872 | tf_op jit(solution)/shard_map/ppermute | solution.py:27
  57.0 32.3 %copy-start.9 = (bf16[4,4,32,512]{3,2,1,0:T(8,128)(2,1)}, bf16[4,4,32,512]{3,2,1,0:T(8,128)(2,1)S(1)}, u32[]{:S(2)}) copy-start(bf16[4,4,32,512]{3,2,1,0:T(8,128)(2,1)S(1)} %collective-permute-done.24.refs_13_) | copy-start | bytes 1572868
  57.0 20.2 %collective-permute-start.25 = (bf16[2,4,32,512]{3,2,1,0:T(8,128)(2,1)S(1)}, bf16[2,4,32,512]{3,2,1,0:T(8,128)(2,1)S(1)}, u32[]{:S(2)}, u32[]{:S(2)}) collective-permute-start(bf16[2,4,32,512]{3,2,1,0:T(8,128)(2,1)S(1)} %slice.38), channel_id=1, source_target_pairs={{0,2},{2,4},{4,6},{6,0},{8,10},{10,12},{12,14},{14,8},{16,18},{18,... | collective-permute-start | bytes 786440 | tf_op jit(solution)/shard_map/ppermute | solution.py:27
  69.3 11.4 %collective-permute-start.26 = (bf16[2,4,32,512]{3,2,1,0:T(8,128)(2,1)S(1)}, bf16[2,4,32,512]{3,2,1,0:T(8,128)(2,1)S(1)}, u32[]{:S(2)}, u32[]{:S(2)}) collective-permute-start(bf16[2,4,32,512]{3,2,1,0:T(8,128)(2,1)S(1)} %slice.39), channel_id=1, source_target_pairs={{0,6},{2,0},{4,2},{6,4},{8,14},{10,8},{12,10},{14,12},{16,22},{18,... | collective-permute-start | bytes 786440 | tf_op jit(solution)/shard_map/ppermute | solution.py:27
  69.3 11.4 %collective-permute-start.15 = (bf16[2,4,32,512]{3,2,1,0:T(8,128)(2,1)S(1)}, bf16[2,4,32,512]{3,2,1,0:T(8,128)(2,1)S(1)}, u32[]{:S(2)}, u32[]{:S(2)}) collective-permute-start(bf16[2,4,32,512]{3,2,1,0:T(8,128)(2,1)S(1)} %slice.36), channel_id=1, source_target_pairs={{0,8},{2,10},{4,12},{6,14},{8,16},{10,18},{12,20},{14,22},{16,24},... | collective-permute-start | bytes 786440 | tf_op jit(solution)/shard_map/ppermute | solution.py:27
  71.3 9.5 %collective-permute-start.16 = (bf16[2,4,32,512]{3,2,1,0:T(8,128)(2,1)}, bf16[2,4,32,512]{3,2,1,0:T(8,128)(2,1)S(1)}, u32[]{:S(2)}, u32[]{:S(2)}) collective-permute-start(bf16[2,4,32,512]{3,2,1,0:T(8,128)(2,1)} %slice.37), channel_id=1, source_target_pairs={{0,24},{2,26},{4,28},{6,30},{8,0},{10,2},{12,4},{14,6},{16,8},{18,... | collective-permute-start | bytes 786440 | tf_op jit(solution)/shard_map/ppermute | solution.py:27
  75.6 11.8 %collective-permute-start.8 = (bf16[2,4,32,512]{3,2,1,0:T(8,128)(2,1)}, bf16[2,4,32,512]{3,2,1,0:T(8,128)(2,1)S(1)}, u32[]{:S(2)}, u32[]{:S(2)}) collective-permute-start(bf16[2,4,32,512]{3,2,1,0:T(8,128)(2,1)} %slice.33), channel_id=1, source_target_pairs={{0,32},{2,34},{4,36},{6,38},{8,40},{10,42},{12,44},{14,46},{16,48}... | collective-permute-start | bytes 786440 | tf_op jit(solution)/shard_map/ppermute | solution.py:27
  77.3 12.0 %collective-permute-start.9 = (bf16[2,4,32,512]{3,2,1,0:T(8,128)(2,1)}, bf16[2,4,32,512]{3,2,1,0:T(8,128)(2,1)S(1)}, u32[]{:S(2)}, u32[]{:S(2)}) collective-permute-start(bf16[2,4,32,512]{3,2,1,0:T(8,128)(2,1)} %slice.34), channel_id=1, source_target_pairs={{0,96},{2,98},{4,100},{6,102},{8,104},{10,106},{12,108},{14,110},{... | collective-permute-start | bytes 786440 | tf_op jit(solution)/shard_map/ppermute | solution.py:27
  100.0 20.6 %collective-permute-start.27 = (f32[512,2048]{1,0:T(8,128)}, f32[512,2048]{1,0:T(8,128)}, u32[]{:S(2)}, u32[]{:S(2)}) collective-permute-start(f32[512,2048]{1,0:T(8,128)} %mixer_other.1), channel_id=1, source_target_pairs={{0,1},{1,0},{2,3},{3,2},{4,5},{5,4},{6,7},{7,6},{8,9},{9,8},{10,11... | collective-permute-start | bytes 12582920 | tf_op jit(solution)/shard_map/ppermute | solution.py:315
  (18 other events, 210.5 us)
Sparse Core Ops, SparseCore 0:
  10.3 124.4 all-gather.2
